TPU v7x, 256 devices: a whole 4x4x8 slice. The times are simulated.
256 devices in a mesh: ep: 64 (over z, y, core), tp: 4 (over x).
Axes of the slice: x: 4, y: 4, z: 8, core: 2. Of those that a mesh axis runs over, the one named last changes fastest.
Arguments:
- resid: bfloat16 [2048, 2048], P('ep'), may hold values from -6 to 6
- mix_gain: bfloat16 [2048], replicated, may hold values from 0.099609375 to 1.8984375
- proj_x: bfloat16 [2048, 512], P(None, 'tp'), may hold values from -0.125 to 0.125
- proj_z: bfloat16 [2048, 512], P(None, 'tp'), may hold values from -0.125 to 0.125
- proj_b: bfloat16 [2048, 512], P(None, 'tp'), may hold values from -0.125 to 0.125
- proj_c: bfloat16 [2048, 512], P(None, 'tp'), may hold values from -0.125 to 0.125
- proj_step: bfloat16 [2048, 8], replicated, may hold values from -0.125 to 0.125
- step_bias: float32 [8], P('tp'), may hold values from -5 to -1
- decay_rate: float32 [8], P('tp'), may hold values from 1 to 16
- conv_taps: bfloat16 [3, 4, 512], P(None, None, 'tp'), may hold values from -3 to 3
- conv_state: bfloat16 [2048, 3, 3, 512], P('ep', None, None, 'tp'), may hold values from -6 to 6
- scan_state: float32 [2048, 8, 64, 128], P('ep', 'tp'), may hold values from -2.5 to 2.5
- inner_gain: bfloat16 [512], P('tp'), may hold values from 0.099609375 to 1.8984375
- proj_out: bfloat16 [512, 2048], P('tp'), may hold values from -0.25 to 0.25
- post_gain: bfloat16 [2048], replicated, may hold values from 0.099609375 to 1.8984375
- ffn_gain: bfloat16 [2048], replicated, may hold values from 0.099609375 to 1.8984375
- group_router: bfloat16 [2048, 2], replicated, may hold values from -0.125 to 0.125
- expert_router: bfloat16 [2048, 64], replicated, may hold values from -0.125 to 0.125
- route_experts: int32 [2048, 4], P('ep'), may hold values from 0 to 63, as said below
- expert_gate: bfloat16 [64, 2048, 1024], P('ep', None, 'tp'), may hold values from -0.125 to 0.125
- expert_up: bfloat16 [64, 2048, 1024], P('ep', None, 'tp'), may hold values from -0.125 to 0.125
- expert_down: bfloat16 [64, 1024, 2048], P('ep', 'tp')
- dense_switch: bfloat16 [2048], replicated, may hold values from -0.125 to 0.125
- dense_gate: bfloat16 [2048, 2048], P('ep', 'tp'), may hold values from -0.125 to 0.125
- dense_up: bfloat16 [2048, 2048], P('ep', 'tp'), may hold values from -0.125 to 0.125
- dense_down: bfloat16 [2048, 2048], P('ep', 'tp')
- out_gain: bfloat16 [2048], P('tp'), may hold values from 0.099609375 to 1.8984375
Outputs:
- layer_out: bfloat16 [2048, 2048], P('ep', 'tp')
- new_state: float32 [2048, 8, 64, 128], P('ep', 'tp')
- new_conv: bfloat16 [2048, 3, 3, 512], P('ep', None, None, 'tp')
Inputs may be any that keep to these rules, and one draw needn't show every extreme that they name: `route_experts`: each row names 4 different experts, all from one group of 32 consecutive expert numbers. Within each aligned block of 32 rows (the rows of one index of ep) no expert is named more than 4 times, and one expert, the same in every block, is named exactly 4 times in every block.
All inputs are finite; a program needn't handle non-finite values.
Results may differ from a plain program's by a relative error of at most 0.019.
Values may be sent and summed in bfloat16 or wider, within the bound.
No kernel may reach another device: no remote copies, remote signals or barrier semaphores. Data moves between devices by JAX's collectives and lax.ppermute only.
A program may use at most 64 MiB of HBM per device.

v0:
```python
import jax
import jax.numpy as jnp
from jax import lax
from jax.sharding import Mesh
from jax.experimental import pallas as pl
from jax.experimental.pallas import tpu as pltpu
from jax.sharding import PartitionSpec as P


EP = ("ep_0", "ep_1", "ep_2")


norm_eps = 1e-06
MIXER_VMEM = 16 * 2**20


def from_shift(array, axis, shift):
    count = lax.axis_size(axis)
    return lax.ppermute(array, axis, [(i, (i + shift) % count) for i in range(count)])


def from_all(array, axis):
    count = lax.axis_size(axis)
    return [array] + [from_shift(array, axis, s) for s in range(1, count)]


def scaled_rows(values, gain):
    values = values.astype(jnp.float32)
    mean_square = jnp.mean(values * values, axis=-1, keepdims=True)
    return values * lax.rsqrt(mean_square + norm_eps) * gain.astype(jnp.float32)


def dot32(a, b):
    return jnp.dot(a, b, preferred_element_type=jnp.float32)


def sum_of(arrays):
    total = arrays[0].astype(jnp.float32)
    for array in arrays[1:]:
        total = total + array.astype(jnp.float32)
    return total


def from_flip(array, axis, bit):
    count = lax.axis_size(axis)
    return lax.ppermute(array, axis, [(i, i ^ bit) for i in range(count)])


def silu(values):
    return values * (1.0 / (1.0 + jnp.exp(-values)))


def mixer_kernel(
    place,
    step_bias,
    decay_rate,
    resid,
    mix_gain,
    proj_x,
    proj_z,
    proj_b,
    proj_c,
    proj_step,
    conv_taps,
    conv_state,
    scan_state,
    inner_gain,
    proj_out,
    routes,
    part,
    new_state,
    new_conv,
    in_slot,
):
    seqs = resid.shape[0]
    slots = in_slot.shape[0]
    slot_ids = lax.broadcasted_iota(jnp.int32, (slots, seqs), 0)
    picked = jnp.zeros((slots, seqs), jnp.bool_)
    for k in range(routes.shape[0]):
        picked = picked | ((slot_ids >> 2) == routes[k : k + 1])
    earlier = lax.broadcasted_iota(jnp.int32, (seqs, seqs), 0) < lax.broadcasted_iota(
        jnp.int32, (seqs, seqs), 1
    )
    rank = dot32(
        jnp.where(picked, 1.0, 0.0).astype(jnp.bfloat16),
        jnp.where(earlier, 1.0, 0.0).astype(jnp.bfloat16),
    )
    in_slot[...] = jnp.where(
        picked & (rank.astype(jnp.int32) == (slot_ids & 3)), 1.0, 0.0
    ).astype(jnp.bfloat16)
    heads, head_dim, lanes = scan_state.shape[1:]
    values = resid[...].astype(jnp.float32)
    mean_square = jnp.mean(values * values, axis=-1, keepdims=True)
    normed = values * lax.rsqrt(mean_square + norm_eps) * mix_gain[...].astype(jnp.float32)
    normed = normed.astype(jnp.bfloat16)
    parts = []
    for k, proj in enumerate((proj_x, proj_b, proj_c)):
        fresh = dot32(normed, proj[...]).astype(jnp.bfloat16)
        taps = conv_taps[k].astype(jnp.float32)
        total = fresh.astype(jnp.float32) * taps[3:4]
        for pos in range(3):
            total = total + conv_state[k, pos].astype(jnp.float32) * taps[pos : pos + 1]
        new_conv[k, 0] = conv_state[k, 1]
        new_conv[k, 1] = conv_state[k, 2]
        new_conv[k, 2] = fresh
        parts.append(silu(total))
    xs, bs, cs = parts
    gate = silu(dot32(normed, proj_z[...])) * inner_gain[...].astype(jnp.float32)
    step_all = lax.dot_general(
        normed, proj_step[...], (((1,), (1,)), ((), ())), preferred_element_type=jnp.float32
    )
    head_ids = lax.broadcasted_iota(jnp.int32, step_all.shape, 1)
    lane_ids = lax.broadcasted_iota(jnp.int32, (seqs, lanes), 1)
    steps, keeps = [], []
    for h in range(heads):
        raw = jnp.sum(
            jnp.where(head_ids == place[0] * heads + h, step_all, 0.0), axis=1, keepdims=True
        )
        raw = raw + step_bias[h]
        step = jnp.maximum(raw, 0.0) + jnp.log1p(jnp.exp(-jnp.abs(raw)))
        steps.append(step)
        keeps.append(jnp.exp(-decay_rate[h] * step))
    driven = xs * jnp.where(lane_ids < head_dim, steps[0], steps[1])
    filler = jnp.zeros((lanes - seqs, lanes), jnp.float32)
    driven = jnp.concatenate([driven, filler], axis=0).T
    wide_ids = lax.broadcasted_iota(jnp.int32, (head_dim, lanes), 1)
    reads = [jnp.zeros((head_dim, lanes), jnp.float32) for _ in range(heads)]
    for t in range(seqs):
        for h in range(heads):
            column = driven[h * head_dim : (h + 1) * head_dim, t : t + 1]
            state = keeps[h][t : t + 1] * scan_state[t, h] + column * bs[t : t + 1]
            new_state[t, h] = state
            read = jnp.sum(state * cs[t : t + 1], axis=1, keepdims=True)
            reads[h] = jnp.where(wide_ids == t, read, reads[h])
    read = jnp.concatenate(reads, axis=0).T[:seqs]
    gated = (read * gate).astype(jnp.bfloat16)
    part[...] = dot32(gated, proj_out[...]).astype(jnp.bfloat16)


def mixer(slots, place, step_bias, decay_rate, *arrays):
    resid, conv_state, scan_state = arrays[0], arrays[8], arrays[9]
    smem = pl.BlockSpec(memory_space=pltpu.SMEM)
    vmem = pl.BlockSpec(memory_space=pltpu.VMEM)
    return pl.pallas_call(
        mixer_kernel,
        name="mixer",
        in_specs=[smem] * 3 + [vmem] * len(arrays),
        out_specs=[vmem] * 4,
        compiler_params=pltpu.CompilerParams(vmem_limit_bytes=MIXER_VMEM),
        out_shape=[
            jax.ShapeDtypeStruct(resid.shape, jnp.bfloat16),
            jax.ShapeDtypeStruct(scan_state.shape, jnp.float32),
            jax.ShapeDtypeStruct(conv_state.shape, jnp.bfloat16),
            jax.ShapeDtypeStruct((slots, resid.shape[0]), jnp.bfloat16),
        ],
    )(place, step_bias, decay_rate, *arrays)


def feeder_kernel(
    part_0, part_1, part_2, part_3, resid, post_gain, ffn_gain, in_slot, stream, feed, outgoing
):
    mixed = sum_of([part_0[...], part_1[...], part_2[...], part_3[...]])
    total = resid[...].astype(jnp.float32) + scaled_rows(mixed, post_gain[...])
    total = total.astype(jnp.bfloat16)
    stream[...] = total
    fed = scaled_rows(total, ffn_gain[...]).astype(jnp.bfloat16)
    feed[...] = fed
    outgoing[...] = dot32(in_slot[...], fed).astype(jnp.bfloat16)


def feeder(*arrays):
    vmem = pl.BlockSpec(memory_space=pltpu.VMEM)
    rows = jax.ShapeDtypeStruct(arrays[0].shape, jnp.bfloat16)
    return pl.pallas_call(
        feeder_kernel,
        name="feeder",
        in_specs=[vmem] * len(arrays),
        out_specs=[vmem] * 3,
        compiler_params=pltpu.CompilerParams(vmem_limit_bytes=MIXER_VMEM),
        out_shape=[
            rows,
            rows,
            jax.ShapeDtypeStruct((arrays[-1].shape[0], arrays[0].shape[1]), jnp.bfloat16),
        ],
    )(*arrays)


def on_device(
    resid,
    mix_gain,
    proj_x,
    proj_z,
    proj_b,
    proj_c,
    proj_step,
    step_bias,
    decay_rate,
    conv_taps,
    conv_state,
    scan_state,
    inner_gain,
    proj_out,
    post_gain,
    ffn_gain,
    group_router,
    expert_router,
    route_experts,
    expert_gate,
    expert_up,
    expert_down,
    dense_switch,
    dense_gate,
    dense_up,
    dense_down,
    out_gain,
):
    tp_index = lax.axis_index("tp")
    tp_count = lax.axis_size("tp")
    seqs, width = resid.shape
    quarter = width // tp_count
    units = dense_gate.shape[0]

    blocks = jnp.stack([dense_gate, dense_up, dense_down])[None]
    blocks = jnp.concatenate([blocks, from_flip(blocks, "ep_0", 4)])
    blocks = jnp.concatenate([blocks, from_flip(blocks, "ep_0", 2)])
    blocks = jnp.concatenate([blocks, from_flip(blocks, "ep_0", 1)])
    unit_rows = jnp.moveaxis(blocks, 0, 1).reshape(3, blocks.shape[0] * units, quarter)
    down = expert_down[0]
    down_parts = [
        lax.dynamic_slice_in_dim(down, ((tp_index + s) % tp_count) * quarter, quarter, 1)
        for s in range(tp_count)
    ]
    down_parts = [down_parts[0]] + [from_shift(down_parts[s], "tp", s) for s in range(1, tp_count)]

    expert_count = expert_router.shape[1]
    group_size = expert_count // group_router.shape[1]
    pick_count = route_experts.shape[1]
    capacity = 2 * seqs * pick_count // expert_count

    part, new_state, new_conv, in_slot = mixer(
        expert_count * capacity,
        jnp.full((1,), tp_index, jnp.int32),
        step_bias,
        decay_rate,
        resid,
        mix_gain[None],
        proj_x,
        proj_z,
        proj_b,
        proj_c,
        proj_step.T,
        conv_taps,
        conv_state.transpose(1, 2, 0, 3),
        scan_state,
        inner_gain[None],
        proj_out,
        route_experts.T,
    )
    new_conv = new_conv.transpose(2, 0, 1, 3)
    mixed_parts = from_all(part, "tp")
    stream, feed, outgoing = feeder(*mixed_parts, resid, post_gain[None], ffn_gain[None], in_slot)

    feed_quarter = lax.dynamic_slice_in_dim(feed, tp_index * quarter, quarter, 1)
    arrived = lax.all_to_all(outgoing.reshape(expert_count, capacity, width), EP, 0, 0, tiled=True)
    rows = arrived.reshape(expert_count * capacity, width)

    tokens = jnp.concatenate([feed_quarter, from_flip(feed_quarter, "ep_2", 1)], axis=0)
    tokens = jnp.concatenate(from_all(tokens, "ep_1"), axis=0)
    gate_rows, up_rows, down_rows = unit_rows
    across = (((1,), (1,)), ((), ()))
    gate_piece = lax.dot_general(tokens, gate_rows, across, preferred_element_type=jnp.float32)
    up_piece = lax.dot_general(tokens, up_rows, across, preferred_element_type=jnp.float32)
    pieces = jnp.stack([gate_piece, up_piece]).astype(jnp.bfloat16)
    sums = sum_of(from_all(pieces, "tp"))
    dense_hidden = (jax.nn.silu(sums[0]) * sums[1]).astype(jnp.bfloat16)
    dense_part = dot32(dense_hidden, down_rows).astype(jnp.bfloat16)
    lots = dense_part.reshape(lax.axis_size("ep_1"), 2 * seqs, quarter)
    lots = sum_of([lots[0]] + [from_shift(lots[b], "ep_1", -b) for b in range(1, lots.shape[0])])
    dense_part = lots[:seqs] + from_flip(lots[seqs:].astype(jnp.bfloat16), "ep_2", 1)
    dense_out = dense_part

    gate_value = dot32(rows, expert_gate[0])
    up_value = dot32(rows, expert_up[0])
    hidden = (jax.nn.silu(gate_value) * up_value).astype(jnp.bfloat16)
    hidden_parts = from_all(hidden, "tp")
    served = sum(dot32(r, w) for r, w in zip(hidden_parts, down_parts)).astype(jnp.bfloat16)
    returned = lax.all_to_all(
        served.reshape(expert_count, capacity, quarter), EP, 0, 0, tiled=True
    ).reshape(expert_count * capacity, quarter)

    features = (((0,), (1,)), ((), ()))
    group_exp = jnp.exp(
        lax.dot_general(group_router, feed, features, preferred_element_type=jnp.float32)
    )
    group_prob = group_exp / jnp.sum(group_exp, axis=0, keepdims=True)
    routes = route_experts.T
    group_ids = jnp.arange(group_router.shape[1], dtype=jnp.int32)[:, None]
    group_weight = jnp.sum(
        jnp.where(routes[:1] // group_size == group_ids, group_prob, 0.0), axis=0, keepdims=True
    )
    expert_ids = jnp.arange(expert_count, dtype=jnp.int32)[:, None]
    picked = expert_ids == routes[0:1]
    for k in range(1, pick_count):
        picked = picked | (expert_ids == routes[k : k + 1])
    logits = lax.dot_general(expert_router, feed, features, preferred_element_type=jnp.float32)
    pick_exp = jnp.exp(jnp.where(picked, logits, -jnp.inf))
    pick_weight = pick_exp / jnp.sum(pick_exp, axis=0, keepdims=True) * group_weight
    slot_weight = in_slot.astype(jnp.float32) * jnp.repeat(pick_weight, capacity, axis=0)
    weight_high = slot_weight.astype(jnp.bfloat16)
    weight_low = (slot_weight - weight_high.astype(jnp.float32)).astype(jnp.bfloat16)
    slotwise = (((0,), (0,)), ((), ()))
    routed = lax.dot_general(
        weight_high, returned, slotwise, preferred_element_type=jnp.float32
    ) + lax.dot_general(weight_low, returned, slotwise, preferred_element_type=jnp.float32)

    switch = jax.nn.sigmoid(dot32(feed, dense_switch))
    combined = routed + switch[:, None] * dense_out
    squares = jnp.sum(combined * combined, axis=1)
    total_square = sum_of(from_all(squares, "tp"))
    scale = lax.rsqrt(total_square / width + norm_eps)
    stream_part = lax.dynamic_slice_in_dim(stream, tp_index * quarter, quarter, 1).astype(
        jnp.float32
    )
    layer_out = (stream_part + combined * scale[:, None] * out_gain.astype(jnp.float32)).astype(
        jnp.bfloat16
    )
    return (layer_out, new_state, new_conv)


def solution(mesh):
    torus = Mesh(mesh.devices.reshape(8, 4, 2, mesh.shape["tp"]), ("ep_0", "ep_1", "ep_2", "tp"))
    in_specs = (
        P(EP, None),
        P(),
        P(None, "tp"),
        P(None, "tp"),
        P(None, "tp"),
        P(None, "tp"),
        P(),
        P("tp"),
        P("tp"),
        P(None, None, "tp"),
        P(EP, None, None, "tp"),
        P(EP, "tp", None, None),
        P("tp"),
        P("tp", None),
        P(),
        P(),
        P(),
        P(),
        P(EP, None),
        P(EP, None, "tp"),
        P(EP, None, "tp"),
        P(EP, "tp", None),
        P(),
        P(EP, "tp"),
        P(EP, "tp"),
        P(EP, "tp"),
        P("tp"),
    )
    out_specs = (P(EP, "tp"), P(EP, "tp", None, None), P(EP, None, None, "tp"))

    return jax.shard_map(
        on_device, mesh=torus, in_specs=in_specs, out_specs=out_specs, check_vma=False
    )
```

profile of v0, /device:TPU:32, one launch (start us, length us, event | category | flops | bytes accessed | tf_op | source)
XLA Modules:
  0.0 154.3 jit_solution(9827631998027304529)
XLA Ops:
  0.6 0.8 broadcast_in_dim.38.mix_gain
  1.4 1.6 %copy-done.1 = f32[32,2,64,128]{3,2,1,0:T(8,128)S(1)} copy-done((f32[32,2,64,128]{3,2,1,0:T(8,128)S(1)}, f32[32,2,64,128]{3,2,1,0:T(8,128)}, u32[]{:S(2)}) %copy-start.1) | copy-done | bytes 2097176
  3.0 1.0 copy-done.2
  4.1 1.0 copy-done.3
  5.1 1.0 copy-done.4
  6.2 1.0 copy-done.5
  7.2 1.0 copy-done.6
  8.2 0.9 copy-done.7
  9.1 0.9 copy-done.9
  10.0 0.8 copy-done.10
  10.8 0.7 copy-done.11
  11.5 0.7 copy-done.13
  12.1 0.7 copy-done.14
  12.8 0.7 copy-done.15
  14.2 7.2 %mixer.1 = (bf16[32,2048]{1,0:T(8,128)(2,1)S(1)}, f32[32,2,64,128]{3,2,1,0:T(8,128)}, bf16[3,3,32,128]{3,2,1,0:T(8,128)(2,1)}, bf16[256,32]{1,0:T(8,128)(2,1)S(1)}) custom-call(s32[1]{0:T(128)} %bitcast.place, f32[2]{0:T(128)S(1)} %copy-done.14, f32[2]{0:T(128)S(1)} %copy-done.15, bf16[32,2048]{1,0:T(8,128)(2,1)S(1)} %copy-done.7, ...), custom_call_target="tpu_custom_call" | custom-call | tf_op jit(solution)/shard_map/mixer/pallas_call | solution.py:144
  21.4 1.5 collective-permute-start
  22.9 2.7 %collective-permute-start.1 = (bf16[32,2048]{1,0:T(8,128)(2,1)S(1)}, bf16[32,2048]{1,0:T(8,128)(2,1)S(1)}, u32[]{:S(2)}, u32[]{:S(2)}) collective-permute-start(bf16[32,2048]{1,0:T(8,128)(2,1)S(1)} %get-tuple-element.10.part_0), channel_id=1, source_target_pairs={{0,2},{1,3},{2,0},{3,1},{4,6},{5,7},{6,4},{7,5},{8,10},{9,11},{10,... | collective-permute-start | bytes 393224 | tf_op jit(solution)/shard_map/ppermute | solution.py:19
  25.6 1.4 collective-permute-start.2
  27.0 0.9 dynamic-slice_bitcast_fusion.1
  28.6 6.4 %collective-permute-start.13 = (bf16[1,3,32,512]{3,2,1,0:T(8,128)(2,1)S(1)}, bf16[1,3,32,512]{3,2,1,0:T(8,128)(2,1)S(1)}, u32[]{:S(2)}, u32[]{:S(2)}) collective-permute-start(bf16[1,3,32,512]{3,2,1,0:T(8,128)(2,1)S(1)} %maximum_bitcast_fusion.1), channel_id=1, source_target_pairs={{0,128},{32,160},{64,192},{96,224},{128,0},{160,32},{192,64},{224,... | collective-permute-start | bytes 294920 | tf_op jit(solution)/shard_map/ppermute | solution.py:46
  35.1 3.6 %collective-permute-done.13 = bf16[1,3,32,512]{3,2,1,0:T(8,128)(2,1)S(1)} collective-permute-done((bf16[1,3,32,512]{3,2,1,0:T(8,128)(2,1)S(1)}, bf16[1,3,32,512]{3,2,1,0:T(8,128)(2,1)S(1)}, u32[]{:S(2)}, u32[]{:S(2)}) %collective-permute-start.13) | collective-permute-done | bytes 98336 | tf_op jit(solution)/shard_map/ppermute | solution.py:46
  38.7 2.6 %collective-permute-start.8 = (bf16[256,512]{1,0:T(8,128)(2,1)}, bf16[256,512]{1,0:T(8,128)(2,1)}, u32[]{:S(2)}, u32[]{:S(2)}) collective-permute-start(bf16[256,512]{1,0:T(8,128)(2,1)} %get-tuple-element.21), channel_id=1, source_target_pairs={{0,3},{1,0},{2,1},{3,2},{4,7},{5,4},{6,5},{7,6},{8,11},{9,8},{10,9... | collective-permute-start | bytes 786440 | tf_op jit(solution)/shard_map/ppermute | solution.py:19
  41.3 0.7 pad_maximum_fusion.2
  42.0 2.8 %collective-permute-start.14 = (bf16[2,3,32,512]{3,2,1,0:T(8,128)(2,1)}, bf16[2,3,32,512]{3,2,1,0:T(8,128)(2,1)}, u32[]{:S(2)}, u32[]{:S(2)}) collective-permute-start(bf16[2,3,32,512]{3,2,1,0:T(8,128)(2,1)} %pad_maximum_fusion.2), channel_id=1, source_target_pairs={{0,64},{32,96},{64,0},{96,32},{128,192},{160,224},{192,128},{224,1... | collective-permute-start | bytes 589832 | tf_op jit(solution)/shard_map/ppermute | solution.py:46
  44.9 0.7 feeder.1
  45.6 1.2 reshape.49
  46.8 9.8 %all-to-all-start = ((bf16[64,4,2048]{2,1,0:T(4,128)(2,1)}), bf16[64,4,2048]{2,1,0:T(4,128)(2,1)S(1)}, u32[]{:S(2)}, u32[]{:S(2)}) async-start(bf16[64,4,2048]{2,1,0:T(4,128)(2,1)} %reshape.49), calls=%async_computation | async-start | bytes 2097152 | tf_op jit(solution)/shard_map/all_to_all | solution.py:264
  57.2 0.9 collective-permute-done.9
  58.1 1.5 collective-permute-start.10
  59.6 2.7 %collective-permute-start.11 = (bf16[64,512]{1,0:T(8,128)(2,1)S(1)}, bf16[64,512]{1,0:T(8,128)(2,1)S(1)}, u32[]{:S(2)}, u32[]{:S(2)}) collective-permute-start(bf16[64,512]{1,0:T(8,128)(2,1)S(1)} %pad_maximum_fusion.3), channel_id=1, source_target_pairs={{0,16},{8,24},{16,0},{24,8},{1,17},{9,25},{17,1},{25,9},{2,18},{10... | collective-permute-start | bytes 196616 | tf_op jit(solution)/shard_map/ppermute | solution.py:19
  62.3 1.0 pad_maximum_fusion
  64.0 2.9 %collective-permute-start.12 = (bf16[64,512]{1,0:T(8,128)(2,1)S(1)}, bf16[64,512]{1,0:T(8,128)(2,1)S(1)}, u32[]{:S(2)}, u32[]{:S(2)}) collective-permute-start(bf16[64,512]{1,0:T(8,128)(2,1)S(1)} %pad_maximum_fusion.3), channel_id=1, source_target_pairs={{0,24},{8,0},{16,8},{24,16},{1,25},{9,1},{17,9},{25,17},{2,26},{10... | collective-permute-start | bytes 196616 | tf_op jit(solution)/shard_map/ppermute | solution.py:19
  66.9 1.4 collective-permute-done.11
  68.3 1.0 collective-permute-done.12
  69.3 19.4 %collective-permute-done.15 = bf16[4,3,32,512]{3,2,1,0:T(8,128)(2,1)S(1)} collective-permute-done((bf16[4,3,32,512]{3,2,1,0:T(8,128)(2,1)S(1)}, bf16[4,3,32,512]{3,2,1,0:T(8,128)(2,1)S(1)}, u32[]{:S(2)}, u32[]{:S(2)}) %collective-permute-start.15) | collective-permute-done | bytes 393248 | tf_op jit(solution)/shard_map/ppermute | solution.py:46
  88.7 1.1 maximum_bitcast_fusion
  90.5 1.5 collective-permute-start.17
  92.0 1.7 %collective-permute-start.18 = (bf16[2,256,256]{2,1,0:T(8,128)(2,1)S(1)}, bf16[2,256,256]{2,1,0:T(8,128)(2,1)S(1)}, u32[]{:S(2)}, u32[]{:S(2)}) collective-permute-start(bf16[2,256,256]{2,1,0:T(8,128)(2,1)S(1)} %pad_maximum_fusion.1), channel_id=1, source_target_pairs={{0,3},{1,0},{2,1},{3,2},{4,7},{5,4},{6,5},{7,6},{8,11},{9,8},{10,9... | collective-permute-start | bytes 786440 | tf_op jit(solution)/shard_map/ppermute | solution.py:19
  94.1 11.1 %collective-permute-done.16 = bf16[2,256,256]{2,1,0:T(8,128)(2,1)S(1)} collective-permute-done((bf16[2,256,256]{2,1,0:T(8,128)(2,1)S(1)}, bf16[2,256,256]{2,1,0:T(8,128)(2,1)S(1)}, u32[]{:S(2)}, u32[]{:S(2)}) %collective-permute-start.16) | collective-permute-done | bytes 262176 | tf_op jit(solution)/shard_map/ppermute | solution.py:19
  105.2 2.2 %collective-permute-done.18 = bf16[2,256,256]{2,1,0:T(8,128)(2,1)S(1)} collective-permute-done((bf16[2,256,256]{2,1,0:T(8,128)(2,1)S(1)}, bf16[2,256,256]{2,1,0:T(8,128)(2,1)S(1)}, u32[]{:S(2)}, u32[]{:S(2)}) %collective-permute-start.18) | collective-permute-done | bytes 262176 | tf_op jit(solution)/shard_map/ppermute | solution.py:19
  107.5 1.0 convolution_convert_fusion
  109.2 0.8 copy-done.29
  110.5 3.2 %collective-permute-start.7 = (bf16[256,256]{1,0:T(8,128)(2,1)S(1)}, bf16[256,256]{1,0:T(8,128)(2,1)S(1)}, u32[]{:S(2)}, u32[]{:S(2)}) collective-permute-start(bf16[256,256]{1,0:T(8,128)(2,1)S(1)} %fusion.2), channel_id=1, source_target_pairs={{0,3},{1,0},{2,1},{3,2},{4,7},{5,4},{6,5},{7,6},{8,11},{9,8},{10,9... | collective-permute-start | bytes 393224 | tf_op jit(solution)/shard_map/ppermute | solution.py:19
  113.7 1.2 fusion.15
  115.2 1.4 collective-permute-done.3
  116.7 1.2 convolution_add_fusion.1
  117.9 1.2 collective-permute-done.7
  119.1 1.2 fusion.36
  120.2 1.2 collective-permute-done.5
  121.5 1.2 fusion.1
  122.7 0.8 reshape.51
  123.4 9.8 %all-to-all-start.1 = ((bf16[64,4,512]{2,1,0:T(4,128)(2,1)}), bf16[64,4,512]{2,1,0:T(4,128)(2,1)S(1)}, u32[]{:S(2)}, u32[]{:S(2)}) async-start(bf16[64,4,512]{2,1,0:T(4,128)(2,1)} %reshape.51), calls=%async_computation.1 | async-start | bytes 524288 | tf_op jit(solution)/shard_map/all_to_all | solution.py:287
  133.2 2.8 %collective-permute-start.19 = (bf16[64,512]{1,0:T(8,128)(2,1)S(1)}, bf16[64,512]{1,0:T(8,128)(2,1)S(1)}, u32[]{:S(2)}, u32[]{:S(2)}) collective-permute-start(bf16[64,512]{1,0:T(8,128)(2,1)S(1)} %get-tuple-element.25), channel_id=1, source_target_pairs={{0,24},{8,0},{16,8},{24,16},{1,25},{9,1},{17,9},{25,17},{2,26},{10... | collective-permute-start | bytes 196616 | tf_op jit(solution)/shard_map/ppermute | solution.py:19
  136.0 0.9 collective-permute-start.20
  136.9 0.9 collective-permute-start.21
  137.9 2.6 %collective-permute-done.19 = bf16[64,512]{1,0:T(8,128)(2,1)S(1)} collective-permute-done((bf16[64,512]{1,0:T(8,128)(2,1)S(1)}, bf16[64,512]{1,0:T(8,128)(2,1)S(1)}, u32[]{:S(2)}, u32[]{:S(2)}) %collective-permute-start.19) | collective-permute-done | bytes 65568 | tf_op jit(solution)/shard_map/ppermute | solution.py:19
  140.5 2.7 %collective-permute-done.20 = bf16[64,512]{1,0:T(8,128)(2,1)S(1)} collective-permute-done((bf16[64,512]{1,0:T(8,128)(2,1)S(1)}, bf16[64,512]{1,0:T(8,128)(2,1)S(1)}, u32[]{:S(2)}, u32[]{:S(2)}) %collective-permute-start.20) | collective-permute-done | bytes 65568 | tf_op jit(solution)/shard_map/ppermute | solution.py:19
  143.2 1.0 collective-permute-done.21
  144.3 1.1 all-to-all-done.1
  146.1 3.9 %collective-permute-start.24 = (f32[32]{0:T(128)S(1)}, f32[32]{0:T(128)S(1)}, u32[]{:S(2)}, u32[]{:S(2)}) collective-permute-start(f32[32]{0:T(128)S(1)} %get-tuple-element.37), channel_id=1, source_target_pairs={{0,2},{1,3},{2,0},{3,1},{4,6},{5,7},{6,4},{7,5},{8,10},{9,11},{10,... | collective-permute-start | bytes 392 | tf_op jit(solution)/shard_map/ppermute | solution.py:19
  150.0 0.9 collective-permute-done.23
  150.8 0.7 collective-permute-done.24
  151.5 2.0 %collective-permute-done.25 = f32[32]{0:T(128)S(1)} collective-permute-done((f32[32]{0:T(128)S(1)}, f32[32]{0:T(128)S(1)}, u32[]{:S(2)}, u32[]{:S(2)}) %collective-permute-start.25) | collective-permute-done | bytes 160 | tf_op jit(solution)/shard_map/ppermute | solution.py:19
  153.6 0.7 add_convert_fusion
  (105 shorter events, 6.2 us)
Async XLA Ops:
  0.6 108.1 %copy-start = (bf16[1,2048,256]{2,1,0:T(8,128)(2,1)S(1)}, bf16[1,2048,256]{2,1,0:T(8,128)(2,1)}, u32[]{:S(2)}) copy-start(bf16[1,2048,256]{2,1,0:T(8,128)(2,1)} %param.46) | copy-start | bytes 3145732
  1.4 1.6 %copy-start.1 = (f32[32,2,64,128]{3,2,1,0:T(8,128)S(1)}, f32[32,2,64,128]{3,2,1,0:T(8,128)}, u32[]{:S(2)}) copy-start(f32[32,2,64,128]{3,2,1,0:T(8,128)} %scan_state.1) | copy-start | bytes 6291460
  3.0 1.0 copy-start.2
  4.1 1.0 copy-start.3
  5.1 1.0 copy-start.4
  6.1 1.0 copy-start.5
  7.2 1.0 copy-start.6
  8.2 0.9 copy-start.7
  9.1 0.9 copy-start.9
  10.0 0.8 copy-start.10
  10.8 0.7 copy-start.11
  11.5 0.7 copy-start.13
  12.1 0.7 copy-start.14
  12.8 0.7 copy-start.15
  13.5 0.7 copy-start.16
  14.1 12.9 %copy-start.19 = (bf16[1,256,2048]{2,1,0:T(8,128)(2,1)S(1)}, bf16[1,256,2048]{2,1,0:T(8,128)(2,1)}, u32[]{:S(2)}) copy-start(bf16[1,256,2048]{2,1,0:T(8,128)(2,1)} %param.48) | copy-start | bytes 3145732
  14.1 14.4 %copy-start.22 = (bf16[32,512]{1,0:T(8,128)(2,1)S(1)}, bf16[32,512]{1,0:T(8,128)(2,1)}, u32[]{:S(2)}) copy-start(bf16[32,512]{1,0:T(8,128)(2,1)} %param.52) | copy-start | bytes 98308
  14.1 14.4 %copy-start.23 = (bf16[32,512]{1,0:T(8,128)(2,1)S(1)}, bf16[32,512]{1,0:T(8,128)(2,1)}, u32[]{:S(2)}) copy-start(bf16[32,512]{1,0:T(8,128)(2,1)} %param.51) | copy-start | bytes 98308
  14.1 14.4 %copy-start.24 = (bf16[32,512]{1,0:T(8,128)(2,1)S(1)}, bf16[32,512]{1,0:T(8,128)(2,1)}, u32[]{:S(2)}) copy-start(bf16[32,512]{1,0:T(8,128)(2,1)} %param.50) | copy-start | bytes 98308
  14.1 20.8 %copy-start.12 = (s32[32,4]{0,1:T(4,128)S(1)}, s32[32,4]{0,1:T(4,128)}, u32[]{:S(2)}) copy-start(s32[32,4]{0,1:T(4,128)} %param.45) | copy-start | bytes 1540
  14.1 20.9 %copy-start.25 = (bf16[2048]{0:T(1024)(128)(2,1)S(1)}, bf16[2048]{0:T(1024)(128)(2,1)}, u32[]{:S(2)}) copy-start(bf16[2048]{0:T(1024)(128)(2,1)} %param.41) | copy-start | bytes 12292
  14.1 20.9 %copy-start.26 = (bf16[2048]{0:T(1024)(128)(2,1)S(1)}, bf16[2048]{0:T(1024)(128)(2,1)}, u32[]{:S(2)}) copy-start(bf16[2048]{0:T(1024)(128)(2,1)} %param.42) | copy-start | bytes 12292
  14.2 20.9 %copy-start.27 = (bf16[2048]{0:T(1024)(128)(2,1)S(1)}, bf16[2048]{0:T(1024)(128)(2,1)}, u32[]{:S(2)}) copy-start(bf16[2048]{0:T(1024)(128)(2,1)} %param.49) | copy-start | bytes 12292
  14.2 20.9 %copy-start.28 = (bf16[512]{0:T(512)(128)(2,1)S(1)}, bf16[512]{0:T(512)(128)(2,1)}, u32[]{:S(2)}) copy-start(bf16[512]{0:T(512)(128)(2,1)} %param.53) | copy-start | bytes 3076
  21.4 23.5 %copy-start.8 = (bf16[32,2048]{1,0:T(8,128)(2,1)S(1)}, bf16[32,2048]{1,0:T(8,128)(2,1)}, u32[]{:S(2)}) copy-start(bf16[32,2048]{1,0:T(8,128)(2,1)} %resid.3) | copy-start | bytes 393220
  21.4 20.6 %collective-permute-start = (bf16[32,2048]{1,0:T(8,128)(2,1)S(1)}, bf16[32,2048]{1,0:T(8,128)(2,1)S(1)}, u32[]{:S(2)}, u32[]{:S(2)}) collective-permute-start(bf16[32,2048]{1,0:T(8,128)(2,1)S(1)} %get-tuple-element.10.part_0), channel_id=1, source_target_pairs={{0,1},{1,2},{2,3},{3,0},{4,5},{5,6},{6,7},{7,4},{8,9},{9,10},{10,1... | collective-permute-start | bytes 393224 | tf_op jit(solution)/shard_map/ppermute | solution.py:19
  22.9 22.0 %collective-permute-start.1 = (bf16[32,2048]{1,0:T(8,128)(2,1)S(1)}, bf16[32,2048]{1,0:T(8,128)(2,1)S(1)}, u32[]{:S(2)}, u32[]{:S(2)}) collective-permute-start(bf16[32,2048]{1,0:T(8,128)(2,1)S(1)} %get-tuple-element.10.part_0), channel_id=1, source_target_pairs={{0,2},{1,3},{2,0},{3,1},{4,6},{5,7},{6,4},{7,5},{8,10},{9,11},{10,... | collective-permute-start | bytes 393224 | tf_op jit(solution)/shard_map/ppermute | solution.py:19
  25.6 19.2 %collective-permute-start.2 = (bf16[32,2048]{1,0:T(8,128)(2,1)S(1)}, bf16[32,2048]{1,0:T(8,128)(2,1)S(1)}, u32[]{:S(2)}, u32[]{:S(2)}) collective-permute-start(bf16[32,2048]{1,0:T(8,128)(2,1)S(1)} %get-tuple-element.10.part_0), channel_id=1, source_target_pairs={{0,3},{1,0},{2,1},{3,2},{4,7},{5,4},{6,5},{7,6},{8,11},{9,8},{10,9... | collective-permute-start | bytes 393224 | tf_op jit(solution)/shard_map/ppermute | solution.py:19
  28.0 86.9 %collective-permute-start.4 = (bf16[256,512]{1,0:T(8,128)(2,1)}, bf16[256,512]{1,0:T(8,128)(2,1)}, u32[]{:S(2)}, u32[]{:S(2)}) collective-permute-start(bf16[256,512]{1,0:T(8,128)(2,1)} %get-tuple-element.20), channel_id=1, source_target_pairs={{0,1},{1,2},{2,3},{3,0},{4,5},{5,6},{6,7},{7,4},{8,9},{9,10},{10,1... | collective-permute-start | bytes 786440 | tf_op jit(solution)/shard_map/ppermute | solution.py:19
  28.6 16.3 %copy-start.17 = (bf16[1,3,32,512]{3,2,1,0:T(8,128)(2,1)}, bf16[1,3,32,512]{3,2,1,0:T(8,128)(2,1)S(1)}, u32[]{:S(2)}) copy-start(bf16[1,3,32,512]{3,2,1,0:T(8,128)(2,1)S(1)} %maximum_bitcast_fusion.1) | copy-start | bytes 294916
  28.6 10.1 %collective-permute-start.13 = (bf16[1,3,32,512]{3,2,1,0:T(8,128)(2,1)S(1)}, bf16[1,3,32,512]{3,2,1,0:T(8,128)(2,1)S(1)}, u32[]{:S(2)}, u32[]{:S(2)}) collective-permute-start(bf16[1,3,32,512]{3,2,1,0:T(8,128)(2,1)S(1)} %maximum_bitcast_fusion.1), channel_id=1, source_target_pairs={{0,128},{32,160},{64,192},{96,224},{128,0},{160,32},{192,64},{224,... | collective-permute-start | bytes 294920 | tf_op jit(solution)/shard_map/ppermute | solution.py:46
  38.7 8.1 %copy-start.20 = (bf16[1,3,32,512]{3,2,1,0:T(8,128)(2,1)}, bf16[1,3,32,512]{3,2,1,0:T(8,128)(2,1)S(1)}, u32[]{:S(2)}) copy-start(bf16[1,3,32,512]{3,2,1,0:T(8,128)(2,1)S(1)} %collective-permute-done.13) | copy-start | bytes 294916
  38.7 79.2 %collective-permute-start.8 = (bf16[256,512]{1,0:T(8,128)(2,1)}, bf16[256,512]{1,0:T(8,128)(2,1)}, u32[]{:S(2)}, u32[]{:S(2)}) collective-permute-start(bf16[256,512]{1,0:T(8,128)(2,1)} %get-tuple-element.21), channel_id=1, source_target_pairs={{0,3},{1,0},{2,1},{3,2},{4,7},{5,4},{6,5},{7,6},{8,11},{9,8},{10,9... | collective-permute-start | bytes 786440 | tf_op jit(solution)/shard_map/ppermute | solution.py:19
  42.0 20.2 %collective-permute-start.14 = (bf16[2,3,32,512]{3,2,1,0:T(8,128)(2,1)}, bf16[2,3,32,512]{3,2,1,0:T(8,128)(2,1)}, u32[]{:S(2)}, u32[]{:S(2)}) collective-permute-start(bf16[2,3,32,512]{3,2,1,0:T(8,128)(2,1)} %pad_maximum_fusion.2), channel_id=1, source_target_pairs={{0,64},{32,96},{64,0},{96,32},{128,192},{160,224},{192,128},{224,1... | collective-permute-start | bytes 589832 | tf_op jit(solution)/shard_map/ppermute | solution.py:46
  45.5 11.1 %copy-start.31 = (bf16[2048,2]{0,1:T(2,128)(2,1)S(1)}, bf16[2048,2]{0,1:T(2,128)(2,1)}, u32[]{:S(2)}) copy-start(bf16[2048,2]{0,1:T(2,128)(2,1)} %param.43) | copy-start | bytes 24580
  46.8 15.5 %copy-start.18 = (bf16[1,3,32,512]{3,2,1,0:T(8,128)(2,1)S(1)}, bf16[1,3,32,512]{3,2,1,0:T(8,128)(2,1)}, u32[]{:S(2)}) copy-start(bf16[1,3,32,512]{3,2,1,0:T(8,128)(2,1)} %copy-done.17) | copy-start | bytes 294916
  46.8 61.7 %all-to-all-start = ((bf16[64,4,2048]{2,1,0:T(4,128)(2,1)}), bf16[64,4,2048]{2,1,0:T(4,128)(2,1)S(1)}, u32[]{:S(2)}, u32[]{:S(2)}) async-start(bf16[64,4,2048]{2,1,0:T(4,128)(2,1)} %reshape.49), calls=%async_computation | async-start | bytes 2097152 | tf_op jit(solution)/shard_map/all_to_all | solution.py:264
  56.8 1.3 collective-permute-start.9
  58.1 5.8 %collective-permute-start.10 = (bf16[64,512]{1,0:T(8,128)(2,1)S(1)}, bf16[64,512]{1,0:T(8,128)(2,1)S(1)}, u32[]{:S(2)}, u32[]{:S(2)}) collective-permute-start(bf16[64,512]{1,0:T(8,128)(2,1)S(1)} %pad_maximum_fusion.3), channel_id=1, source_target_pairs={{0,8},{8,16},{16,24},{24,0},{1,9},{9,17},{17,25},{25,1},{2,10},{10... | collective-permute-start | bytes 196616 | tf_op jit(solution)/shard_map/ppermute | solution.py:19
  59.6 8.7 %collective-permute-start.11 = (bf16[64,512]{1,0:T(8,128)(2,1)S(1)}, bf16[64,512]{1,0:T(8,128)(2,1)S(1)}, u32[]{:S(2)}, u32[]{:S(2)}) collective-permute-start(bf16[64,512]{1,0:T(8,128)(2,1)S(1)} %pad_maximum_fusion.3), channel_id=1, source_target_pairs={{0,16},{8,24},{16,0},{24,8},{1,17},{9,25},{17,1},{25,9},{2,18},{10... | collective-permute-start | bytes 196616 | tf_op jit(solution)/shard_map/ppermute | solution.py:19
  63.3 25.4 %collective-permute-start.15 = (bf16[4,3,32,512]{3,2,1,0:T(8,128)(2,1)S(1)}, bf16[4,3,32,512]{3,2,1,0:T(8,128)(2,1)S(1)}, u32[]{:S(2)}, u32[]{:S(2)}) collective-permute-start(bf16[4,3,32,512]{3,2,1,0:T(8,128)(2,1)S(1)} %pad_maximum_fusion), channel_id=1, source_target_pairs={{0,32},{32,0},{64,96},{96,64},{128,160},{160,128},{192,224},{224,1... | collective-permute-start | bytes 1179656 | tf_op jit(solution)/shard_map/ppermute | solution.py:46
  64.0 5.3 %collective-permute-start.12 = (bf16[64,512]{1,0:T(8,128)(2,1)S(1)}, bf16[64,512]{1,0:T(8,128)(2,1)S(1)}, u32[]{:S(2)}, u32[]{:S(2)}) collective-permute-start(bf16[64,512]{1,0:T(8,128)(2,1)S(1)} %pad_maximum_fusion.3), channel_id=1, source_target_pairs={{0,24},{8,0},{16,8},{24,16},{1,25},{9,1},{17,9},{25,17},{2,26},{10... | collective-permute-start | bytes 196616 | tf_op jit(solution)/shard_map/ppermute | solution.py:19
  89.8 4.0 %copy-start.30 = (bf16[2048,64]{0,1:T(8,128)(2,1)S(1)}, bf16[2048,64]{0,1:T(8,128)(2,1)}, u32[]{:S(2)}) copy-start(bf16[2048,64]{0,1:T(8,128)(2,1)} %param.44) | copy-start | bytes 786436
  90.4 14.7 %collective-permute-start.16 = (bf16[2,256,256]{2,1,0:T(8,128)(2,1)S(1)}, bf16[2,256,256]{2,1,0:T(8,128)(2,1)S(1)}, u32[]{:S(2)}, u32[]{:S(2)}) collective-permute-start(bf16[2,256,256]{2,1,0:T(8,128)(2,1)S(1)} %pad_maximum_fusion.1), channel_id=1, source_target_pairs={{0,1},{1,2},{2,3},{3,0},{4,5},{5,6},{6,7},{7,4},{8,9},{9,10},{10,1... | collective-permute-start | bytes 786440 | tf_op jit(solution)/shard_map/ppermute | solution.py:19
  90.5 14.6 %collective-permute-start.17 = (bf16[2,256,256]{2,1,0:T(8,128)(2,1)S(1)}, bf16[2,256,256]{2,1,0:T(8,128)(2,1)S(1)}, u32[]{:S(2)}, u32[]{:S(2)}) collective-permute-start(bf16[2,256,256]{2,1,0:T(8,128)(2,1)S(1)} %pad_maximum_fusion.1), channel_id=1, source_target_pairs={{0,2},{1,3},{2,0},{3,1},{4,6},{5,7},{6,4},{7,5},{8,10},{9,11},{10,... | collective-permute-start | bytes 786440 | tf_op jit(solution)/shard_map/ppermute | solution.py:19
  92.0 15.4 %collective-permute-start.18 = (bf16[2,256,256]{2,1,0:T(8,128)(2,1)S(1)}, bf16[2,256,256]{2,1,0:T(8,128)(2,1)S(1)}, u32[]{:S(2)}, u32[]{:S(2)}) collective-permute-start(bf16[2,256,256]{2,1,0:T(8,128)(2,1)S(1)} %pad_maximum_fusion.1), channel_id=1, source_target_pairs={{0,3},{1,0},{2,1},{3,2},{4,7},{5,4},{6,5},{7,6},{8,11},{9,8},{10,9... | collective-permute-start | bytes 786440 | tf_op jit(solution)/shard_map/ppermute | solution.py:19
  105.1 15.1 %collective-permute-start.6 = (bf16[256,512]{1,0:T(8,128)(2,1)}, bf16[256,512]{1,0:T(8,128)(2,1)}, u32[]{:S(2)}, u32[]{:S(2)}) collective-permute-start(bf16[256,512]{1,0:T(8,128)(2,1)} %get-tuple-element.19), channel_id=1, source_target_pairs={{0,2},{1,3},{2,0},{3,1},{4,6},{5,7},{6,4},{7,5},{8,10},{9,11},{10,... | collective-permute-start | bytes 786440 | tf_op jit(solution)/shard_map/ppermute | solution.py:19
  108.7 1.2 copy-start.29
  110.4 6.3 %collective-permute-start.3 = (bf16[256,256]{1,0:T(8,128)(2,1)S(1)}, bf16[256,256]{1,0:T(8,128)(2,1)S(1)}, u32[]{:S(2)}, u32[]{:S(2)}) collective-permute-start(bf16[256,256]{1,0:T(8,128)(2,1)S(1)} %fusion.2), channel_id=1, source_target_pairs={{0,1},{1,2},{2,3},{3,0},{4,5},{5,6},{6,7},{7,4},{8,9},{9,10},{10,1... | collective-permute-start | bytes 393224 | tf_op jit(solution)/shard_map/ppermute | solution.py:19
  110.5 8.6 %collective-permute-start.7 = (bf16[256,256]{1,0:T(8,128)(2,1)S(1)}, bf16[256,256]{1,0:T(8,128)(2,1)S(1)}, u32[]{:S(2)}, u32[]{:S(2)}) collective-permute-start(bf16[256,256]{1,0:T(8,128)(2,1)S(1)} %fusion.2), channel_id=1, source_target_pairs={{0,3},{1,0},{2,1},{3,2},{4,7},{5,4},{6,5},{7,6},{8,11},{9,8},{10,9... | collective-permute-start | bytes 393224 | tf_op jit(solution)/shard_map/ppermute | solution.py:19
  114.9 6.6 %collective-permute-start.5 = (bf16[256,256]{1,0:T(8,128)(2,1)S(1)}, bf16[256,256]{1,0:T(8,128)(2,1)S(1)}, u32[]{:S(2)}, u32[]{:S(2)}) collective-permute-start(bf16[256,256]{1,0:T(8,128)(2,1)S(1)} %fusion.2), channel_id=1, source_target_pairs={{0,2},{1,3},{2,0},{3,1},{4,6},{5,7},{6,4},{7,5},{8,10},{9,11},{10,... | collective-permute-start | bytes 393224 | tf_op jit(solution)/shard_map/ppermute | solution.py:19
  117.8 15.4 %copy-start.21 = (bf16[256,512]{1,0:T(8,128)(2,1)S(1)}, bf16[256,512]{1,0:T(8,128)(2,1)}, u32[]{:S(2)}) copy-start(bf16[256,512]{1,0:T(8,128)(2,1)} %convolution_convert_fusion) | copy-start | bytes 786436
  123.4 22.0 %all-to-all-start.1 = ((bf16[64,4,512]{2,1,0:T(4,128)(2,1)}), bf16[64,4,512]{2,1,0:T(4,128)(2,1)S(1)}, u32[]{:S(2)}, u32[]{:S(2)}) async-start(bf16[64,4,512]{2,1,0:T(4,128)(2,1)} %reshape.51), calls=%async_computation.1 | async-start | bytes 524288 | tf_op jit(solution)/shard_map/all_to_all | solution.py:287
  133.2 7.3 %collective-permute-start.19 = (bf16[64,512]{1,0:T(8,128)(2,1)S(1)}, bf16[64,512]{1,0:T(8,128)(2,1)S(1)}, u32[]{:S(2)}, u32[]{:S(2)}) collective-permute-start(bf16[64,512]{1,0:T(8,128)(2,1)S(1)} %get-tuple-element.25), channel_id=1, source_target_pairs={{0,24},{8,0},{16,8},{24,16},{1,25},{9,1},{17,9},{25,17},{2,26},{10... | collective-permute-start | bytes 196616 | tf_op jit(solution)/shard_map/ppermute | solution.py:19
  136.0 7.2 %collective-permute-start.20 = (bf16[64,512]{1,0:T(8,128)(2,1)S(1)}, bf16[64,512]{1,0:T(8,128)(2,1)S(1)}, u32[]{:S(2)}, u32[]{:S(2)}) collective-permute-start(bf16[64,512]{1,0:T(8,128)(2,1)S(1)} %get-tuple-element.27), channel_id=1, source_target_pairs={{0,16},{8,24},{16,0},{24,8},{1,17},{9,25},{17,1},{25,9},{2,18},{10... | collective-permute-start | bytes 196616 | tf_op jit(solution)/shard_map/ppermute | solution.py:19
  136.9 7.3 %collective-permute-start.21 = (bf16[64,512]{1,0:T(8,128)(2,1)S(1)}, bf16[64,512]{1,0:T(8,128)(2,1)S(1)}, u32[]{:S(2)}, u32[]{:S(2)}) collective-permute-start(bf16[64,512]{1,0:T(8,128)(2,1)S(1)} %get-tuple-element.26), channel_id=1, source_target_pairs={{0,8},{8,16},{16,24},{24,0},{1,9},{9,17},{17,25},{25,1},{2,10},{10... | collective-permute-start | bytes 196616 | tf_op jit(solution)/shard_map/ppermute | solution.py:19
  144.2 1.5 collective-permute-start.22
  146.0 4.9 %collective-permute-start.23 = (f32[32]{0:T(128)S(1)}, f32[32]{0:T(128)S(1)}, u32[]{:S(2)}, u32[]{:S(2)}) collective-permute-start(f32[32]{0:T(128)S(1)} %get-tuple-element.37), channel_id=1, source_target_pairs={{0,1},{1,2},{2,3},{3,0},{4,5},{5,6},{6,7},{7,4},{8,9},{9,10},{10,1... | collective-permute-start | bytes 392 | tf_op jit(solution)/shard_map/ppermute | solution.py:19
  146.1 5.4 %collective-permute-start.24 = (f32[32]{0:T(128)S(1)}, f32[32]{0:T(128)S(1)}, u32[]{:S(2)}, u32[]{:S(2)}) collective-permute-start(f32[32]{0:T(128)S(1)} %get-tuple-element.37), channel_id=1, source_target_pairs={{0,2},{1,3},{2,0},{3,1},{4,6},{5,7},{6,4},{7,5},{8,10},{9,11},{10,... | collective-permute-start | bytes 392 | tf_op jit(solution)/shard_map/ppermute | solution.py:19
  150.0 3.6 %collective-permute-start.25 = (f32[32]{0:T(128)S(1)}, f32[32]{0:T(128)S(1)}, u32[]{:S(2)}, u32[]{:S(2)}) collective-permute-start(f32[32]{0:T(128)S(1)} %get-tuple-element.37), channel_id=1, source_target_pairs={{0,3},{1,0},{2,1},{3,2},{4,7},{5,4},{6,5},{7,6},{8,11},{9,8},{10,9... | collective-permute-start | bytes 392 | tf_op jit(solution)/shard_map/ppermute | solution.py:19
where the time goes:
time: 156 us; the launch traced here: 154 us
  starting transfers between devices  61 us (39%)
  waiting for transfers between devices  54.5 us (35%)
  local copies, waits for them, and re-layouts  17.8 us (11%)
  matrix products  8.1 us (5%)
  Pallas kernels  7.89 us (5%)
  other arithmetic  3.82 us (2%)
    ppermute x21, starting transfers between devices, from_shift(): lax.ppermute(array, axis, [(i, (i + shift) % count) for i in range(count)])  31.3 us
    ppermute x21, waiting for transfers between devices, from_shift(): lax.ppermute(array, axis, [(i, (i + shift) % count) for i in range(count)])  29.5 us
    ppermute x5, waiting for transfers between devices, from_flip(): return lax.ppermute(array, axis, [(i, i ^ bit) for i in range(count)])  24 us
    unnamed x69, local copies, waits for them, and re-layouts  13.6 us
    ppermute x5, starting transfers between devices, from_flip(): return lax.ppermute(array, axis, [(i, i ^ bit) for i in range(count)])  10.1 us
    all_to_all x1, starting transfers between devices, on_device(): lax.all_to_all(outgoing.reshape(expert_count, capacity, width), EP, 0, 0,...  9.83 us
    all_to_all x1, starting transfers between devices, on_device(): lax.all_to_all(served.reshape(expert_count, capacity, quarter), EP, 0, 0,...  9.77 us
    pallas_call x1, Pallas kernels, mixer(): pl.pallas_call(mixer_kernel, name='mixer', in_specs=[smem] * 3 + [vmem] *...  7.2 us
  transfers between devices with their start and end apart: 28, of which 17 were waited for; matrix products, arithmetic and copies ran while one was open for 8% of the time, Pallas kernels for 0%

commit v1 on v0

v1 whole, which is shorter than its diff:
```python
import jax
import jax.numpy as jnp
from jax import lax
from jax.sharding import Mesh
from jax.experimental import pallas as pl
from jax.experimental.pallas import tpu as pltpu
from jax.sharding import PartitionSpec as P


EP = ("ep_0", "ep_1", "ep_2")


norm_eps = 1e-06
FEEDER_VMEM = 16 * 2**20
STATE_CHUNKS = 4


def from_shift(array, axis, shift):
    count = lax.axis_size(axis)
    return lax.ppermute(array, axis, [(i, (i + shift) % count) for i in range(count)])


def from_all(array, axis):
    count = lax.axis_size(axis)
    return [array] + [from_shift(array, axis, s) for s in range(1, count)]


def scaled_rows(values, gain):
    values = values.astype(jnp.float32)
    mean_square = jnp.mean(values * values, axis=-1, keepdims=True)
    return values * lax.rsqrt(mean_square + norm_eps) * gain.astype(jnp.float32)


def dot32(a, b):
    return jnp.dot(a, b, preferred_element_type=jnp.float32)


def sum_of(arrays):
    total = arrays[0].astype(jnp.float32)
    for array in arrays[1:]:
        total = total + array.astype(jnp.float32)
    return total


def from_flip(array, axis, bit):
    count = lax.axis_size(axis)
    return lax.ppermute(array, axis, [(i, i ^ bit) for i in range(count)])


def silu(values):
    return values * (1.0 / (1.0 + jnp.exp(-values)))


MIXER_INPUTS = (
    "resid", "mix_gain", "routes", "proj_x", "proj_b", "proj_c", "proj_step", "conv_taps",
    "conv_state", "step_bias", "decay_rate", "scan_state", "proj_z", "inner_gain", "proj_out",
)


def in_two(values):
    high = values.astype(jnp.bfloat16).astype(jnp.float32)
    return high, values - high


def across_last(a, b):
    return lax.dot_general(a, b, (((1,), (1,)), ((), ())), preferred_element_type=jnp.float32)


def mixer_kernel(place, *refs):
    count = len(MIXER_INPUTS)
    sources, refs = refs[:count], refs[count:]
    (part, state_out, conv_out, in_slot), refs = refs[:4], refs[4:]
    held, refs = refs[:count], refs[count:]
    new_state, new_conv, keep_rows, sems, in_sems, out_sems = refs
    at = dict(zip(MIXER_INPUTS, held))
    scan_state = at["scan_state"]
    copies = {
        name: pltpu.make_async_copy(source, target, sems.at[k])
        for k, (name, source, target) in enumerate(zip(MIXER_INPUTS, sources, held))
        if name != "scan_state"
    }
    state_in = dict(zip(MIXER_INPUTS, sources))["scan_state"]

    def share(i):
        some = state_in.shape[0] // STATE_CHUNKS
        return pl.ds(i * some, some)

    def state_copy(i):
        return pltpu.make_async_copy(
            state_in.at[share(i)], scan_state.at[share(i)], in_sems.at[i]
        )

    def out_copy(i):
        return pltpu.make_async_copy(
            new_state.at[share(i)], state_out.at[share(i)], out_sems.at[i]
        )

    for name in MIXER_INPUTS:
        if name == "scan_state":
            for i in range(STATE_CHUNKS):
                state_copy(i).start()
        else:
            copies[name].start()

    seqs = part.shape[0]
    heads, head_dim, lanes = new_state.shape[1:]
    slots = in_slot.shape[0]
    copies["resid"].wait()
    copies["mix_gain"].wait()
    values = at["resid"][...].astype(jnp.float32)
    mean_square = jnp.mean(values * values, axis=-1, keepdims=True)
    values = values * lax.rsqrt(mean_square + norm_eps)
    gains = at["mix_gain"][...].astype(jnp.float32)
    normed = jnp.concatenate(
        [
            values[:, k * lanes : (k + 1) * lanes] * gains[k : k + 1]
            for k in range(gains.shape[0])
        ],
        axis=1,
    ).astype(jnp.bfloat16)

    copies["routes"].wait()
    slot_ids = lax.broadcasted_iota(jnp.int32, (slots, seqs), 0)
    picked = jnp.zeros((slots, seqs), jnp.bool_)
    for k in range(at["routes"].shape[0]):
        picked = picked | ((slot_ids >> 2) == at["routes"][k : k + 1])
    earlier = lax.broadcasted_iota(jnp.int32, (seqs, seqs), 0) < lax.broadcasted_iota(
        jnp.int32, (seqs, seqs), 1
    )
    rank = dot32(
        jnp.where(picked, 1.0, 0.0).astype(jnp.bfloat16),
        jnp.where(earlier, 1.0, 0.0).astype(jnp.bfloat16),
    )
    in_slot[...] = jnp.where(
        picked & (rank.astype(jnp.int32) == (slot_ids & 3)), 1.0, 0.0
    )

    raws = []
    for name in ("proj_x", "proj_b", "proj_c"):
        copies[name].wait()
        raws.append(dot32(normed, at[name][...]))
    for name in ("proj_step", "conv_taps", "conv_state", "step_bias", "decay_rate"):
        copies[name].wait()
    conv_state, conv_taps = at["conv_state"], at["conv_taps"]
    parts = []
    for k, raw in enumerate(raws):
        fresh = raw.astype(jnp.bfloat16)
        taps = conv_taps[k].astype(jnp.float32)
        total = fresh.astype(jnp.float32) * taps[3:4]
        for pos in range(3):
            total = total + conv_state[k, pos].astype(jnp.float32) * taps[pos : pos + 1]
        new_conv[k, 0] = conv_state[k, 1]
        new_conv[k, 1] = conv_state[k, 2]
        new_conv[k, 2] = fresh
        parts.append(silu(total))
    conv_copy = pltpu.make_async_copy(new_conv, conv_out, out_sems.at[STATE_CHUNKS])
    conv_copy.start()
    xs, bs, cs = parts
    step_all = lax.dot_general(
        normed, at["proj_step"][...], (((1,), (1,)), ((), ())), preferred_element_type=jnp.float32
    )
    head_ids = lax.broadcasted_iota(jnp.int32, step_all.shape, 1)
    lane_ids = lax.broadcasted_iota(jnp.int32, (seqs, lanes), 1)
    steps, keeps = [], []
    for h in range(heads):
        raw = jnp.sum(
            jnp.where(head_ids == place[0] * heads + h, step_all, 0.0), axis=1, keepdims=True
        )
        raw = raw + at["step_bias"][h]
        step = jnp.maximum(raw, 0.0) + jnp.log1p(jnp.exp(-jnp.abs(raw)))
        steps.append(step)
        keeps.append(jnp.exp(-at["decay_rate"][h] * step))
    driven = xs * jnp.where(lane_ids < head_dim, steps[0], steps[1])
    blank = jnp.zeros((lanes - 3 * seqs, lanes), jnp.float32)
    high, low = in_two(driven)
    columns = jnp.concatenate([high, low, high, blank], axis=0).T
    high, low = in_two(bs)
    b_rows = jnp.concatenate([high, high, low, blank], axis=0).astype(jnp.bfloat16)
    blank = jnp.zeros((lanes - seqs, lanes), jnp.float32)
    c_high, c_low = [
        jnp.concatenate([c, blank], axis=0).astype(jnp.bfloat16) for c in in_two(cs)
    ]
    for h in range(heads):
        keep_rows[h] = jnp.broadcast_to(keeps[h], (seqs, lanes))
    wide_ids = lax.broadcasted_iota(jnp.int32, (heads * head_dim, lanes), 1)
    lots = heads * head_dim
    some = seqs // STATE_CHUNKS

    def chunk(i, read):
        first = pl.multiple_of(i * some, some)
        state_copy(i).wait()
        masked = [
            jnp.where((wide_ids & (seqs - 1)) == first + k, columns, 0.0).astype(jnp.bfloat16)
            for k in range(some)
        ]
        outer = dot32(jnp.concatenate(masked, axis=0), b_rows)
        states = []
        for h in range(heads):
            keep = keep_rows[h, pl.ds(first, some)]
            for k in range(some):
                at_row = k * lots + h * head_dim
                state = (
                    keep[k : k + 1] * scan_state[first + k, h]
                    + outer[at_row : at_row + head_dim]
                )
                new_state[first + k, h] = state
                states.append((at_row, state))
        out_copy(i).start()
        states = jnp.concatenate([state for _, state in sorted(states, key=lambda x: x[0])])
        high, low = [x.astype(jnp.bfloat16) for x in in_two(states)]
        found = across_last(high, c_high) + (across_last(low, c_high) + across_last(high, c_low))
        for k in range(some):
            read = read + jnp.where(
                wide_ids == first + k, found[k * lots : (k + 1) * lots], 0.0
            )
        return read

    read = lax.fori_loop(0, STATE_CHUNKS, chunk, jnp.zeros((lots, lanes), jnp.float32))
    read = read.T[:seqs]
    copies["proj_z"].wait()
    copies["inner_gain"].wait()
    gate = silu(dot32(normed, at["proj_z"][...])) * at["inner_gain"][...].astype(jnp.float32)
    gated = (read * gate).astype(jnp.bfloat16)
    copies["proj_out"].wait()
    part[...] = dot32(gated, at["proj_out"][...]).astype(jnp.bfloat16)
    for i in range(STATE_CHUNKS):
        out_copy(i).wait()
    conv_copy.wait()


def mixer(slots, place, **arrays):
    arrays = [arrays[name] for name in MIXER_INPUTS]
    at = dict(zip(MIXER_INPUTS, arrays))
    resid, conv_state, scan_state = at["resid"], at["conv_state"], at["scan_state"]
    vmem = pl.BlockSpec(memory_space=pltpu.VMEM)
    hbm = pl.BlockSpec(memory_space=pltpu.HBM)
    scalars = ("step_bias", "decay_rate")
    held = [
        (pltpu.SMEM if name in scalars else pltpu.VMEM)(array.shape, array.dtype)
        for name, array in at.items()
    ]
    return pl.pallas_call(
        mixer_kernel,
        name="mixer",
        in_specs=[pl.BlockSpec(memory_space=pltpu.SMEM)] + [hbm] * len(arrays),
        out_specs=[vmem, hbm, hbm, vmem],
        scratch_shapes=held
        + [
            pltpu.VMEM(scan_state.shape, scan_state.dtype),
            pltpu.VMEM(conv_state.shape, conv_state.dtype),
            pltpu.VMEM((scan_state.shape[1], resid.shape[0], scan_state.shape[3]), jnp.float32),
            pltpu.SemaphoreType.DMA((len(arrays),)),
            pltpu.SemaphoreType.DMA((STATE_CHUNKS,)),
            pltpu.SemaphoreType.DMA((STATE_CHUNKS + 1,)),
        ],
        out_shape=[
            jax.ShapeDtypeStruct(resid.shape, jnp.bfloat16),
            jax.ShapeDtypeStruct(scan_state.shape, jnp.float32),
            jax.ShapeDtypeStruct(conv_state.shape, jnp.bfloat16),
            jax.ShapeDtypeStruct((slots, resid.shape[0]), jnp.float32),
        ],
    )(place, *arrays)


def feeder_kernel(
    place, part_0, part_1, part_2, part_3, resid, post_gain, ffn_gain, in_slot,
    stream_quarter, feed, feed_quarter, outgoing,
):
    mixed = sum_of([part_0[...], part_1[...], part_2[...], part_3[...]])
    total = resid[...].astype(jnp.float32) + scaled_rows(mixed, post_gain[...])
    total = total.astype(jnp.bfloat16)
    fed = scaled_rows(total, ffn_gain[...]).astype(jnp.bfloat16)
    feed[...] = fed
    quarter = feed_quarter.shape[1]
    for q in range(feed.shape[1] // quarter):

        @pl.when(place[0] == q)
        def _(q=q):
            stream_quarter[...] = total[:, q * quarter : (q + 1) * quarter]
            feed_quarter[...] = fed[:, q * quarter : (q + 1) * quarter]

    outgoing[...] = dot32(in_slot[...], fed).reshape(outgoing.shape).astype(jnp.bfloat16)


def feeder(quarter, place, *arrays):
    vmem = pl.BlockSpec(memory_space=pltpu.VMEM)
    rows = jax.ShapeDtypeStruct(arrays[0].shape, jnp.bfloat16)
    share = jax.ShapeDtypeStruct((arrays[0].shape[0], quarter), jnp.bfloat16)
    return pl.pallas_call(
        feeder_kernel,
        name="feeder",
        in_specs=[pl.BlockSpec(memory_space=pltpu.SMEM)] + [vmem] * len(arrays),
        out_specs=[vmem] * 4,
        compiler_params=pltpu.CompilerParams(vmem_limit_bytes=FEEDER_VMEM),
        out_shape=[
            share,
            rows,
            share,
            jax.ShapeDtypeStruct((arrays[-1].shape[0] // 4, 4, arrays[0].shape[1]), jnp.bfloat16),
        ],
    )(place, *arrays)


def on_device(
    resid,
    mix_gain,
    proj_x,
    proj_z,
    proj_b,
    proj_c,
    proj_step,
    step_bias,
    decay_rate,
    conv_taps,
    conv_state,
    scan_state,
    inner_gain,
    proj_out,
    post_gain,
    ffn_gain,
    group_router,
    expert_router,
    route_experts,
    expert_gate,
    expert_up,
    expert_down,
    dense_switch,
    dense_gate,
    dense_up,
    dense_down,
    out_gain,
):
    tp_index = lax.axis_index("tp")
    tp_count = lax.axis_size("tp")
    seqs, width = resid.shape
    quarter = width // tp_count
    channels = conv_state.shape[3]
    units = dense_gate.shape[0]

    blocks = jnp.stack([dense_gate, dense_up, dense_down])[None]
    blocks = jnp.concatenate([blocks, from_flip(blocks, "ep_0", 4)])
    blocks = jnp.concatenate([blocks, from_flip(blocks, "ep_0", 2)])
    blocks = jnp.concatenate([blocks, from_flip(blocks, "ep_0", 1)])
    unit_rows = jnp.moveaxis(blocks, 0, 1).reshape(3, blocks.shape[0] * units, quarter)
    expert_count = expert_router.shape[1]
    group_size = expert_count // group_router.shape[1]
    pick_count = route_experts.shape[1]
    capacity = 2 * seqs * pick_count // expert_count

    place = jnp.full((1,), tp_index, jnp.int32)
    part, new_state, new_conv, in_slot = mixer(
        expert_count * capacity,
        place,
        resid=resid,
        mix_gain=mix_gain.reshape(-1, channels),
        routes=route_experts.T,
        proj_x=proj_x,
        proj_b=proj_b,
        proj_c=proj_c,
        proj_step=proj_step.T,
        conv_taps=conv_taps,
        conv_state=conv_state.transpose(1, 2, 0, 3),
        step_bias=step_bias,
        decay_rate=decay_rate,
        scan_state=scan_state,
        proj_z=proj_z,
        inner_gain=inner_gain[None],
        proj_out=proj_out,
    )
    new_conv = new_conv.transpose(2, 0, 1, 3)
    mixed_parts = from_all(part, "tp")
    mixed_parts[0] = part.astype(jnp.float32)
    down, part = lax.optimization_barrier((expert_down[0], part))
    down_parts = [
        lax.dynamic_slice_in_dim(down, ((tp_index + s) % tp_count) * quarter, quarter, 1)
        for s in range(tp_count)
    ]
    stream_quarter, feed, feed_quarter, outgoing = feeder(
        quarter, place, *mixed_parts, resid.astype(jnp.float32), post_gain[None],
        ffn_gain[None], in_slot.astype(jnp.bfloat16),
    )

    arrived = lax.all_to_all(
        outgoing, EP, 0, 0, tiled=True
    )
    rows = arrived.reshape(expert_count * capacity, width)

    tokens = jnp.concatenate([feed_quarter, from_flip(feed_quarter, "ep_2", 1)], axis=0)
    tokens = jnp.concatenate(from_all(tokens, "ep_1"), axis=0)
    feed, tokens = lax.optimization_barrier((feed, tokens))
    gate_rows, up_rows, down_rows = unit_rows
    down_parts = [down_parts[0]] + [from_shift(down_parts[s], "tp", s) for s in range(1, tp_count)]
    across = (((1,), (1,)), ((), ()))
    gate_piece = lax.dot_general(tokens, gate_rows, across, preferred_element_type=jnp.float32)
    up_piece = lax.dot_general(tokens, up_rows, across, preferred_element_type=jnp.float32)
    pieces = jnp.stack([gate_piece, up_piece]).astype(jnp.bfloat16)
    sums = from_all(pieces, "tp")

    gate_value = dot32(rows, expert_gate[0])
    up_value = dot32(rows, expert_up[0])
    hidden = (jax.nn.silu(gate_value) * up_value).astype(jnp.bfloat16)
    _, *sums = lax.optimization_barrier((hidden, *sums))
    hidden_parts = from_all(hidden, "tp")
    sums = sum_of(sums)
    dense_hidden = (jax.nn.silu(sums[0]) * sums[1]).astype(jnp.bfloat16)
    dense_part = dot32(dense_hidden, down_rows).astype(jnp.bfloat16)
    lots = dense_part.reshape(lax.axis_size("ep_1"), 2 * seqs, quarter)
    lots = sum_of([lots[0]] + [from_shift(lots[b], "ep_1", -b) for b in range(1, lots.shape[0])])
    dense_part = lots[:seqs] + from_flip(lots[seqs:].astype(jnp.bfloat16), "ep_2", 1)
    dense_out = dense_part

    served = dot32(
        jnp.concatenate(hidden_parts, axis=1), jnp.concatenate(down_parts, axis=0)
    ).astype(jnp.bfloat16)
    returned = lax.all_to_all(
        served.reshape(expert_count, capacity, quarter), EP, 0, 0, tiled=True
    ).reshape(expert_count * capacity, quarter)

    features = (((0,), (1,)), ((), ()))
    group_exp = jnp.exp(
        lax.dot_general(group_router, feed, features, preferred_element_type=jnp.float32)
    )
    group_prob = group_exp / jnp.sum(group_exp, axis=0, keepdims=True)
    routes = route_experts.T
    group_ids = jnp.arange(group_router.shape[1], dtype=jnp.int32)[:, None]
    group_weight = jnp.sum(
        jnp.where(routes[:1] // group_size == group_ids, group_prob, 0.0), axis=0, keepdims=True
    )
    expert_ids = jnp.arange(expert_count, dtype=jnp.int32)[:, None]
    picked = expert_ids == routes[0:1]
    for k in range(1, pick_count):
        picked = picked | (expert_ids == routes[k : k + 1])
    logits = lax.dot_general(expert_router, feed, features, preferred_element_type=jnp.float32)
    pick_exp = jnp.exp(jnp.where(picked, logits, -jnp.inf))
    pick_weight = pick_exp / jnp.sum(pick_exp, axis=0, keepdims=True) * group_weight
    slot_weight = in_slot * jnp.repeat(pick_weight, capacity, axis=0)
    weight_high = slot_weight.astype(jnp.bfloat16)
    weight_low = (slot_weight - weight_high.astype(jnp.float32)).astype(jnp.bfloat16)
    slotwise = (((0,), (0,)), ((), ()))
    routed = lax.dot_general(
        weight_high, returned, slotwise, preferred_element_type=jnp.float32
    ) + lax.dot_general(weight_low, returned, slotwise, preferred_element_type=jnp.float32)

    switch = jax.nn.sigmoid(dot32(feed, dense_switch))
    combined = routed + switch[:, None] * dense_out
    squares = jnp.sum(combined * combined, axis=1)
    total_square = sum_of(from_all(squares, "tp"))
    scale = lax.rsqrt(total_square / width + norm_eps)
    layer_out = (stream_quarter.astype(jnp.float32) + combined * scale[:, None] * out_gain.astype(jnp.float32)).astype(
        jnp.bfloat16
    )
    return (layer_out, new_state, new_conv)


def solution(mesh):
    torus = Mesh(mesh.devices.reshape(8, 4, 2, mesh.shape["tp"]), ("ep_0", "ep_1", "ep_2", "tp"))
    in_specs = (
        P(EP, None),
        P(),
        P(None, "tp"),
        P(None, "tp"),
        P(None, "tp"),
        P(None, "tp"),
        P(),
        P("tp"),
        P("tp"),
        P(None, None, "tp"),
        P(EP, None, None, "tp"),
        P(EP, "tp", None, None),
        P("tp"),
        P("tp", None),
        P(),
        P(),
        P(),
        P(),
        P(EP, None),
        P(EP, None, "tp"),
        P(EP, None, "tp"),
        P(EP, "tp", None),
        P(),
        P(EP, "tp"),
        P(EP, "tp"),
        P(EP, "tp"),
        P("tp"),
    )
    out_specs = (P(EP, "tp"), P(EP, "tp", None, None), P(EP, None, None, "tp"))

    return jax.shard_map(
        on_device, mesh=torus, in_specs=in_specs, out_specs=out_specs, check_vma=False
    )
```

time: 156 us -> 140 us (0.90)
  local copies, waits for them, and re-layouts: 17.8 us -> 3.81 us
  starting transfers between devices: 61 us -> 66.5 us
  matrix products: 8.1 us -> 4.38 us
  waiting for transfers between devices: 54.5 us -> 52.1 us
    unnamed x69 -> x42, local copies, waits for them, and re-layouts: 13.6 us -> 0.8 us
    ppermute x21, waiting for transfers between devices: 29.5 us -> 25.1 us  [from_shift(): lax.ppermute(array, axis, [(i, (i + shift) % count) for i in range(count)])]
    ppermute x21, starting transfers between devices: 31.3 us -> 35.2 us  [from_shift(): lax.ppermute(array, axis, [(i, (i + shift) % count) for i in range(count)])]
    dot_general x8 -> x5, matrix products: 6.66 us -> 2.93 us  [dot32(): return jnp.dot(a, b, preferred_element_type=jnp.float32)]
    ppermute x5, starting transfers between devices: 10.1 us -> 12.4 us  [from_flip(): return lax.ppermute(array, axis, [(i, i ^ bit) for i in range(count)])]
    ppermute x5, waiting for transfers between devices: 24 us -> 25.7 us  [from_flip(): return lax.ppermute(array, axis, [(i, i ^ bit) for i in range(count)])]
  transfers between devices with their start and end apart: 28 -> 28, of which waited for: 17 -> 13; matrix products, arithmetic and copies ran while one was open for 8% -> 5% of each run, Pallas kernels for 0% -> 1%
where the time goes in v1:
time: 140 us; the launch traced here: 139 us
  starting transfers between devices  66.5 us (48%)
  waiting for transfers between devices  52.1 us (37%)
  Pallas kernels  7.79 us (6%)
  matrix products  4.38 us (3%)
  local copies, waits for them, and re-layouts  3.81 us (3%)
  other arithmetic  3.1 us (2%)
    ppermute x21, starting transfers between devices, from_shift(): lax.ppermute(array, axis, [(i, (i + shift) % count) for i in range(count)])  35.2 us
    ppermute x5, waiting for transfers between devices, from_flip(): return lax.ppermute(array, axis, [(i, i ^ bit) for i in range(count)])  25.7 us
    ppermute x21, waiting for transfers between devices, from_shift(): lax.ppermute(array, axis, [(i, (i + shift) % count) for i in range(count)])  25.1 us
    ppermute x5, starting transfers between devices, from_flip(): return lax.ppermute(array, axis, [(i, i ^ bit) for i in range(count)])  12.4 us
    all_to_all x1, starting transfers between devices, on_device(): lax.all_to_all(served.reshape(expert_count, capacity, quarter), EP, 0, 0,...  9.82 us
    all_to_all x1, starting transfers between devices, on_device(): arrived = lax.all_to_all(outgoing, EP, 0, 0, tiled=True)  9.02 us
    pallas_call x1, Pallas kernels, mixer(): pl.pallas_call(mixer_kernel, name='mixer', in_specs=[pl.BlockSpec(memory_...  6.01 us
    dot_general x5, matrix products, dot32(): return jnp.dot(a, b, preferred_element_type=jnp.float32)  2.93 us
  transfers between devices with their start and end apart: 28, of which 13 were waited for; matrix products, arithmetic and copies ran while one was open for 5% of the time, Pallas kernels for 1%

profile of v1, /device:TPU:32, one launch (start us, length us, event | category | flops | bytes accessed | tf_op | source)
XLA Modules:
  0.0 138.8 jit_solution(17414490071657267112)
XLA Ops:
  0.6 0.0 copy-start
  0.7 6.0 %mixer.1 = (bf16[32,2048]{1,0:T(8,128)(2,1)}, f32[32,2,64,128]{3,2,1,0:T(8,128)}, bf16[3,3,32,128]{3,2,1,0:T(8,128)(2,1)}, f32[256,32]{1,0:T(8,128)}) custom-call(s32[1]{0:T(128)} %bitcast.place, bf16[32,2048]{1,0:T(8,128)(2,1)} %refs_0_.1, bf16[16,128]{1,0:T(8,128)(2,1)} %bitcast.88, s32[4,32]{1,0:T(4,128)} %bitcast.86, bf16[2048,128]{1,0:T(8,128)(2,1)} %refs_3_.1, ...), custom_call_target="tpu_custom_call" | custom-call | tf_op jit(solution)/shard_map/mixer/pallas_call | solution.py:242
  6.8 2.8 %collective-permute-start.2 = (bf16[32,2048]{1,0:T(8,128)(2,1)}, bf16[32,2048]{1,0:T(8,128)(2,1)S(1)}, u32[]{:S(2)}, u32[]{:S(2)}) collective-permute-start(bf16[32,2048]{1,0:T(8,128)(2,1)} %get-tuple-element.18), channel_id=1, source_target_pairs={{0,3},{1,0},{2,1},{3,2},{4,7},{5,4},{6,5},{7,6},{8,11},{9,8},{10,9... | collective-permute-start | bytes 393224 | tf_op jit(solution)/shard_map/ppermute | solution.py:20
  9.6 0.8 collective-permute-start.1
  10.4 0.9 collective-permute-start
  11.3 6.4 %collective-permute-start.13 = (bf16[1,3,32,512]{3,2,1,0:T(8,128)(2,1)S(1)}, bf16[1,3,32,512]{3,2,1,0:T(8,128)(2,1)S(1)}, u32[]{:S(2)}, u32[]{:S(2)}) collective-permute-start(bf16[1,3,32,512]{3,2,1,0:T(8,128)(2,1)S(1)} %maximum_bitcast_fusion.1), channel_id=1, source_target_pairs={{0,128},{32,160},{64,192},{96,224},{128,0},{160,32},{192,64},{224,... | collective-permute-start | bytes 294920 | tf_op jit(solution)/shard_map/ppermute | solution.py:47
  17.7 1.0 constant_dynamic-slice_fusion.3
  18.7 2.4 %collective-permute-start.12 = (bf16[256,512]{1,0:T(8,128)(2,1)}, bf16[256,512]{1,0:T(8,128)(2,1)}, u32[]{:S(2)}, u32[]{:S(2)}) collective-permute-start(bf16[256,512]{1,0:T(8,128)(2,1)} %get-tuple-element.34), channel_id=1, source_target_pairs={{0,3},{1,0},{2,1},{3,2},{4,7},{5,4},{6,5},{7,6},{8,11},{9,8},{10,9... | collective-permute-start | bytes 786440 | tf_op jit(solution)/shard_map/ppermute | solution.py:20
  21.3 1.6 %collective-permute-start.11 = (bf16[256,512]{1,0:T(8,128)(2,1)}, bf16[256,512]{1,0:T(8,128)(2,1)}, u32[]{:S(2)}, u32[]{:S(2)}) collective-permute-start(bf16[256,512]{1,0:T(8,128)(2,1)} %get-tuple-element.35), channel_id=1, source_target_pairs={{0,2},{1,3},{2,0},{3,1},{4,6},{5,7},{6,4},{7,5},{8,10},{9,11},{10,... | collective-permute-start | bytes 786440 | tf_op jit(solution)/shard_map/ppermute | solution.py:20
  22.9 1.8 %feeder.1 = (bf16[32,512]{1,0:T(8,128)(2,1)S(1)}, bf16[32,2048]{1,0:T(8,128)(2,1)S(1)}, bf16[32,512]{1,0:T(8,128)(2,1)S(1)}, bf16[64,4,2048]{2,1,0:T(4,128)(2,1)}) custom-call(s32[1]{0:T(128)} %bitcast.place, f32[32,2048]{1,0:T(8,128)S(1)} %convert_element_type.71.part_0, bf16[32,2048]{1,0:T(8,128)(2,1)S(1)} %collective-permute-done.part_1, ...), custom_call_target="tpu_custom_call" | custom-call | tf_op jit(solution)/shard_map/feeder/pallas_call | solution.py:289
  24.7 9.0 %all-to-all-start = ((bf16[64,4,2048]{2,1,0:T(4,128)(2,1)}), bf16[64,4,2048]{2,1,0:T(4,128)(2,1)S(1)}, u32[]{:S(2)}, u32[]{:S(2)}) async-start(bf16[64,4,2048]{2,1,0:T(4,128)(2,1)} %get-tuple-element.24), calls=%async_computation | async-start | bytes 2097152 | tf_op jit(solution)/shard_map/all_to_all | solution.py:383
  33.8 1.5 %collective-permute-start.4 = (bf16[64,512]{1,0:T(8,128)(2,1)S(1)}, bf16[64,512]{1,0:T(8,128)(2,1)S(1)}, u32[]{:S(2)}, u32[]{:S(2)}) collective-permute-start(bf16[64,512]{1,0:T(8,128)(2,1)S(1)} %get-tuple-element.43), channel_id=1, source_target_pairs={{0,8},{8,16},{16,24},{24,0},{1,9},{9,17},{17,25},{25,1},{2,10},{10... | collective-permute-start | bytes 196616 | tf_op jit(solution)/shard_map/ppermute | solution.py:20
  35.3 2.5 %collective-permute-start.14 = (bf16[2,3,32,512]{3,2,1,0:T(8,128)(2,1)S(1)}, bf16[2,3,32,512]{3,2,1,0:T(8,128)(2,1)S(1)}, u32[]{:S(2)}, u32[]{:S(2)}) collective-permute-start(bf16[2,3,32,512]{3,2,1,0:T(8,128)(2,1)S(1)} %pad_maximum_fusion.2), channel_id=1, source_target_pairs={{0,64},{32,96},{64,0},{96,32},{128,192},{160,224},{192,128},{224,1... | collective-permute-start | bytes 589832 | tf_op jit(solution)/shard_map/ppermute | solution.py:47
  37.8 1.8 %collective-permute-start.6 = (bf16[64,512]{1,0:T(8,128)(2,1)S(1)}, bf16[64,512]{1,0:T(8,128)(2,1)S(1)}, u32[]{:S(2)}, u32[]{:S(2)}) collective-permute-start(bf16[64,512]{1,0:T(8,128)(2,1)S(1)} %get-tuple-element.43), channel_id=1, source_target_pairs={{0,24},{8,0},{16,8},{24,16},{1,25},{9,1},{17,9},{25,17},{2,26},{10... | collective-permute-start | bytes 196616 | tf_op jit(solution)/shard_map/ppermute | solution.py:20
  39.6 0.7 collective-permute-done.4
  40.3 2.8 %collective-permute-start.5 = (bf16[64,512]{1,0:T(8,128)(2,1)S(1)}, bf16[64,512]{1,0:T(8,128)(2,1)S(1)}, u32[]{:S(2)}, u32[]{:S(2)}) collective-permute-start(bf16[64,512]{1,0:T(8,128)(2,1)S(1)} %get-tuple-element.43), channel_id=1, source_target_pairs={{0,16},{8,24},{16,0},{24,8},{1,17},{9,25},{17,1},{25,9},{2,18},{10... | collective-permute-start | bytes 196616 | tf_op jit(solution)/shard_map/ppermute | solution.py:20
  43.1 4.3 %collective-permute-done.5 = bf16[64,512]{1,0:T(8,128)(2,1)S(1)} collective-permute-done((bf16[64,512]{1,0:T(8,128)(2,1)S(1)}, bf16[64,512]{1,0:T(8,128)(2,1)S(1)}, u32[]{:S(2)}, u32[]{:S(2)}) %collective-permute-start.5) | collective-permute-done | bytes 65568 | tf_op jit(solution)/shard_map/ppermute | solution.py:20
  47.4 0.2 fusion.42
  47.6 17.4 %collective-permute-done.14 = bf16[2,3,32,512]{3,2,1,0:T(8,128)(2,1)S(1)} collective-permute-done((bf16[2,3,32,512]{3,2,1,0:T(8,128)(2,1)S(1)}, bf16[2,3,32,512]{3,2,1,0:T(8,128)(2,1)S(1)}, u32[]{:S(2)}, u32[]{:S(2)}) %collective-permute-start.14) | collective-permute-done | bytes 196640 | tf_op jit(solution)/shard_map/ppermute | solution.py:47
  65.0 3.5 %collective-permute-start.15 = (bf16[4,3,32,512]{3,2,1,0:T(8,128)(2,1)S(1)}, bf16[4,3,32,512]{3,2,1,0:T(8,128)(2,1)S(1)}, u32[]{:S(2)}, u32[]{:S(2)}) collective-permute-start(bf16[4,3,32,512]{3,2,1,0:T(8,128)(2,1)S(1)} %pad_maximum_fusion), channel_id=1, source_target_pairs={{0,32},{32,0},{64,96},{96,64},{128,160},{160,128},{192,224},{224,1... | collective-permute-start | bytes 1179656 | tf_op jit(solution)/shard_map/ppermute | solution.py:47
  68.5 0.1 fusion.8
  68.7 0.3 fusion.43
  69.0 8.3 %collective-permute-done.15 = bf16[4,3,32,512]{3,2,1,0:T(8,128)(2,1)S(1)} collective-permute-done((bf16[4,3,32,512]{3,2,1,0:T(8,128)(2,1)S(1)}, bf16[4,3,32,512]{3,2,1,0:T(8,128)(2,1)S(1)}, u32[]{:S(2)}, u32[]{:S(2)}) %collective-permute-start.15) | collective-permute-done | bytes 393248 | tf_op jit(solution)/shard_map/ppermute | solution.py:47
  77.3 0.1 maximum_bitcast_fusion
  77.4 0.8 fusion.40
  78.2 0.3 fusion.2
  78.4 0.3 fusion.1
  78.7 0.7 pad_maximum_fusion.1
  79.4 0.6 collective-permute-start.18
  80.0 2.3 %collective-permute-start.17 = (bf16[2,256,256]{2,1,0:T(8,128)(2,1)}, bf16[2,256,256]{2,1,0:T(8,128)(2,1)}, u32[]{:S(2)}, u32[]{:S(2)}) collective-permute-start(bf16[2,256,256]{2,1,0:T(8,128)(2,1)} %pad_maximum_fusion.1), channel_id=1, source_target_pairs={{0,2},{1,3},{2,0},{3,1},{4,6},{5,7},{6,4},{7,5},{8,10},{9,11},{10,... | collective-permute-start | bytes 786440 | tf_op jit(solution)/shard_map/ppermute | solution.py:20
  82.3 0.3 reshape.46
  82.6 0.5 fusion.17
  83.1 0.7 copy-done.16
  83.8 0.5 fusion
  84.4 4.5 %collective-permute-done.18 = bf16[2,256,256]{2,1,0:T(8,128)(2,1)} collective-permute-done((bf16[2,256,256]{2,1,0:T(8,128)(2,1)}, bf16[2,256,256]{2,1,0:T(8,128)(2,1)}, u32[]{:S(2)}, u32[]{:S(2)}) %collective-permute-start.18) | collective-permute-done | bytes 262176 | tf_op jit(solution)/shard_map/ppermute | solution.py:20
  88.9 4.4 %collective-permute-start.10 = (bf16[256,512]{1,0:T(8,128)(2,1)S(1)}, bf16[256,512]{1,0:T(8,128)(2,1)S(1)}, u32[]{:S(2)}, u32[]{:S(2)}) collective-permute-start(bf16[256,512]{1,0:T(8,128)(2,1)S(1)} %copy-done.5), channel_id=1, source_target_pairs={{0,1},{1,2},{2,3},{3,0},{4,5},{5,6},{6,7},{7,4},{8,9},{9,10},{10,1... | collective-permute-start | bytes 786440 | tf_op jit(solution)/shard_map/ppermute | solution.py:20
  93.3 2.8 %collective-permute-start.9 = (bf16[256,256]{0,1:T(8,128)(2,1)S(1)}, bf16[256,256]{0,1:T(8,128)(2,1)S(1)}, u32[]{:S(2)}, u32[]{:S(2)}) collective-permute-start(bf16[256,256]{0,1:T(8,128)(2,1)S(1)} %fusion), channel_id=1, source_target_pairs={{0,3},{1,0},{2,1},{3,2},{4,7},{5,4},{6,5},{7,6},{8,11},{9,8},{10,9... | collective-permute-start | bytes 393224 | tf_op jit(solution)/shard_map/ppermute | solution.py:20
  96.1 0.6 collective-permute-start.8
  96.7 1.3 convert_add_fusion
  98.0 1.4 %collective-permute-start.7 = (bf16[256,256]{0,1:T(8,128)(2,1)S(1)}, bf16[256,256]{0,1:T(8,128)(2,1)S(1)}, u32[]{:S(2)}, u32[]{:S(2)}) collective-permute-start(bf16[256,256]{0,1:T(8,128)(2,1)S(1)} %fusion), channel_id=1, source_target_pairs={{0,1},{1,2},{2,3},{3,0},{4,5},{5,6},{6,7},{7,4},{8,9},{9,10},{10,1... | collective-permute-start | bytes 393224 | tf_op jit(solution)/shard_map/ppermute | solution.py:20
  99.4 0.2 convolution_convert_fusion
  99.7 2.1 %collective-permute-done.10 = bf16[256,512]{1,0:T(8,128)(2,1)S(1)} collective-permute-done((bf16[256,512]{1,0:T(8,128)(2,1)S(1)}, bf16[256,512]{1,0:T(8,128)(2,1)S(1)}, u32[]{:S(2)}, u32[]{:S(2)}) %collective-permute-start.10) | collective-permute-done | bytes 262176 | tf_op jit(solution)/shard_map/ppermute | solution.py:20
  101.8 2.4 %collective-permute-done.8 = bf16[256,256]{0,1:T(8,128)(2,1)S(1)} collective-permute-done((bf16[256,256]{0,1:T(8,128)(2,1)S(1)}, bf16[256,256]{0,1:T(8,128)(2,1)S(1)}, u32[]{:S(2)}, u32[]{:S(2)}) %collective-permute-start.8) | collective-permute-done | bytes 131104 | tf_op jit(solution)/shard_map/ppermute | solution.py:20
  104.1 1.3 collective-permute-done.7
  105.4 1.5 %convolution_convert_fusion.1 = bf16[256,512]{1,0:T(8,128)(2,1)S(1)} fusion(bf16[256,512]{1,0:T(8,128)(2,1)} %collective-permute-done.12, bf16[256,512]{1,0:T(8,128)(2,1)} %collective-permute-done.11, bf16[256,512]{1,0:T(8,128)(2,1)S(1)} %collective-permute-done.10, bf16[256,512]{1,0:T(8,128)(2,1)S(1)} %copy-done.4, ...), kind=kOutput, calls=%fused_computation.1 | convolution fusion | flops 274857984 | bytes 1835008 | tf_op jit(solution)/shard_map/dot_general | solution.py:35
  106.9 0.8 reshape.47
  107.7 9.8 %all-to-all-start.1 = ((bf16[64,4,512]{2,1,0:T(4,128)(2,1)}), bf16[64,4,512]{2,1,0:T(4,128)(2,1)S(1)}, u32[]{:S(2)}, u32[]{:S(2)}) async-start(bf16[64,4,512]{2,1,0:T(4,128)(2,1)} %reshape.47), calls=%async_computation.1 | async-start | bytes 524288 | tf_op jit(solution)/shard_map/all_to_all | solution.py:415
  117.5 2.8 %collective-permute-start.19 = (bf16[64,512]{1,0:T(8,128)(2,1)S(1)}, bf16[64,512]{1,0:T(8,128)(2,1)S(1)}, u32[]{:S(2)}, u32[]{:S(2)}) collective-permute-start(bf16[64,512]{1,0:T(8,128)(2,1)S(1)} %get-tuple-element.40), channel_id=1, source_target_pairs={{0,24},{8,0},{16,8},{24,16},{1,25},{9,1},{17,9},{25,17},{2,26},{10... | collective-permute-start | bytes 196616 | tf_op jit(solution)/shard_map/ppermute | solution.py:20
  120.3 2.3 %collective-permute-start.20 = (bf16[64,512]{1,0:T(8,128)(2,1)S(1)}, bf16[64,512]{1,0:T(8,128)(2,1)S(1)}, u32[]{:S(2)}, u32[]{:S(2)}) collective-permute-start(bf16[64,512]{1,0:T(8,128)(2,1)S(1)} %get-tuple-element.42), channel_id=1, source_target_pairs={{0,16},{8,24},{16,0},{24,8},{1,17},{9,25},{17,1},{25,9},{2,18},{10... | collective-permute-start | bytes 196616 | tf_op jit(solution)/shard_map/ppermute | solution.py:20
  122.6 0.1 divide_multiply_fusion
  122.7 0.1 copy.30
  122.8 5.5 %collective-permute-done.21 = bf16[64,512]{1,0:T(8,128)(2,1)S(1)} collective-permute-done((bf16[64,512]{1,0:T(8,128)(2,1)S(1)}, bf16[64,512]{1,0:T(8,128)(2,1)S(1)}, u32[]{:S(2)}, u32[]{:S(2)}) %collective-permute-start.21) | collective-permute-done | bytes 65568 | tf_op jit(solution)/shard_map/ppermute | solution.py:20
  128.4 0.1 collective-permute-start.22
  128.5 1.2 all-to-all-done.1
  129.7 0.1 reshape.48
  129.8 0.2 fusion.32
  130.0 0.3 multiply_reduce_fusion
  130.3 1.2 collective-permute-start.25
  131.5 1.8 %collective-permute-start.24 = (f32[32]{0:T(128)S(1)}, f32[32]{0:T(128)S(1)}, u32[]{:S(2)}, u32[]{:S(2)}) collective-permute-start(f32[32]{0:T(128)S(1)} %get-tuple-element.56), channel_id=1, source_target_pairs={{0,2},{1,3},{2,0},{3,1},{4,6},{5,7},{6,4},{7,5},{8,10},{9,11},{10,... | collective-permute-start | bytes 392 | tf_op jit(solution)/shard_map/ppermute | solution.py:20
  133.3 0.5 collective-permute-start.23
  133.8 0.1 collective-permute-done.25
  133.9 2.6 %collective-permute-done.24 = f32[32]{0:T(128)S(1)} collective-permute-done((f32[32]{0:T(128)S(1)}, f32[32]{0:T(128)S(1)}, u32[]{:S(2)}, u32[]{:S(2)}) %collective-permute-start.24) | collective-permute-done | bytes 160 | tf_op jit(solution)/shard_map/ppermute | solution.py:20
  136.6 1.5 %collective-permute-done.23 = f32[32]{0:T(128)S(1)} collective-permute-done((f32[32]{0:T(128)S(1)}, f32[32]{0:T(128)S(1)}, u32[]{:S(2)}, u32[]{:S(2)}) %collective-permute-start.23) | collective-permute-done | bytes 160 | tf_op jit(solution)/shard_map/ppermute | solution.py:20
  138.1 0.7 add_convert_fusion
  (76 shorter events, 0.5 us)
Async XLA Ops:
  0.6 81.9 %copy-start = (bf16[1,2048,256]{2,1,0:T(8,128)(2,1)S(1)}, bf16[1,2048,256]{2,1,0:T(8,128)(2,1)}, u32[]{:S(2)}) copy-start(bf16[1,2048,256]{2,1,0:T(8,128)(2,1)} %param.46) | copy-start | bytes 3145732
  0.7 10.7 %copy-start.8 = (bf16[32,512]{1,0:T(8,128)(2,1)S(1)}, bf16[32,512]{1,0:T(8,128)(2,1)}, u32[]{:S(2)}) copy-start(bf16[32,512]{1,0:T(8,128)(2,1)} %param.52) | copy-start | bytes 98308
  0.7 10.7 %copy-start.9 = (bf16[32,512]{1,0:T(8,128)(2,1)S(1)}, bf16[32,512]{1,0:T(8,128)(2,1)}, u32[]{:S(2)}) copy-start(bf16[32,512]{1,0:T(8,128)(2,1)} %param.51) | copy-start | bytes 98308
  0.7 10.7 %copy-start.10 = (bf16[32,512]{1,0:T(8,128)(2,1)S(1)}, bf16[32,512]{1,0:T(8,128)(2,1)}, u32[]{:S(2)}) copy-start(bf16[32,512]{1,0:T(8,128)(2,1)} %param.50) | copy-start | bytes 98308
  0.7 17.0 %copy-start.2 = (bf16[1,256,2048]{2,1,0:T(8,128)(2,1)S(1)}, bf16[1,256,2048]{2,1,0:T(8,128)(2,1)}, u32[]{:S(2)}) copy-start(bf16[1,256,2048]{2,1,0:T(8,128)(2,1)} %param.48) | copy-start | bytes 3145732
  6.7 14.4 %copy-start.3 = (bf16[32,2048]{1,0:T(8,128)(2,1)S(1)}, bf16[32,2048]{1,0:T(8,128)(2,1)}, u32[]{:S(2)}) copy-start(bf16[32,2048]{1,0:T(8,128)(2,1)} %refs_0_.1) | copy-start | bytes 393220
  6.7 14.4 %copy-start.7 = (bf16[32,2048]{1,0:T(8,128)(2,1)S(1)}, bf16[32,2048]{1,0:T(8,128)(2,1)}, u32[]{:S(2)}) copy-start(bf16[32,2048]{1,0:T(8,128)(2,1)} %get-tuple-element.18) | copy-start | bytes 393220
  6.7 14.4 %copy-start.15 = (bf16[512]{0:T(512)(128)(2,1)S(1)}, bf16[512]{0:T(512)(128)(2,1)}, u32[]{:S(2)}) copy-start(bf16[512]{0:T(512)(128)(2,1)} %param.53) | copy-start | bytes 3076
  6.8 14.4 %copy-start.12 = (bf16[2048]{0:T(1024)(128)(2,1)S(1)}, bf16[2048]{0:T(1024)(128)(2,1)}, u32[]{:S(2)}) copy-start(bf16[2048]{0:T(1024)(128)(2,1)} %param.41) | copy-start | bytes 12292
  6.8 14.4 %copy-start.13 = (bf16[2048]{0:T(1024)(128)(2,1)S(1)}, bf16[2048]{0:T(1024)(128)(2,1)}, u32[]{:S(2)}) copy-start(bf16[2048]{0:T(1024)(128)(2,1)} %param.42) | copy-start | bytes 12292
  6.8 14.4 %copy-start.14 = (bf16[2048]{0:T(1024)(128)(2,1)S(1)}, bf16[2048]{0:T(1024)(128)(2,1)}, u32[]{:S(2)}) copy-start(bf16[2048]{0:T(1024)(128)(2,1)} %param.49) | copy-start | bytes 12292
  6.8 14.4 %copy-start.1 = (f32[256,32]{1,0:T(8,128)S(1)}, f32[256,32]{1,0:T(8,128)}, u32[]{:S(2)}) copy-start(f32[256,32]{1,0:T(8,128)} %get-tuple-element.19) | copy-start | bytes 98308
  6.8 14.5 %copy-start.11 = (s32[32,4]{0,1:T(4,128)S(1)}, s32[32,4]{0,1:T(4,128)}, u32[]{:S(2)}) copy-start(s32[32,4]{0,1:T(4,128)} %param.45) | copy-start | bytes 1540
  6.8 14.5 %collective-permute-start.2 = (bf16[32,2048]{1,0:T(8,128)(2,1)}, bf16[32,2048]{1,0:T(8,128)(2,1)S(1)}, u32[]{:S(2)}, u32[]{:S(2)}) collective-permute-start(bf16[32,2048]{1,0:T(8,128)(2,1)} %get-tuple-element.18), channel_id=1, source_target_pairs={{0,3},{1,0},{2,1},{3,2},{4,7},{5,4},{6,5},{7,6},{8,11},{9,8},{10,9... | collective-permute-start | bytes 393224 | tf_op jit(solution)/shard_map/ppermute | solution.py:20
  9.6 13.3 %collective-permute-start.1 = (bf16[32,2048]{1,0:T(8,128)(2,1)}, bf16[32,2048]{1,0:T(8,128)(2,1)S(1)}, u32[]{:S(2)}, u32[]{:S(2)}) collective-permute-start(bf16[32,2048]{1,0:T(8,128)(2,1)} %get-tuple-element.18), channel_id=1, source_target_pairs={{0,2},{1,3},{2,0},{3,1},{4,6},{5,7},{6,4},{7,5},{8,10},{9,11},{10,... | collective-permute-start | bytes 393224 | tf_op jit(solution)/shard_map/ppermute | solution.py:20
  10.4 12.5 %collective-permute-start = (bf16[32,2048]{1,0:T(8,128)(2,1)}, bf16[32,2048]{1,0:T(8,128)(2,1)S(1)}, u32[]{:S(2)}, u32[]{:S(2)}) collective-permute-start(bf16[32,2048]{1,0:T(8,128)(2,1)} %get-tuple-element.18), channel_id=1, source_target_pairs={{0,1},{1,2},{2,3},{3,0},{4,5},{5,6},{6,7},{7,4},{8,9},{9,10},{10,1... | collective-permute-start | bytes 393224 | tf_op jit(solution)/shard_map/ppermute | solution.py:20
  11.3 23.9 %collective-permute-start.13 = (bf16[1,3,32,512]{3,2,1,0:T(8,128)(2,1)S(1)}, bf16[1,3,32,512]{3,2,1,0:T(8,128)(2,1)S(1)}, u32[]{:S(2)}, u32[]{:S(2)}) collective-permute-start(bf16[1,3,32,512]{3,2,1,0:T(8,128)(2,1)S(1)} %maximum_bitcast_fusion.1), channel_id=1, source_target_pairs={{0,128},{32,160},{64,192},{96,224},{128,0},{160,32},{192,64},{224,... | collective-permute-start | bytes 294920 | tf_op jit(solution)/shard_map/ppermute | solution.py:47
  18.7 79.3 %collective-permute-start.12 = (bf16[256,512]{1,0:T(8,128)(2,1)}, bf16[256,512]{1,0:T(8,128)(2,1)}, u32[]{:S(2)}, u32[]{:S(2)}) collective-permute-start(bf16[256,512]{1,0:T(8,128)(2,1)} %get-tuple-element.34), channel_id=1, source_target_pairs={{0,3},{1,0},{2,1},{3,2},{4,7},{5,4},{6,5},{7,6},{8,11},{9,8},{10,9... | collective-permute-start | bytes 786440 | tf_op jit(solution)/shard_map/ppermute | solution.py:20
  21.3 26.1 %copy-start.18 = (bf16[2048,2]{0,1:T(2,128)(2,1)S(1)}, bf16[2048,2]{0,1:T(2,128)(2,1)}, u32[]{:S(2)}) copy-start(bf16[2048,2]{0,1:T(2,128)(2,1)} %param.43) | copy-start | bytes 24580
  21.3 78.4 %collective-permute-start.11 = (bf16[256,512]{1,0:T(8,128)(2,1)}, bf16[256,512]{1,0:T(8,128)(2,1)}, u32[]{:S(2)}, u32[]{:S(2)}) collective-permute-start(bf16[256,512]{1,0:T(8,128)(2,1)} %get-tuple-element.35), channel_id=1, source_target_pairs={{0,2},{1,3},{2,0},{3,1},{4,6},{5,7},{6,4},{7,5},{8,10},{9,11},{10,... | collective-permute-start | bytes 786440 | tf_op jit(solution)/shard_map/ppermute | solution.py:20
  24.7 44.0 %copy-start.17 = (bf16[2048,64]{0,1:T(8,128)(2,1)S(1)}, bf16[2048,64]{0,1:T(8,128)(2,1)}, u32[]{:S(2)}) copy-start(bf16[2048,64]{0,1:T(8,128)(2,1)} %param.44) | copy-start | bytes 786436
  24.7 9.0 %collective-permute-start.3 = (bf16[32,512]{1,0:T(8,128)(2,1)S(1)}, bf16[32,512]{1,0:T(8,128)(2,1)S(1)}, u32[]{:S(2)}, u32[]{:S(2)}) collective-permute-start(bf16[32,512]{1,0:T(8,128)(2,1)S(1)} %get-tuple-element.22), channel_id=1, source_target_pairs={{0,4},{4,0},{1,5},{5,1},{2,6},{6,2},{3,7},{7,3},{8,12},{12,8},{9,1... | collective-permute-start | bytes 98312 | tf_op jit(solution)/shard_map/ppermute | solution.py:47
  24.7 57.6 %all-to-all-start = ((bf16[64,4,2048]{2,1,0:T(4,128)(2,1)}), bf16[64,4,2048]{2,1,0:T(4,128)(2,1)S(1)}, u32[]{:S(2)}, u32[]{:S(2)}) async-start(bf16[64,4,2048]{2,1,0:T(4,128)(2,1)} %get-tuple-element.24), calls=%async_computation | async-start | bytes 2097152 | tf_op jit(solution)/shard_map/all_to_all | solution.py:383
  33.8 6.6 %collective-permute-start.4 = (bf16[64,512]{1,0:T(8,128)(2,1)S(1)}, bf16[64,512]{1,0:T(8,128)(2,1)S(1)}, u32[]{:S(2)}, u32[]{:S(2)}) collective-permute-start(bf16[64,512]{1,0:T(8,128)(2,1)S(1)} %get-tuple-element.43), channel_id=1, source_target_pairs={{0,8},{8,16},{16,24},{24,0},{1,9},{9,17},{17,25},{25,1},{2,10},{10... | collective-permute-start | bytes 196616 | tf_op jit(solution)/shard_map/ppermute | solution.py:20
  35.3 29.7 %collective-permute-start.14 = (bf16[2,3,32,512]{3,2,1,0:T(8,128)(2,1)S(1)}, bf16[2,3,32,512]{3,2,1,0:T(8,128)(2,1)S(1)}, u32[]{:S(2)}, u32[]{:S(2)}) collective-permute-start(bf16[2,3,32,512]{3,2,1,0:T(8,128)(2,1)S(1)} %pad_maximum_fusion.2), channel_id=1, source_target_pairs={{0,64},{32,96},{64,0},{96,32},{128,192},{160,224},{192,128},{224,1... | collective-permute-start | bytes 589832 | tf_op jit(solution)/shard_map/ppermute | solution.py:47
  37.8 9.5 %collective-permute-start.6 = (bf16[64,512]{1,0:T(8,128)(2,1)S(1)}, bf16[64,512]{1,0:T(8,128)(2,1)S(1)}, u32[]{:S(2)}, u32[]{:S(2)}) collective-permute-start(bf16[64,512]{1,0:T(8,128)(2,1)S(1)} %get-tuple-element.43), channel_id=1, source_target_pairs={{0,24},{8,0},{16,8},{24,16},{1,25},{9,1},{17,9},{25,17},{2,26},{10... | collective-permute-start | bytes 196616 | tf_op jit(solution)/shard_map/ppermute | solution.py:20
  40.3 7.0 %collective-permute-start.5 = (bf16[64,512]{1,0:T(8,128)(2,1)S(1)}, bf16[64,512]{1,0:T(8,128)(2,1)S(1)}, u32[]{:S(2)}, u32[]{:S(2)}) collective-permute-start(bf16[64,512]{1,0:T(8,128)(2,1)S(1)} %get-tuple-element.43), channel_id=1, source_target_pairs={{0,16},{8,24},{16,0},{24,8},{1,17},{9,25},{17,1},{25,9},{2,18},{10... | collective-permute-start | bytes 196616 | tf_op jit(solution)/shard_map/ppermute | solution.py:20
  65.0 12.3 %collective-permute-start.15 = (bf16[4,3,32,512]{3,2,1,0:T(8,128)(2,1)S(1)}, bf16[4,3,32,512]{3,2,1,0:T(8,128)(2,1)S(1)}, u32[]{:S(2)}, u32[]{:S(2)}) collective-permute-start(bf16[4,3,32,512]{3,2,1,0:T(8,128)(2,1)S(1)} %pad_maximum_fusion), channel_id=1, source_target_pairs={{0,32},{32,0},{64,96},{96,64},{128,160},{160,128},{192,224},{224,1... | collective-permute-start | bytes 1179656 | tf_op jit(solution)/shard_map/ppermute | solution.py:47
  79.4 9.5 %collective-permute-start.18 = (bf16[2,256,256]{2,1,0:T(8,128)(2,1)}, bf16[2,256,256]{2,1,0:T(8,128)(2,1)}, u32[]{:S(2)}, u32[]{:S(2)}) collective-permute-start(bf16[2,256,256]{2,1,0:T(8,128)(2,1)} %pad_maximum_fusion.1), channel_id=1, source_target_pairs={{0,3},{1,0},{2,1},{3,2},{4,7},{5,4},{6,5},{7,6},{8,11},{9,8},{10,9... | collective-permute-start | bytes 786440 | tf_op jit(solution)/shard_map/ppermute | solution.py:20
  80.0 13.4 %collective-permute-start.17 = (bf16[2,256,256]{2,1,0:T(8,128)(2,1)}, bf16[2,256,256]{2,1,0:T(8,128)(2,1)}, u32[]{:S(2)}, u32[]{:S(2)}) collective-permute-start(bf16[2,256,256]{2,1,0:T(8,128)(2,1)} %pad_maximum_fusion.1), channel_id=1, source_target_pairs={{0,2},{1,3},{2,0},{3,1},{4,6},{5,7},{6,4},{7,5},{8,10},{9,11},{10,... | collective-permute-start | bytes 786440 | tf_op jit(solution)/shard_map/ppermute | solution.py:20
  82.3 13.8 %collective-permute-start.16 = (bf16[2,256,256]{2,1,0:T(8,128)(2,1)}, bf16[2,256,256]{2,1,0:T(8,128)(2,1)}, u32[]{:S(2)}, u32[]{:S(2)}) collective-permute-start(bf16[2,256,256]{2,1,0:T(8,128)(2,1)} %pad_maximum_fusion.1), channel_id=1, source_target_pairs={{0,1},{1,2},{2,3},{3,0},{4,5},{5,6},{6,7},{7,4},{8,9},{9,10},{10,1... | collective-permute-start | bytes 786440 | tf_op jit(solution)/shard_map/ppermute | solution.py:20
  82.6 1.2 copy-start.16
  83.8 5.1 %copy-start.5 = (bf16[256,512]{1,0:T(8,128)(2,1)S(1)}, bf16[256,512]{1,0:T(8,128)(2,1)}, u32[]{:S(2)}) copy-start(bf16[256,512]{1,0:T(8,128)(2,1)} %get-tuple-element.36) | copy-start | bytes 786436
  83.8 15.6 %copy-start.6 = (bf16[1,8,32,512]{3,2,0,1:T(8,128)(2,1)S(1)}, bf16[1,8,32,512]{3,2,0,1:T(8,128)(2,1)}, u32[]{:S(2)}) copy-start(bf16[1,8,32,512]{3,2,0,1:T(8,128)(2,1)} %get-tuple-element.38) | copy-start | bytes 786436
  84.4 21.1 %copy-start.4 = (bf16[256,512]{1,0:T(8,128)(2,1)S(1)}, bf16[256,512]{1,0:T(8,128)(2,1)}, u32[]{:S(2)}) copy-start(bf16[256,512]{1,0:T(8,128)(2,1)} %get-tuple-element.33) | copy-start | bytes 786436
  88.9 12.9 %collective-permute-start.10 = (bf16[256,512]{1,0:T(8,128)(2,1)S(1)}, bf16[256,512]{1,0:T(8,128)(2,1)S(1)}, u32[]{:S(2)}, u32[]{:S(2)}) collective-permute-start(bf16[256,512]{1,0:T(8,128)(2,1)S(1)} %copy-done.5), channel_id=1, source_target_pairs={{0,1},{1,2},{2,3},{3,0},{4,5},{5,6},{6,7},{7,4},{8,9},{9,10},{10,1... | collective-permute-start | bytes 786440 | tf_op jit(solution)/shard_map/ppermute | solution.py:20
  93.3 8.5 %collective-permute-start.9 = (bf16[256,256]{0,1:T(8,128)(2,1)S(1)}, bf16[256,256]{0,1:T(8,128)(2,1)S(1)}, u32[]{:S(2)}, u32[]{:S(2)}) collective-permute-start(bf16[256,256]{0,1:T(8,128)(2,1)S(1)} %fusion), channel_id=1, source_target_pairs={{0,3},{1,0},{2,1},{3,2},{4,7},{5,4},{6,5},{7,6},{8,11},{9,8},{10,9... | collective-permute-start | bytes 393224 | tf_op jit(solution)/shard_map/ppermute | solution.py:20
  96.1 8.0 %collective-permute-start.8 = (bf16[256,256]{0,1:T(8,128)(2,1)S(1)}, bf16[256,256]{0,1:T(8,128)(2,1)S(1)}, u32[]{:S(2)}, u32[]{:S(2)}) collective-permute-start(bf16[256,256]{0,1:T(8,128)(2,1)S(1)} %fusion), channel_id=1, source_target_pairs={{0,2},{1,3},{2,0},{3,1},{4,6},{5,7},{6,4},{7,5},{8,10},{9,11},{10,... | collective-permute-start | bytes 393224 | tf_op jit(solution)/shard_map/ppermute | solution.py:20
  98.0 7.4 %collective-permute-start.7 = (bf16[256,256]{0,1:T(8,128)(2,1)S(1)}, bf16[256,256]{0,1:T(8,128)(2,1)S(1)}, u32[]{:S(2)}, u32[]{:S(2)}) collective-permute-start(bf16[256,256]{0,1:T(8,128)(2,1)S(1)} %fusion), channel_id=1, source_target_pairs={{0,1},{1,2},{2,3},{3,0},{4,5},{5,6},{6,7},{7,4},{8,9},{9,10},{10,1... | collective-permute-start | bytes 393224 | tf_op jit(solution)/shard_map/ppermute | solution.py:20
  107.7 22.0 %all-to-all-start.1 = ((bf16[64,4,512]{2,1,0:T(4,128)(2,1)}), bf16[64,4,512]{2,1,0:T(4,128)(2,1)S(1)}, u32[]{:S(2)}, u32[]{:S(2)}) async-start(bf16[64,4,512]{2,1,0:T(4,128)(2,1)} %reshape.47), calls=%async_computation.1 | async-start | bytes 524288 | tf_op jit(solution)/shard_map/all_to_all | solution.py:415
  117.5 5.2 %collective-permute-start.19 = (bf16[64,512]{1,0:T(8,128)(2,1)S(1)}, bf16[64,512]{1,0:T(8,128)(2,1)S(1)}, u32[]{:S(2)}, u32[]{:S(2)}) collective-permute-start(bf16[64,512]{1,0:T(8,128)(2,1)S(1)} %get-tuple-element.40), channel_id=1, source_target_pairs={{0,24},{8,0},{16,8},{24,16},{1,25},{9,1},{17,9},{25,17},{2,26},{10... | collective-permute-start | bytes 196616 | tf_op jit(solution)/shard_map/ppermute | solution.py:20
  120.3 8.0 %collective-permute-start.21 = (bf16[64,512]{1,0:T(8,128)(2,1)S(1)}, bf16[64,512]{1,0:T(8,128)(2,1)S(1)}, u32[]{:S(2)}, u32[]{:S(2)}) collective-permute-start(bf16[64,512]{1,0:T(8,128)(2,1)S(1)} %get-tuple-element.41), channel_id=1, source_target_pairs={{0,8},{8,16},{16,24},{24,0},{1,9},{9,17},{17,25},{25,1},{2,10},{10... | collective-permute-start | bytes 196616 | tf_op jit(solution)/shard_map/ppermute | solution.py:20
  120.3 8.0 %collective-permute-start.20 = (bf16[64,512]{1,0:T(8,128)(2,1)S(1)}, bf16[64,512]{1,0:T(8,128)(2,1)S(1)}, u32[]{:S(2)}, u32[]{:S(2)}) collective-permute-start(bf16[64,512]{1,0:T(8,128)(2,1)S(1)} %get-tuple-element.42), channel_id=1, source_target_pairs={{0,16},{8,24},{16,0},{24,8},{1,17},{9,25},{17,1},{25,9},{2,18},{10... | collective-permute-start | bytes 196616 | tf_op jit(solution)/shard_map/ppermute | solution.py:20
  128.4 1.6 %collective-permute-start.22 = (bf16[32,512]{1,0:T(8,128)(2,1)S(1)}, bf16[32,512]{1,0:T(8,128)(2,1)S(1)}, u32[]{:S(2)}, u32[]{:S(2)}) collective-permute-start(bf16[32,512]{1,0:T(8,128)(2,1)S(1)} %slice.91), channel_id=1, source_target_pairs={{0,4},{4,0},{1,5},{5,1},{2,6},{6,2},{3,7},{7,3},{8,12},{12,8},{9,1... | collective-permute-start | bytes 98312 | tf_op jit(solution)/shard_map/ppermute | solution.py:47
  130.3 3.6 %collective-permute-start.25 = (f32[32]{0:T(128)S(1)}, f32[32]{0:T(128)S(1)}, u32[]{:S(2)}, u32[]{:S(2)}) collective-permute-start(f32[32]{0:T(128)S(1)} %get-tuple-element.56), channel_id=1, source_target_pairs={{0,3},{1,0},{2,1},{3,2},{4,7},{5,4},{6,5},{7,6},{8,11},{9,8},{10,9... | collective-permute-start | bytes 392 | tf_op jit(solution)/shard_map/ppermute | solution.py:20
  131.5 5.1 %collective-permute-start.24 = (f32[32]{0:T(128)S(1)}, f32[32]{0:T(128)S(1)}, u32[]{:S(2)}, u32[]{:S(2)}) collective-permute-start(f32[32]{0:T(128)S(1)} %get-tuple-element.56), channel_id=1, source_target_pairs={{0,2},{1,3},{2,0},{3,1},{4,6},{5,7},{6,4},{7,5},{8,10},{9,11},{10,... | collective-permute-start | bytes 392 | tf_op jit(solution)/shard_map/ppermute | solution.py:20
  133.3 4.8 %collective-permute-start.23 = (f32[32]{0:T(128)S(1)}, f32[32]{0:T(128)S(1)}, u32[]{:S(2)}, u32[]{:S(2)}) collective-permute-start(f32[32]{0:T(128)S(1)} %get-tuple-element.56), channel_id=1, source_target_pairs={{0,1},{1,2},{2,3},{3,0},{4,5},{5,6},{6,7},{7,4},{8,9},{9,10},{10,1... | collective-permute-start | bytes 392 | tf_op jit(solution)/shard_map/ppermute | solution.py:20

commit v2 on v1

--- a/solution.py
+++ b/solution.py
@@ -52,7 +52,7 @@
 
 
 MIXER_INPUTS = (
-    "resid", "mix_gain", "routes", "proj_x", "proj_b", "proj_c", "proj_step", "conv_taps",
+    "resid", "mix_gain", "proj_x", "proj_b", "proj_c", "proj_step", "conv_taps",
     "conv_state", "step_bias", "decay_rate", "scan_state", "proj_z", "inner_gain", "proj_out",
 )
 
@@ -69,7 +69,7 @@
 def mixer_kernel(place, *refs):
     count = len(MIXER_INPUTS)
     sources, refs = refs[:count], refs[count:]
-    (part, state_out, conv_out, in_slot), refs = refs[:4], refs[4:]
+    (part, state_out, conv_out), refs = refs[:3], refs[3:]
     held, refs = refs[:count], refs[count:]
     new_state, new_conv, keep_rows, sems, in_sems, out_sems = refs
     at = dict(zip(MIXER_INPUTS, held))
@@ -104,7 +104,6 @@
 
     seqs = part.shape[0]
     heads, head_dim, lanes = new_state.shape[1:]
-    slots = in_slot.shape[0]
     copies["resid"].wait()
     copies["mix_gain"].wait()
     values = at["resid"][...].astype(jnp.float32)
@@ -118,22 +117,6 @@
         ],
         axis=1,
     ).astype(jnp.bfloat16)
-
-    copies["routes"].wait()
-    slot_ids = lax.broadcasted_iota(jnp.int32, (slots, seqs), 0)
-    picked = jnp.zeros((slots, seqs), jnp.bool_)
-    for k in range(at["routes"].shape[0]):
-        picked = picked | ((slot_ids >> 2) == at["routes"][k : k + 1])
-    earlier = lax.broadcasted_iota(jnp.int32, (seqs, seqs), 0) < lax.broadcasted_iota(
-        jnp.int32, (seqs, seqs), 1
-    )
-    rank = dot32(
-        jnp.where(picked, 1.0, 0.0).astype(jnp.bfloat16),
-        jnp.where(earlier, 1.0, 0.0).astype(jnp.bfloat16),
-    )
-    in_slot[...] = jnp.where(
-        picked & (rank.astype(jnp.int32) == (slot_ids & 3)), 1.0, 0.0
-    )
 
     raws = []
     for name in ("proj_x", "proj_b", "proj_c"):
@@ -228,7 +211,7 @@
     conv_copy.wait()
 
 
-def mixer(slots, place, **arrays):
+def mixer(place, **arrays):
     arrays = [arrays[name] for name in MIXER_INPUTS]
     at = dict(zip(MIXER_INPUTS, arrays))
     resid, conv_state, scan_state = at["resid"], at["conv_state"], at["scan_state"]
@@ -243,7 +226,7 @@
         mixer_kernel,
         name="mixer",
         in_specs=[pl.BlockSpec(memory_space=pltpu.SMEM)] + [hbm] * len(arrays),
-        out_specs=[vmem, hbm, hbm, vmem],
+        out_specs=[vmem, hbm, hbm],
         scratch_shapes=held
         + [
             pltpu.VMEM(scan_state.shape, scan_state.dtype),
@@ -257,15 +240,52 @@
             jax.ShapeDtypeStruct(resid.shape, jnp.bfloat16),
             jax.ShapeDtypeStruct(scan_state.shape, jnp.float32),
             jax.ShapeDtypeStruct(conv_state.shape, jnp.bfloat16),
-            jax.ShapeDtypeStruct((slots, resid.shape[0]), jnp.float32),
         ],
     )(place, *arrays)
 
 
+def expert_in_kernel(rows, gate, up, hidden):
+    gate_value = dot32(rows[...], gate[...])
+    hidden[...] = (silu(gate_value) * dot32(rows[...], up[...])).astype(jnp.bfloat16)
+
+
+def expert_out_kernel(*refs):
+    half = len(refs) // 2
+    total = dot32(refs[0][...], refs[half][...])
+    for k in range(1, half):
+        total = total + dot32(refs[k][...], refs[half + k][...])
+    refs[-1][...] = total.astype(jnp.bfloat16)
+
+
+def simple_call(kernel, shape, *arrays):
+    vmem = pl.BlockSpec(memory_space=pltpu.VMEM)
+    return pl.pallas_call(
+        kernel,
+        in_specs=[vmem] * len(arrays),
+        out_specs=vmem,
+        compiler_params=pltpu.CompilerParams(vmem_limit_bytes=FEEDER_VMEM),
+        out_shape=jax.ShapeDtypeStruct(shape, jnp.bfloat16),
+    )(*arrays)
+
+
 def feeder_kernel(
-    place, part_0, part_1, part_2, part_3, resid, post_gain, ffn_gain, in_slot,
-    stream_quarter, feed, feed_quarter, outgoing,
+    place, part_0, part_1, part_2, part_3, resid, post_gain, ffn_gain, routes,
+    stream_quarter, feed, feed_quarter, outgoing, in_slot,
 ):
+    slots, seqs = in_slot.shape
+    slot_ids = lax.broadcasted_iota(jnp.int32, (slots, seqs), 0)
+    picked = jnp.zeros((slots, seqs), jnp.bool_)
+    for k in range(routes.shape[0]):
+        picked = picked | ((slot_ids >> 2) == routes[k : k + 1])
+    earlier = lax.broadcasted_iota(jnp.int32, (seqs, seqs), 0) < lax.broadcasted_iota(
+        jnp.int32, (seqs, seqs), 1
+    )
+    rank = dot32(
+        jnp.where(picked, 1.0, 0.0).astype(jnp.bfloat16),
+        jnp.where(earlier, 1.0, 0.0).astype(jnp.bfloat16),
+    )
+    placed = jnp.where(picked & (rank.astype(jnp.int32) == (slot_ids & 3)), 1.0, 0.0)
+    in_slot[...] = placed
     mixed = sum_of([part_0[...], part_1[...], part_2[...], part_3[...]])
     total = resid[...].astype(jnp.float32) + scaled_rows(mixed, post_gain[...])
     total = total.astype(jnp.bfloat16)
@@ -279,10 +299,10 @@
             stream_quarter[...] = total[:, q * quarter : (q + 1) * quarter]
             feed_quarter[...] = fed[:, q * quarter : (q + 1) * quarter]
 
-    outgoing[...] = dot32(in_slot[...], fed).reshape(outgoing.shape).astype(jnp.bfloat16)
-
-
-def feeder(quarter, place, *arrays):
+    outgoing[...] = dot32(placed.astype(jnp.bfloat16), fed).reshape(outgoing.shape).astype(jnp.bfloat16)
+
+
+def feeder(slots, quarter, place, *arrays):
     vmem = pl.BlockSpec(memory_space=pltpu.VMEM)
     rows = jax.ShapeDtypeStruct(arrays[0].shape, jnp.bfloat16)
     share = jax.ShapeDtypeStruct((arrays[0].shape[0], quarter), jnp.bfloat16)
@@ -290,13 +310,14 @@
         feeder_kernel,
         name="feeder",
         in_specs=[pl.BlockSpec(memory_space=pltpu.SMEM)] + [vmem] * len(arrays),
-        out_specs=[vmem] * 4,
+        out_specs=[vmem] * 5,
         compiler_params=pltpu.CompilerParams(vmem_limit_bytes=FEEDER_VMEM),
         out_shape=[
             share,
             rows,
             share,
-            jax.ShapeDtypeStruct((arrays[-1].shape[0] // 4, 4, arrays[0].shape[1]), jnp.bfloat16),
+            jax.ShapeDtypeStruct((slots // 4, 4, arrays[0].shape[1]), jnp.bfloat16),
+            jax.ShapeDtypeStruct((slots, arrays[0].shape[0]), jnp.float32),
         ],
     )(place, *arrays)
 
@@ -340,7 +361,6 @@
     blocks = jnp.stack([dense_gate, dense_up, dense_down])[None]
     blocks = jnp.concatenate([blocks, from_flip(blocks, "ep_0", 4)])
     blocks = jnp.concatenate([blocks, from_flip(blocks, "ep_0", 2)])
-    blocks = jnp.concatenate([blocks, from_flip(blocks, "ep_0", 1)])
     unit_rows = jnp.moveaxis(blocks, 0, 1).reshape(3, blocks.shape[0] * units, quarter)
     expert_count = expert_router.shape[1]
     group_size = expert_count // group_router.shape[1]
@@ -348,12 +368,10 @@
     capacity = 2 * seqs * pick_count // expert_count
 
     place = jnp.full((1,), tp_index, jnp.int32)
-    part, new_state, new_conv, in_slot = mixer(
-        expert_count * capacity,
+    part, new_state, new_conv = mixer(
         place,
         resid=resid,
         mix_gain=mix_gain.reshape(-1, channels),
-        routes=route_experts.T,
         proj_x=proj_x,
         proj_b=proj_b,
         proj_c=proj_c,
@@ -370,51 +388,32 @@
     new_conv = new_conv.transpose(2, 0, 1, 3)
     mixed_parts = from_all(part, "tp")
     mixed_parts[0] = part.astype(jnp.float32)
-    down, part = lax.optimization_barrier((expert_down[0], part))
+    stream_quarter, feed, feed_quarter, outgoing, in_slot = feeder(
+        expert_count * capacity, quarter, place, *mixed_parts, resid.astype(jnp.float32),
+        post_gain[None], ffn_gain[None], route_experts.T,
+    )
+
+    arrived = lax.all_to_all(
+        outgoing, EP, 0, 0, tiled=True
+    )
+    rows = arrived.reshape(expert_count * capacity, width)
+
+    tokens = jnp.concatenate([feed_quarter, from_flip(feed_quarter, "ep_0", 1)], axis=0)
+    tokens = jnp.concatenate(from_all(tokens, "ep_1"), axis=0)
+    tokens = jnp.concatenate([tokens, from_flip(tokens, "ep_2", 1)], axis=0)
+    feed, tokens = lax.optimization_barrier((feed, tokens))
+    gate_rows, up_rows, down_rows = unit_rows
+    down = expert_down[0]
     down_parts = [
         lax.dynamic_slice_in_dim(down, ((tp_index + s) % tp_count) * quarter, quarter, 1)
         for s in range(tp_count)
     ]
-    stream_quarter, feed, feed_quarter, outgoing = feeder(
-        quarter, place, *mixed_parts, resid.astype(jnp.float32), post_gain[None],
-        ffn_gain[None], in_slot.astype(jnp.bfloat16),
-    )
-
-    arrived = lax.all_to_all(
-        outgoing, EP, 0, 0, tiled=True
-    )
-    rows = arrived.reshape(expert_count * capacity, width)
-
-    tokens = jnp.concatenate([feed_quarter, from_flip(feed_quarter, "ep_2", 1)], axis=0)
-    tokens = jnp.concatenate(from_all(tokens, "ep_1"), axis=0)
-    feed, tokens = lax.optimization_barrier((feed, tokens))
-    gate_rows, up_rows, down_rows = unit_rows
     down_parts = [down_parts[0]] + [from_shift(down_parts[s], "tp", s) for s in range(1, tp_count)]
     across = (((1,), (1,)), ((), ()))
     gate_piece = lax.dot_general(tokens, gate_rows, across, preferred_element_type=jnp.float32)
     up_piece = lax.dot_general(tokens, up_rows, across, preferred_element_type=jnp.float32)
     pieces = jnp.stack([gate_piece, up_piece]).astype(jnp.bfloat16)
     sums = from_all(pieces, "tp")
-
-    gate_value = dot32(rows, expert_gate[0])
-    up_value = dot32(rows, expert_up[0])
-    hidden = (jax.nn.silu(gate_value) * up_value).astype(jnp.bfloat16)
-    _, *sums = lax.optimization_barrier((hidden, *sums))
-    hidden_parts = from_all(hidden, "tp")
-    sums = sum_of(sums)
-    dense_hidden = (jax.nn.silu(sums[0]) * sums[1]).astype(jnp.bfloat16)
-    dense_part = dot32(dense_hidden, down_rows).astype(jnp.bfloat16)
-    lots = dense_part.reshape(lax.axis_size("ep_1"), 2 * seqs, quarter)
-    lots = sum_of([lots[0]] + [from_shift(lots[b], "ep_1", -b) for b in range(1, lots.shape[0])])
-    dense_part = lots[:seqs] + from_flip(lots[seqs:].astype(jnp.bfloat16), "ep_2", 1)
-    dense_out = dense_part
-
-    served = dot32(
-        jnp.concatenate(hidden_parts, axis=1), jnp.concatenate(down_parts, axis=0)
-    ).astype(jnp.bfloat16)
-    returned = lax.all_to_all(
-        served.reshape(expert_count, capacity, quarter), EP, 0, 0, tiled=True
-    ).reshape(expert_count * capacity, quarter)
 
     features = (((0,), (1,)), ((), ()))
     group_exp = jnp.exp(
@@ -436,12 +435,40 @@
     slot_weight = in_slot * jnp.repeat(pick_weight, capacity, axis=0)
     weight_high = slot_weight.astype(jnp.bfloat16)
     weight_low = (slot_weight - weight_high.astype(jnp.float32)).astype(jnp.bfloat16)
+    switch = jax.nn.sigmoid(dot32(feed, dense_switch))
+    rows, weight_high, weight_low, switch = lax.optimization_barrier(
+        (rows, weight_high, weight_low, switch)
+    )
+
+    hidden = simple_call(
+        expert_in_kernel, (rows.shape[0], expert_gate.shape[2]),
+        rows, expert_gate[0], expert_up[0],
+    )
+    _, *sums = lax.optimization_barrier((hidden, *sums))
+    hidden_parts = from_all(hidden, "tp")
+    sums = sum_of(sums)
+    dense_hidden = (jax.nn.silu(sums[0]) * sums[1]).astype(jnp.bfloat16)
+    dense_part = dot32(dense_hidden, down_rows).astype(jnp.bfloat16)
+    half = dense_part.shape[0] // 2
+    lots = sum_of([dense_part[:half], from_flip(dense_part[half:], "ep_2", 1)])
+    lots = lots.astype(jnp.bfloat16).reshape(lax.axis_size("ep_1"), 2, seqs, quarter)
+    lots = sum_of([lots[:, 0], from_flip(lots[:, 1], "ep_0", 1)])
+    lots = lots.astype(jnp.bfloat16)
+    dense_part = sum_of(
+        [lots[0]] + [from_shift(lots[b], "ep_1", -b) for b in range(1, lots.shape[0])]
+    )
+    dense_out = dense_part
+
+    served = simple_call(expert_out_kernel, (rows.shape[0], quarter), *hidden_parts, *down_parts)
+    returned = lax.all_to_all(
+        served.reshape(expert_count, capacity, quarter), EP, 0, 0, tiled=True
+    ).reshape(expert_count * capacity, quarter)
+
     slotwise = (((0,), (0,)), ((), ()))
     routed = lax.dot_general(
         weight_high, returned, slotwise, preferred_element_type=jnp.float32
     ) + lax.dot_general(weight_low, returned, slotwise, preferred_element_type=jnp.float32)
 
-    switch = jax.nn.sigmoid(dot32(feed, dense_switch))
     combined = routed + switch[:, None] * dense_out
     squares = jnp.sum(combined * combined, axis=1)
     total_square = sum_of(from_all(squares, "tp"))

time: 140 us -> 127 us (0.907)
  waiting for transfers between devices: 52.1 us -> 39.3 us
  matrix products: 4.38 us -> 1.98 us
  other arithmetic: 3.1 us -> 4.73 us
    ppermute x5 -> x6, waiting for transfers between devices: 25.7 us -> 3.69 us  [from_flip(): return lax.ppermute(array, axis, [(i, i ^ bit) for i in range(count)])]
    all_to_all x1, waiting for transfers between devices: 0.01 us -> 8.52 us  [on_device(): arrived = lax.all_to_all(outgoing, EP, 0, 0, tiled=True)]
    all_to_all x1, waiting for transfers between devices: 1.24 us -> 7.65 us  [on_device(): lax.all_to_all(served.reshape(expert_count, capacity, quarter), EP, 0, 0,...]
    ppermute x21, waiting for transfers between devices: 25.1 us -> 19.5 us  [from_shift(): lax.ppermute(array, axis, [(i, (i + shift) % count) for i in range(count)])]
    dot_general x5 -> x2, matrix products: 2.93 us -> 0.45 us  [dot32(): return jnp.dot(a, b, preferred_element_type=jnp.float32)]
    ppermute x5 -> x6, starting transfers between devices: 12.4 us -> 10.7 us  [from_flip(): return lax.ppermute(array, axis, [(i, i ^ bit) for i in range(count)])]
  transfers between devices with their start and end apart: 28 -> 29, of which waited for: 13 -> 12; matrix products, arithmetic and copies ran while one was open for 5% -> 6% of each run, Pallas kernels for 1% -> 2%
where the time goes in v2:
time: 127 us; the launch traced here: 126 us
  starting transfers between devices  65.8 us (52%)
  waiting for transfers between devices  39.3 us (31%)
  Pallas kernels  8.74 us (7%)
  other arithmetic  4.73 us (4%)
  local copies, waits for them, and re-layouts  3.9 us (3%)
  matrix products  1.98 us (2%)
    ppermute x21, starting transfers between devices, from_shift(): lax.ppermute(array, axis, [(i, (i + shift) % count) for i in range(count)])  35.1 us
    ppermute x21, waiting for transfers between devices, from_shift(): lax.ppermute(array, axis, [(i, (i + shift) % count) for i in range(count)])  19.5 us
    all_to_all x1, starting transfers between devices, on_device(): lax.all_to_all(served.reshape(expert_count, capacity, quarter), EP, 0, 0,...  11 us
    ppermute x6, starting transfers between devices, from_flip(): return lax.ppermute(array, axis, [(i, i ^ bit) for i in range(count)])  10.7 us
    all_to_all x1, starting transfers between devices, on_device(): arrived = lax.all_to_all(outgoing, EP, 0, 0, tiled=True)  8.95 us
    all_to_all x1, waiting for transfers between devices, on_device(): arrived = lax.all_to_all(outgoing, EP, 0, 0, tiled=True)  8.52 us
    all_to_all x1, waiting for transfers between devices, on_device(): lax.all_to_all(served.reshape(expert_count, capacity, quarter), EP, 0, 0,...  7.65 us
    pallas_call x1, Pallas kernels, mixer(): pl.pallas_call(mixer_kernel, name='mixer', in_specs=[pl.BlockSpec(memory_...  5.82 us
  transfers between devices with their start and end apart: 29, of which 12 were waited for; matrix products, arithmetic and copies ran while one was open for 6% of the time, Pallas kernels for 2%

profile of v2, /device:TPU:32, one launch (start us, length us, event | category | flops | bytes accessed | tf_op | source)
XLA Modules:
  0.0 125.7 jit_solution(8419665824595000970)
XLA Ops:
  0.7 5.8 %mixer.1 = (bf16[32,2048]{1,0:T(8,128)(2,1)}, f32[32,2,64,128]{3,2,1,0:T(8,128)}, bf16[3,3,32,128]{3,2,1,0:T(8,128)(2,1)}) custom-call(s32[1]{0:T(128)} %bitcast.place, bf16[32,2048]{1,0:T(8,128)(2,1)} %refs_0_.1, bf16[16,128]{1,0:T(8,128)(2,1)} %bitcast.116, bf16[2048,128]{1,0:T(8,128)(2,1)} %refs_2_.1, bf16[2048,128]{1,0:T(8,128)(2,1)} %refs_3_.1, ...), custom_call_target="tpu_custom_call" | custom-call | tf_op jit(solution)/shard_map/mixer/pallas_call | solution.py:225
  6.6 1.6 %collective-permute-start = (bf16[32,2048]{1,0:T(8,128)(2,1)}, bf16[32,2048]{1,0:T(8,128)(2,1)S(1)}, u32[]{:S(2)}, u32[]{:S(2)}) collective-permute-start(bf16[32,2048]{1,0:T(8,128)(2,1)} %get-tuple-element.21), channel_id=1, source_target_pairs={{0,1},{1,2},{2,3},{3,0},{4,5},{5,6},{6,7},{7,4},{8,9},{9,10},{10,1... | collective-permute-start | bytes 393224 | tf_op jit(solution)/shard_map/ppermute | solution.py:20
  8.1 2.7 %collective-permute-start.1 = (bf16[32,2048]{1,0:T(8,128)(2,1)}, bf16[32,2048]{1,0:T(8,128)(2,1)S(1)}, u32[]{:S(2)}, u32[]{:S(2)}) collective-permute-start(bf16[32,2048]{1,0:T(8,128)(2,1)} %get-tuple-element.21), channel_id=1, source_target_pairs={{0,2},{1,3},{2,0},{3,1},{4,6},{5,7},{6,4},{7,5},{8,10},{9,11},{10,... | collective-permute-start | bytes 393224 | tf_op jit(solution)/shard_map/ppermute | solution.py:20
  10.9 1.4 %collective-permute-start.2 = (bf16[32,2048]{1,0:T(8,128)(2,1)}, bf16[32,2048]{1,0:T(8,128)(2,1)S(1)}, u32[]{:S(2)}, u32[]{:S(2)}) collective-permute-start(bf16[32,2048]{1,0:T(8,128)(2,1)} %get-tuple-element.21), channel_id=1, source_target_pairs={{0,3},{1,0},{2,1},{3,2},{4,7},{5,4},{6,5},{7,6},{8,11},{9,8},{10,9... | collective-permute-start | bytes 393224 | tf_op jit(solution)/shard_map/ppermute | solution.py:20
  12.3 6.4 %collective-permute-start.14 = (bf16[1,3,32,512]{3,2,1,0:T(8,128)(2,1)S(1)}, bf16[1,3,32,512]{3,2,1,0:T(8,128)(2,1)S(1)}, u32[]{:S(2)}, u32[]{:S(2)}) collective-permute-start(bf16[1,3,32,512]{3,2,1,0:T(8,128)(2,1)S(1)} %maximum_bitcast_fusion.1), channel_id=1, source_target_pairs={{0,128},{32,160},{64,192},{96,224},{128,0},{160,32},{192,64},{224,... | collective-permute-start | bytes 294920 | tf_op jit(solution)/shard_map/ppermute | solution.py:47
  18.7 0.9 convert_element_type.82.part_0
  19.8 1.8 %feeder.1 = (bf16[32,512]{1,0:T(8,128)(2,1)S(1)}, bf16[32,2048]{1,0:T(8,128)(2,1)S(1)}, bf16[32,512]{1,0:T(8,128)(2,1)S(1)}, bf16[64,4,2048]{2,1,0:T(4,128)(2,1)}, f32[256,32]{1,0:T(8,128)S(1)}) custom-call(s32[1]{0:T(128)} %bitcast.place, f32[32,2048]{1,0:T(8,128)S(1)} %convert_element_type.82.part_0, bf16[32,2048]{1,0:T(8,128)(2,1)S(1)} %collective-permute-done.part_1, ...), custom_call_target="tpu_custom_call" | custom-call | tf_op jit(solution)/shard_map/feeder/pallas_call | solution.py:309
  21.6 0.6 copy-done.3
  22.2 1.0 collective-permute-start.3
  23.2 2.9 %collective-permute-done.3 = bf16[32,512]{1,0:T(8,128)(2,1)S(1)} collective-permute-done((bf16[32,512]{1,0:T(8,128)(2,1)S(1)}, bf16[32,512]{1,0:T(8,128)(2,1)S(1)}, u32[]{:S(2)}, u32[]{:S(2)}) %collective-permute-start.3) | collective-permute-done | bytes 32800 | tf_op jit(solution)/shard_map/ppermute | solution.py:47
  26.1 1.6 %collective-permute-start.4 = (bf16[64,512]{1,0:T(8,128)(2,1)S(1)}, bf16[64,512]{1,0:T(8,128)(2,1)S(1)}, u32[]{:S(2)}, u32[]{:S(2)}) collective-permute-start(bf16[64,512]{1,0:T(8,128)(2,1)S(1)} %get-tuple-element.59), channel_id=1, source_target_pairs={{0,8},{8,16},{16,24},{24,0},{1,9},{9,17},{17,25},{25,1},{2,10},{10... | collective-permute-start | bytes 196616 | tf_op jit(solution)/shard_map/ppermute | solution.py:20
  27.8 1.6 %collective-permute-start.15 = (bf16[2,3,32,512]{3,2,1,0:T(8,128)(2,1)S(1)}, bf16[2,3,32,512]{3,2,1,0:T(8,128)(2,1)S(1)}, u32[]{:S(2)}, u32[]{:S(2)}) collective-permute-start(bf16[2,3,32,512]{3,2,1,0:T(8,128)(2,1)S(1)} %pad_maximum_fusion.1), channel_id=1, source_target_pairs={{0,64},{32,96},{64,0},{96,32},{128,192},{160,224},{192,128},{224,1... | collective-permute-start | bytes 589832 | tf_op jit(solution)/shard_map/ppermute | solution.py:47
  29.4 8.9 %all-to-all-start = ((bf16[64,4,2048]{2,1,0:T(4,128)(2,1)}), bf16[64,4,2048]{2,1,0:T(4,128)(2,1)}, u32[]{:S(2)}, u32[]{:S(2)}) async-start(bf16[64,4,2048]{2,1,0:T(4,128)(2,1)} %get-tuple-element.23), calls=%async_computation | async-start | bytes 2097152 | tf_op jit(solution)/shard_map/all_to_all | solution.py:396
  38.3 3.1 %collective-permute-start.5 = (bf16[64,512]{1,0:T(8,128)(2,1)S(1)}, bf16[64,512]{1,0:T(8,128)(2,1)S(1)}, u32[]{:S(2)}, u32[]{:S(2)}) collective-permute-start(bf16[64,512]{1,0:T(8,128)(2,1)S(1)} %get-tuple-element.59), channel_id=1, source_target_pairs={{0,16},{8,24},{16,0},{24,8},{1,17},{9,25},{17,1},{25,9},{2,18},{10... | collective-permute-start | bytes 196616 | tf_op jit(solution)/shard_map/ppermute | solution.py:20
  41.4 1.2 collective-permute-start.6
  42.6 3.4 %collective-permute-done.5 = bf16[64,512]{1,0:T(8,128)(2,1)S(1)} collective-permute-done((bf16[64,512]{1,0:T(8,128)(2,1)S(1)}, bf16[64,512]{1,0:T(8,128)(2,1)S(1)}, u32[]{:S(2)}, u32[]{:S(2)}) %collective-permute-start.5) | collective-permute-done | bytes 65568 | tf_op jit(solution)/shard_map/ppermute | solution.py:20
  45.9 1.8 %collective-permute-done.6 = bf16[64,512]{1,0:T(8,128)(2,1)S(1)} collective-permute-done((bf16[64,512]{1,0:T(8,128)(2,1)S(1)}, bf16[64,512]{1,0:T(8,128)(2,1)S(1)}, u32[]{:S(2)}, u32[]{:S(2)}) %collective-permute-start.6) | collective-permute-done | bytes 65568 | tf_op jit(solution)/shard_map/ppermute | solution.py:20
  47.8 0.1 collective-permute-start.7
  47.9 0.7 fusion.22
  48.6 0.8 collective-permute-done.7
  49.4 0.3 fusion
  49.7 0.3 fusion.1
  50.0 0.7 pad_maximum_fusion
  50.7 1.3 %collective-permute-start.16 = (bf16[2,512,128]{2,1,0:T(8,128)(2,1)}, bf16[2,512,128]{2,1,0:T(8,128)(2,1)}, u32[]{:S(2)}, u32[]{:S(2)}) collective-permute-start(bf16[2,512,128]{2,1,0:T(8,128)(2,1)} %pad_maximum_fusion), channel_id=1, source_target_pairs={{0,1},{1,2},{2,3},{3,0},{4,5},{5,6},{6,7},{7,4},{8,9},{9,10},{10,1... | collective-permute-start | bytes 786440 | tf_op jit(solution)/shard_map/ppermute | solution.py:20
  52.1 2.4 %collective-permute-start.17 = (bf16[2,512,128]{2,1,0:T(8,128)(2,1)}, bf16[2,512,128]{2,1,0:T(8,128)(2,1)}, u32[]{:S(2)}, u32[]{:S(2)}) collective-permute-start(bf16[2,512,128]{2,1,0:T(8,128)(2,1)} %pad_maximum_fusion), channel_id=1, source_target_pairs={{0,2},{1,3},{2,0},{3,1},{4,6},{5,7},{6,4},{7,5},{8,10},{9,11},{10,... | collective-permute-start | bytes 786440 | tf_op jit(solution)/shard_map/ppermute | solution.py:20
  54.5 1.6 %collective-permute-start.18 = (bf16[2,512,128]{2,1,0:T(8,128)(2,1)}, bf16[2,512,128]{2,1,0:T(8,128)(2,1)}, u32[]{:S(2)}, u32[]{:S(2)}) collective-permute-start(bf16[2,512,128]{2,1,0:T(8,128)(2,1)} %pad_maximum_fusion), channel_id=1, source_target_pairs={{0,3},{1,0},{2,1},{3,2},{4,7},{5,4},{6,5},{7,6},{8,11},{9,8},{10,9... | collective-permute-start | bytes 786440 | tf_op jit(solution)/shard_map/ppermute | solution.py:20
  56.1 0.2 fusion.23
  56.2 0.1 fusion.8
  56.4 0.3 fusion.24
  56.8 0.1 copy.31
  57.0 0.7 subtract_convert_fusion
  57.6 8.5 %all-to-all-done = bf16[64,4,2048]{2,1,0:T(4,128)(2,1)} async-done(((bf16[64,4,2048]{2,1,0:T(4,128)(2,1)}), bf16[64,4,2048]{2,1,0:T(4,128)(2,1)}, u32[]{:S(2)}, u32[]{:S(2)}) %all-to-all-start) | async-done | bytes 1048608 | tf_op jit(solution)/shard_map/all_to_all | solution.py:396
  66.1 1.3 %reshape.47.rows = bf16[256,2048]{1,0:T(8,128)(2,1)S(1)} reshape(bf16[64,4,2048]{2,1,0:T(4,128)(2,1)} %all-to-all-done) | data formatting | bytes 2097152 | tf_op jit(solution)/shard_map/reshape | solution.py:399
  67.5 0.7 shard_map.274.refs_0_
  68.3 1.4 %convert_add_fusion = f32[2,512,128]{2,1,0:T(8,128)S(1)} fusion(bf16[2,512,128]{2,1,0:T(8,128)(2,1)} %collective-permute-done.18, bf16[2,512,128]{2,1,0:T(8,128)(2,1)} %collective-permute-done.17, bf16[2,512,128]{2,1,0:T(8,128)(2,1)} %collective-permute-done.16, bf16[2,512,128]{2,1,0:T(8,128)(2,1)} %pad_maximum_fusion), kind=kLoop, calls=%fused_computation.17 | loop fusion | flops 917504 | bytes 1572864 | tf_op jit(solution)/shard_map/add | solution.py:41
  69.7 0.3 convolution_convert_fusion
  70.0 0.3 collective-permute-start.19
  70.4 0.1 dynamic-slice_bitcast_fusion
  70.5 1.4 %collective-permute-start.11 = (bf16[256,512]{1,0:T(8,128)(2,1)S(1)}, bf16[256,512]{1,0:T(8,128)(2,1)S(1)}, u32[]{:S(2)}, u32[]{:S(2)}) collective-permute-start(bf16[256,512]{1,0:T(8,128)(2,1)S(1)} %get-tuple-element.40), channel_id=1, source_target_pairs={{0,1},{1,2},{2,3},{3,0},{4,5},{5,6},{6,7},{7,4},{8,9},{9,10},{10,1... | collective-permute-start | bytes 786440 | tf_op jit(solution)/shard_map/ppermute | solution.py:20
  71.9 2.4 %collective-permute-start.12 = (bf16[256,512]{1,0:T(8,128)(2,1)S(1)}, bf16[256,512]{1,0:T(8,128)(2,1)S(1)}, u32[]{:S(2)}, u32[]{:S(2)}) collective-permute-start(bf16[256,512]{1,0:T(8,128)(2,1)S(1)} %get-tuple-element.42), channel_id=1, source_target_pairs={{0,2},{1,3},{2,0},{3,1},{4,6},{5,7},{6,4},{7,5},{8,10},{9,11},{10,... | collective-permute-start | bytes 786440 | tf_op jit(solution)/shard_map/ppermute | solution.py:20
  74.3 1.6 %collective-permute-start.13 = (bf16[256,512]{1,0:T(8,128)(2,1)S(1)}, bf16[256,512]{1,0:T(8,128)(2,1)S(1)}, u32[]{:S(2)}, u32[]{:S(2)}) collective-permute-start(bf16[256,512]{1,0:T(8,128)(2,1)S(1)} %get-tuple-element.39), channel_id=1, source_target_pairs={{0,3},{1,0},{2,1},{3,2},{4,7},{5,4},{6,5},{7,6},{8,11},{9,8},{10,9... | collective-permute-start | bytes 786440 | tf_op jit(solution)/shard_map/ppermute | solution.py:20
  75.8 0.1 collective-permute-start.10
  76.0 1.9 %collective-permute-start.8 = (bf16[256,256]{1,0:T(8,128)(2,1)S(1)}, bf16[256,256]{1,0:T(8,128)(2,1)S(1)}, u32[]{:S(2)}, u32[]{:S(2)}) collective-permute-start(bf16[256,256]{1,0:T(8,128)(2,1)S(1)} %shard_map.274.refs_0_), channel_id=1, source_target_pairs={{0,1},{1,2},{2,3},{3,0},{4,5},{5,6},{6,7},{7,4},{8,9},{9,10},{10,1... | collective-permute-start | bytes 393224 | tf_op jit(solution)/shard_map/ppermute | solution.py:20
  77.9 8.1 %collective-permute-done.11.refs_5_ = bf16[256,512]{1,0:T(8,128)(2,1)S(1)} collective-permute-done((bf16[256,512]{1,0:T(8,128)(2,1)S(1)}, bf16[256,512]{1,0:T(8,128)(2,1)S(1)}, u32[]{:S(2)}, u32[]{:S(2)}) %collective-permute-start.11) | collective-permute-done | bytes 262176 | tf_op jit(solution)/shard_map/ppermute | solution.py:20
  86.0 1.8 %collective-permute-start.9 = (bf16[256,256]{1,0:T(8,128)(2,1)S(1)}, bf16[256,256]{1,0:T(8,128)(2,1)S(1)}, u32[]{:S(2)}, u32[]{:S(2)}) collective-permute-start(bf16[256,256]{1,0:T(8,128)(2,1)S(1)} %shard_map.274.refs_0_), channel_id=1, source_target_pairs={{0,2},{1,3},{2,0},{3,1},{4,6},{5,7},{6,4},{7,5},{8,10},{9,11},{10,... | collective-permute-start | bytes 393224 | tf_op jit(solution)/shard_map/ppermute | solution.py:20
  87.8 1.3 %collective-permute-start.20 = (bf16[4,32,512]{2,1,0:T(8,128)(2,1)S(1)}, bf16[4,32,512]{2,1,0:T(8,128)(2,1)S(1)}, u32[]{:S(2)}, u32[]{:S(2)}) collective-permute-start(bf16[4,32,512]{2,1,0:T(8,128)(2,1)S(1)} %slice_bitcast_fusion), channel_id=1, source_target_pairs={{0,32},{32,0},{64,96},{96,64},{128,160},{160,128},{192,224},{224,1... | collective-permute-start | bytes 393224 | tf_op jit(solution)/shard_map/ppermute | solution.py:47
  89.1 1.1 collective-permute-done.10.refs_3_
  90.3 2.2 %collective-permute-done.9.refs_2_ = bf16[256,256]{1,0:T(8,128)(2,1)S(1)} collective-permute-done((bf16[256,256]{1,0:T(8,128)(2,1)S(1)}, bf16[256,256]{1,0:T(8,128)(2,1)S(1)}, u32[]{:S(2)}, u32[]{:S(2)}) %collective-permute-start.9) | collective-permute-done | bytes 131104 | tf_op jit(solution)/shard_map/ppermute | solution.py:20
  92.5 0.4 shard_map.275
  92.9 0.8 reshape.49
  93.7 11.0 %all-to-all-start.1 = ((bf16[64,4,512]{2,1,0:T(4,128)(2,1)}), bf16[64,4,512]{2,1,0:T(4,128)(2,1)S(1)}, u32[]{:S(2)}, u32[]{:S(2)}) async-start(bf16[64,4,512]{2,1,0:T(4,128)(2,1)} %reshape.49), calls=%async_computation.1 | async-start | bytes 524288 | tf_op jit(solution)/shard_map/all_to_all | solution.py:463
  104.8 2.8 %collective-permute-start.21 = (bf16[32,512]{1,0:T(8,128)(2,1)S(1)}, bf16[32,512]{1,0:T(8,128)(2,1)S(1)}, u32[]{:S(2)}, u32[]{:S(2)}) collective-permute-start(bf16[32,512]{1,0:T(8,128)(2,1)S(1)} %get-tuple-element.48), channel_id=1, source_target_pairs={{0,24},{8,0},{16,8},{24,16},{1,25},{9,1},{17,9},{25,17},{2,26},{10... | collective-permute-start | bytes 98312 | tf_op jit(solution)/shard_map/ppermute | solution.py:20
  107.6 0.9 collective-permute-start.22
  108.4 0.9 collective-permute-start.23
  109.3 7.6 %all-to-all-done.1 = bf16[64,4,512]{2,1,0:T(4,128)(2,1)S(1)} async-done(((bf16[64,4,512]{2,1,0:T(4,128)(2,1)}), bf16[64,4,512]{2,1,0:T(4,128)(2,1)S(1)}, u32[]{:S(2)}, u32[]{:S(2)}) %all-to-all-start.1) | async-done | bytes 262176 | tf_op jit(solution)/shard_map/all_to_all | solution.py:463
  117.0 0.2 fusion.25
  117.2 0.3 multiply_reduce_fusion
  117.5 1.8 %collective-permute-start.24 = (f32[32]{0:T(128)S(1)}, f32[32]{0:T(128)S(1)}, u32[]{:S(2)}, u32[]{:S(2)}) collective-permute-start(f32[32]{0:T(128)S(1)} %get-tuple-element.72), channel_id=1, source_target_pairs={{0,1},{1,2},{2,3},{3,0},{4,5},{5,6},{6,7},{7,4},{8,9},{9,10},{10,1... | collective-permute-start | bytes 392 | tf_op jit(solution)/shard_map/ppermute | solution.py:20
  119.3 2.1 %collective-permute-start.25 = (f32[32]{0:T(128)S(1)}, f32[32]{0:T(128)S(1)}, u32[]{:S(2)}, u32[]{:S(2)}) collective-permute-start(f32[32]{0:T(128)S(1)} %get-tuple-element.72), channel_id=1, source_target_pairs={{0,2},{1,3},{2,0},{3,1},{4,6},{5,7},{6,4},{7,5},{8,10},{9,11},{10,... | collective-permute-start | bytes 392 | tf_op jit(solution)/shard_map/ppermute | solution.py:20
  121.4 0.7 collective-permute-start.26
  122.1 0.2 collective-permute-done.24
  122.3 2.1 %collective-permute-done.25 = f32[32]{0:T(128)S(1)} collective-permute-done((f32[32]{0:T(128)S(1)}, f32[32]{0:T(128)S(1)}, u32[]{:S(2)}, u32[]{:S(2)}) %collective-permute-start.25) | collective-permute-done | bytes 160 | tf_op jit(solution)/shard_map/ppermute | solution.py:20
  124.4 0.6 collective-permute-done.26
  125.0 0.7 add_convert_fusion.1
  (79 shorter events, 0.7 us)
Async XLA Ops:
  0.6 55.8 %copy-start = (bf16[2048,64]{0,1:T(8,128)(2,1)S(1)}, bf16[2048,64]{0,1:T(8,128)(2,1)}, u32[]{:S(2)}) copy-start(bf16[2048,64]{0,1:T(8,128)(2,1)} %param.44) | copy-start | bytes 786436
  0.7 11.6 %copy-start.11 = (bf16[32,512]{1,0:T(8,128)(2,1)S(1)}, bf16[32,512]{1,0:T(8,128)(2,1)}, u32[]{:S(2)}) copy-start(bf16[32,512]{1,0:T(8,128)(2,1)} %param.52) | copy-start | bytes 98308
  0.7 11.6 %copy-start.12 = (bf16[32,512]{1,0:T(8,128)(2,1)S(1)}, bf16[32,512]{1,0:T(8,128)(2,1)}, u32[]{:S(2)}) copy-start(bf16[32,512]{1,0:T(8,128)(2,1)} %param.51) | copy-start | bytes 98308
  0.7 11.6 %copy-start.13 = (bf16[32,512]{1,0:T(8,128)(2,1)S(1)}, bf16[32,512]{1,0:T(8,128)(2,1)}, u32[]{:S(2)}) copy-start(bf16[32,512]{1,0:T(8,128)(2,1)} %param.50) | copy-start | bytes 98308
  0.7 19.0 %copy-start.7 = (bf16[32,2048]{1,0:T(8,128)(2,1)S(1)}, bf16[32,2048]{1,0:T(8,128)(2,1)}, u32[]{:S(2)}) copy-start(bf16[32,2048]{1,0:T(8,128)(2,1)} %refs_0_.1) | copy-start | bytes 393220
  0.7 19.0 %copy-start.14 = (bf16[2048]{0:T(1024)(128)(2,1)S(1)}, bf16[2048]{0:T(1024)(128)(2,1)}, u32[]{:S(2)}) copy-start(bf16[2048]{0:T(1024)(128)(2,1)} %param.41) | copy-start | bytes 12292
  0.7 19.0 %copy-start.15 = (bf16[2048]{0:T(1024)(128)(2,1)S(1)}, bf16[2048]{0:T(1024)(128)(2,1)}, u32[]{:S(2)}) copy-start(bf16[2048]{0:T(1024)(128)(2,1)} %param.42) | copy-start | bytes 12292
  0.7 19.0 %copy-start.16 = (bf16[2048]{0:T(1024)(128)(2,1)S(1)}, bf16[2048]{0:T(1024)(128)(2,1)}, u32[]{:S(2)}) copy-start(bf16[2048]{0:T(1024)(128)(2,1)} %param.49) | copy-start | bytes 12292
  0.7 19.0 %copy-start.5 = (s32[32,4]{0,1:T(4,128)S(1)}, s32[32,4]{0,1:T(4,128)}, u32[]{:S(2)}) copy-start(s32[32,4]{0,1:T(4,128)} %param.45) | copy-start | bytes 1540
  6.6 13.2 %collective-permute-start = (bf16[32,2048]{1,0:T(8,128)(2,1)}, bf16[32,2048]{1,0:T(8,128)(2,1)S(1)}, u32[]{:S(2)}, u32[]{:S(2)}) collective-permute-start(bf16[32,2048]{1,0:T(8,128)(2,1)} %get-tuple-element.21), channel_id=1, source_target_pairs={{0,1},{1,2},{2,3},{3,0},{4,5},{5,6},{6,7},{7,4},{8,9},{9,10},{10,1... | collective-permute-start | bytes 393224 | tf_op jit(solution)/shard_map/ppermute | solution.py:20
  8.1 11.7 %collective-permute-start.1 = (bf16[32,2048]{1,0:T(8,128)(2,1)}, bf16[32,2048]{1,0:T(8,128)(2,1)S(1)}, u32[]{:S(2)}, u32[]{:S(2)}) collective-permute-start(bf16[32,2048]{1,0:T(8,128)(2,1)} %get-tuple-element.21), channel_id=1, source_target_pairs={{0,2},{1,3},{2,0},{3,1},{4,6},{5,7},{6,4},{7,5},{8,10},{9,11},{10,... | collective-permute-start | bytes 393224 | tf_op jit(solution)/shard_map/ppermute | solution.py:20
  10.9 8.9 %collective-permute-start.2 = (bf16[32,2048]{1,0:T(8,128)(2,1)}, bf16[32,2048]{1,0:T(8,128)(2,1)S(1)}, u32[]{:S(2)}, u32[]{:S(2)}) collective-permute-start(bf16[32,2048]{1,0:T(8,128)(2,1)} %get-tuple-element.21), channel_id=1, source_target_pairs={{0,3},{1,0},{2,1},{3,2},{4,7},{5,4},{6,5},{7,6},{8,11},{9,8},{10,9... | collective-permute-start | bytes 393224 | tf_op jit(solution)/shard_map/ppermute | solution.py:20
  12.3 15.4 %collective-permute-start.14 = (bf16[1,3,32,512]{3,2,1,0:T(8,128)(2,1)S(1)}, bf16[1,3,32,512]{3,2,1,0:T(8,128)(2,1)S(1)}, u32[]{:S(2)}, u32[]{:S(2)}) collective-permute-start(bf16[1,3,32,512]{3,2,1,0:T(8,128)(2,1)S(1)} %maximum_bitcast_fusion.1), channel_id=1, source_target_pairs={{0,128},{32,160},{64,192},{96,224},{128,0},{160,32},{192,64},{224,... | collective-permute-start | bytes 294920 | tf_op jit(solution)/shard_map/ppermute | solution.py:47
  21.6 0.6 copy-start.3
  22.2 3.9 %collective-permute-start.3 = (bf16[32,512]{1,0:T(8,128)(2,1)S(1)}, bf16[32,512]{1,0:T(8,128)(2,1)S(1)}, u32[]{:S(2)}, u32[]{:S(2)}) collective-permute-start(bf16[32,512]{1,0:T(8,128)(2,1)S(1)} %get-tuple-element.26), channel_id=1, source_target_pairs={{0,32},{32,0},{64,96},{96,64},{128,160},{160,128},{192,224},{224,1... | collective-permute-start | bytes 98312 | tf_op jit(solution)/shard_map/ppermute | solution.py:47
  26.1 16.4 %collective-permute-start.4 = (bf16[64,512]{1,0:T(8,128)(2,1)S(1)}, bf16[64,512]{1,0:T(8,128)(2,1)S(1)}, u32[]{:S(2)}, u32[]{:S(2)}) collective-permute-start(bf16[64,512]{1,0:T(8,128)(2,1)S(1)} %get-tuple-element.59), channel_id=1, source_target_pairs={{0,8},{8,16},{16,24},{24,0},{1,9},{9,17},{17,25},{25,1},{2,10},{10... | collective-permute-start | bytes 196616 | tf_op jit(solution)/shard_map/ppermute | solution.py:20
  27.8 20.1 %collective-permute-start.15 = (bf16[2,3,32,512]{3,2,1,0:T(8,128)(2,1)S(1)}, bf16[2,3,32,512]{3,2,1,0:T(8,128)(2,1)S(1)}, u32[]{:S(2)}, u32[]{:S(2)}) collective-permute-start(bf16[2,3,32,512]{3,2,1,0:T(8,128)(2,1)S(1)} %pad_maximum_fusion.1), channel_id=1, source_target_pairs={{0,64},{32,96},{64,0},{96,32},{128,192},{160,224},{192,128},{224,1... | collective-permute-start | bytes 589832 | tf_op jit(solution)/shard_map/ppermute | solution.py:47
  29.4 36.8 %all-to-all-start = ((bf16[64,4,2048]{2,1,0:T(4,128)(2,1)}), bf16[64,4,2048]{2,1,0:T(4,128)(2,1)}, u32[]{:S(2)}, u32[]{:S(2)}) async-start(bf16[64,4,2048]{2,1,0:T(4,128)(2,1)} %get-tuple-element.23), calls=%async_computation | async-start | bytes 2097152 | tf_op jit(solution)/shard_map/all_to_all | solution.py:396
  38.3 7.6 %collective-permute-start.5 = (bf16[64,512]{1,0:T(8,128)(2,1)S(1)}, bf16[64,512]{1,0:T(8,128)(2,1)S(1)}, u32[]{:S(2)}, u32[]{:S(2)}) collective-permute-start(bf16[64,512]{1,0:T(8,128)(2,1)S(1)} %get-tuple-element.59), channel_id=1, source_target_pairs={{0,16},{8,24},{16,0},{24,8},{1,17},{9,25},{17,1},{25,9},{2,18},{10... | collective-permute-start | bytes 196616 | tf_op jit(solution)/shard_map/ppermute | solution.py:20
  41.4 6.4 %collective-permute-start.6 = (bf16[64,512]{1,0:T(8,128)(2,1)S(1)}, bf16[64,512]{1,0:T(8,128)(2,1)S(1)}, u32[]{:S(2)}, u32[]{:S(2)}) collective-permute-start(bf16[64,512]{1,0:T(8,128)(2,1)S(1)} %get-tuple-element.59), channel_id=1, source_target_pairs={{0,24},{8,0},{16,8},{24,16},{1,25},{9,1},{17,9},{25,17},{2,26},{10... | collective-permute-start | bytes 196616 | tf_op jit(solution)/shard_map/ppermute | solution.py:20
  47.7 8.3 %copy-start.18 = (bf16[2048,2]{0,1:T(2,128)(2,1)S(1)}, bf16[2048,2]{0,1:T(2,128)(2,1)}, u32[]{:S(2)}) copy-start(bf16[2048,2]{0,1:T(2,128)(2,1)} %param.43) | copy-start | bytes 24580
  47.8 1.6 %collective-permute-start.7 = (bf16[256,512]{1,0:T(8,128)(2,1)S(1)}, bf16[256,512]{1,0:T(8,128)(2,1)S(1)}, u32[]{:S(2)}, u32[]{:S(2)}) collective-permute-start(bf16[256,512]{1,0:T(8,128)(2,1)S(1)} %get-tuple-element.51), channel_id=1, source_target_pairs={{0,4},{4,0},{1,5},{5,1},{2,6},{6,2},{3,7},{7,3},{8,12},{12,8},{9,1... | collective-permute-start | bytes 786440 | tf_op jit(solution)/shard_map/ppermute | solution.py:47
  50.0 17.5 %copy-start.1 = (bf16[1,2048,256]{2,1,0:T(8,128)(2,1)S(1)}, bf16[1,2048,256]{2,1,0:T(8,128)(2,1)}, u32[]{:S(2)}) copy-start(bf16[1,2048,256]{2,1,0:T(8,128)(2,1)} %param.46) | copy-start | bytes 3145732
  50.0 17.5 %copy-start.2 = (bf16[1,2048,256]{2,1,0:T(8,128)(2,1)S(1)}, bf16[1,2048,256]{2,1,0:T(8,128)(2,1)}, u32[]{:S(2)}) copy-start(bf16[1,2048,256]{2,1,0:T(8,128)(2,1)} %param.47) | copy-start | bytes 3145732
  50.7 17.5 %collective-permute-start.16 = (bf16[2,512,128]{2,1,0:T(8,128)(2,1)}, bf16[2,512,128]{2,1,0:T(8,128)(2,1)}, u32[]{:S(2)}, u32[]{:S(2)}) collective-permute-start(bf16[2,512,128]{2,1,0:T(8,128)(2,1)} %pad_maximum_fusion), channel_id=1, source_target_pairs={{0,1},{1,2},{2,3},{3,0},{4,5},{5,6},{6,7},{7,4},{8,9},{9,10},{10,1... | collective-permute-start | bytes 786440 | tf_op jit(solution)/shard_map/ppermute | solution.py:20
  52.1 16.2 %collective-permute-start.17 = (bf16[2,512,128]{2,1,0:T(8,128)(2,1)}, bf16[2,512,128]{2,1,0:T(8,128)(2,1)}, u32[]{:S(2)}, u32[]{:S(2)}) collective-permute-start(bf16[2,512,128]{2,1,0:T(8,128)(2,1)} %pad_maximum_fusion), channel_id=1, source_target_pairs={{0,2},{1,3},{2,0},{3,1},{4,6},{5,7},{6,4},{7,5},{8,10},{9,11},{10,... | collective-permute-start | bytes 786440 | tf_op jit(solution)/shard_map/ppermute | solution.py:20
  54.5 13.8 %collective-permute-start.18 = (bf16[2,512,128]{2,1,0:T(8,128)(2,1)}, bf16[2,512,128]{2,1,0:T(8,128)(2,1)}, u32[]{:S(2)}, u32[]{:S(2)}) collective-permute-start(bf16[2,512,128]{2,1,0:T(8,128)(2,1)} %pad_maximum_fusion), channel_id=1, source_target_pairs={{0,3},{1,0},{2,1},{3,2},{4,7},{5,4},{6,5},{7,6},{8,11},{9,8},{10,9... | collective-permute-start | bytes 786440 | tf_op jit(solution)/shard_map/ppermute | solution.py:20
  67.5 2.2 %copy-start.10 = (bf16[1,4,32,512]{3,2,0,1:T(8,128)(2,1)S(1)}, bf16[1,4,32,512]{3,2,0,1:T(8,128)(2,1)}, u32[]{:S(2)}) copy-start(bf16[1,4,32,512]{3,2,0,1:T(8,128)(2,1)} %get-tuple-element.44) | copy-start | bytes 393220
  68.2 2.1 %copy-start.6 = (bf16[1,256,2048]{2,1,0:T(8,128)(2,1)S(1)}, bf16[1,256,2048]{2,1,0:T(8,128)(2,1)}, u32[]{:S(2)}) copy-start(bf16[1,256,2048]{2,1,0:T(8,128)(2,1)} %param.48) | copy-start | bytes 3145732
  70.0 6.0 %collective-permute-start.19 = (bf16[256,512]{1,0:T(8,128)(2,1)S(1)}, bf16[256,512]{1,0:T(8,128)(2,1)S(1)}, u32[]{:S(2)}, u32[]{:S(2)}) collective-permute-start(bf16[256,512]{1,0:T(8,128)(2,1)S(1)} %slice.63), channel_id=1, source_target_pairs={{0,4},{4,0},{1,5},{5,1},{2,6},{6,2},{3,7},{7,3},{8,12},{12,8},{9,1... | collective-permute-start | bytes 786440 | tf_op jit(solution)/shard_map/ppermute | solution.py:47
  70.5 34.3 %copy-start.17 = (bf16[512]{0:T(512)(128)(2,1)S(1)}, bf16[512]{0:T(512)(128)(2,1)}, u32[]{:S(2)}) copy-start(bf16[512]{0:T(512)(128)(2,1)} %param.53) | copy-start | bytes 3076
  70.5 15.5 %collective-permute-start.11 = (bf16[256,512]{1,0:T(8,128)(2,1)S(1)}, bf16[256,512]{1,0:T(8,128)(2,1)S(1)}, u32[]{:S(2)}, u32[]{:S(2)}) collective-permute-start(bf16[256,512]{1,0:T(8,128)(2,1)S(1)} %get-tuple-element.40), channel_id=1, source_target_pairs={{0,1},{1,2},{2,3},{3,0},{4,5},{5,6},{6,7},{7,4},{8,9},{9,10},{10,1... | collective-permute-start | bytes 786440 | tf_op jit(solution)/shard_map/ppermute | solution.py:20
  71.9 15.9 %collective-permute-start.12 = (bf16[256,512]{1,0:T(8,128)(2,1)S(1)}, bf16[256,512]{1,0:T(8,128)(2,1)S(1)}, u32[]{:S(2)}, u32[]{:S(2)}) collective-permute-start(bf16[256,512]{1,0:T(8,128)(2,1)S(1)} %get-tuple-element.42), channel_id=1, source_target_pairs={{0,2},{1,3},{2,0},{3,1},{4,6},{5,7},{6,4},{7,5},{8,10},{9,11},{10,... | collective-permute-start | bytes 786440 | tf_op jit(solution)/shard_map/ppermute | solution.py:20
  74.3 14.9 %collective-permute-start.13 = (bf16[256,512]{1,0:T(8,128)(2,1)S(1)}, bf16[256,512]{1,0:T(8,128)(2,1)S(1)}, u32[]{:S(2)}, u32[]{:S(2)}) collective-permute-start(bf16[256,512]{1,0:T(8,128)(2,1)S(1)} %get-tuple-element.39), channel_id=1, source_target_pairs={{0,3},{1,0},{2,1},{3,2},{4,7},{5,4},{6,5},{7,6},{8,11},{9,8},{10,9... | collective-permute-start | bytes 786440 | tf_op jit(solution)/shard_map/ppermute | solution.py:20
  75.8 14.4 %collective-permute-start.10 = (bf16[256,256]{1,0:T(8,128)(2,1)S(1)}, bf16[256,256]{1,0:T(8,128)(2,1)S(1)}, u32[]{:S(2)}, u32[]{:S(2)}) collective-permute-start(bf16[256,256]{1,0:T(8,128)(2,1)S(1)} %shard_map.274.refs_0_), channel_id=1, source_target_pairs={{0,3},{1,0},{2,1},{3,2},{4,7},{5,4},{6,5},{7,6},{8,11},{9,8},{10,9... | collective-permute-start | bytes 393224 | tf_op jit(solution)/shard_map/ppermute | solution.py:20
  76.0 14.3 %collective-permute-start.8 = (bf16[256,256]{1,0:T(8,128)(2,1)S(1)}, bf16[256,256]{1,0:T(8,128)(2,1)S(1)}, u32[]{:S(2)}, u32[]{:S(2)}) collective-permute-start(bf16[256,256]{1,0:T(8,128)(2,1)S(1)} %shard_map.274.refs_0_), channel_id=1, source_target_pairs={{0,1},{1,2},{2,3},{3,0},{4,5},{5,6},{6,7},{7,4},{8,9},{9,10},{10,1... | collective-permute-start | bytes 393224 | tf_op jit(solution)/shard_map/ppermute | solution.py:20
  86.0 6.5 %collective-permute-start.9 = (bf16[256,256]{1,0:T(8,128)(2,1)S(1)}, bf16[256,256]{1,0:T(8,128)(2,1)S(1)}, u32[]{:S(2)}, u32[]{:S(2)}) collective-permute-start(bf16[256,256]{1,0:T(8,128)(2,1)S(1)} %shard_map.274.refs_0_), channel_id=1, source_target_pairs={{0,2},{1,3},{2,0},{3,1},{4,6},{5,7},{6,4},{7,5},{8,10},{9,11},{10,... | collective-permute-start | bytes 393224 | tf_op jit(solution)/shard_map/ppermute | solution.py:20
  87.8 29.2 %copy-start.9 = (bf16[256,32]{1,0:T(8,128)(2,1)S(1)}, bf16[256,32]{1,0:T(8,128)(2,1)}, u32[]{:S(2)}) copy-start(bf16[256,32]{1,0:T(8,128)(2,1)} %get-tuple-element.30) | copy-start | bytes 49156
  87.8 16.9 %collective-permute-start.20 = (bf16[4,32,512]{2,1,0:T(8,128)(2,1)S(1)}, bf16[4,32,512]{2,1,0:T(8,128)(2,1)S(1)}, u32[]{:S(2)}, u32[]{:S(2)}) collective-permute-start(bf16[4,32,512]{2,1,0:T(8,128)(2,1)S(1)} %slice_bitcast_fusion), channel_id=1, source_target_pairs={{0,32},{32,0},{64,96},{96,64},{128,160},{160,128},{192,224},{224,1... | collective-permute-start | bytes 393224 | tf_op jit(solution)/shard_map/ppermute | solution.py:47
  92.5 24.7 %copy-start.8 = (bf16[256,32]{1,0:T(8,128)(2,1)S(1)}, bf16[256,32]{1,0:T(8,128)(2,1)}, u32[]{:S(2)}) copy-start(bf16[256,32]{1,0:T(8,128)(2,1)} %get-tuple-element.28) | copy-start | bytes 49156
  92.5 32.5 %copy-start.4 = (bf16[32,512]{1,0:T(8,128)(2,1)S(1)}, bf16[32,512]{1,0:T(8,128)(2,1)}, u32[]{:S(2)}) copy-start(bf16[32,512]{1,0:T(8,128)(2,1)} %copy-done.3) | copy-start | bytes 98308
  93.7 23.2 %all-to-all-start.1 = ((bf16[64,4,512]{2,1,0:T(4,128)(2,1)}), bf16[64,4,512]{2,1,0:T(4,128)(2,1)S(1)}, u32[]{:S(2)}, u32[]{:S(2)}) async-start(bf16[64,4,512]{2,1,0:T(4,128)(2,1)} %reshape.49), calls=%async_computation.1 | async-start | bytes 524288 | tf_op jit(solution)/shard_map/all_to_all | solution.py:463
  104.8 12.4 %collective-permute-start.21 = (bf16[32,512]{1,0:T(8,128)(2,1)S(1)}, bf16[32,512]{1,0:T(8,128)(2,1)S(1)}, u32[]{:S(2)}, u32[]{:S(2)}) collective-permute-start(bf16[32,512]{1,0:T(8,128)(2,1)S(1)} %get-tuple-element.48), channel_id=1, source_target_pairs={{0,24},{8,0},{16,8},{24,16},{1,25},{9,1},{17,9},{25,17},{2,26},{10... | collective-permute-start | bytes 98312 | tf_op jit(solution)/shard_map/ppermute | solution.py:20
  107.6 9.6 %collective-permute-start.22 = (bf16[32,512]{1,0:T(8,128)(2,1)S(1)}, bf16[32,512]{1,0:T(8,128)(2,1)S(1)}, u32[]{:S(2)}, u32[]{:S(2)}) collective-permute-start(bf16[32,512]{1,0:T(8,128)(2,1)S(1)} %get-tuple-element.50), channel_id=1, source_target_pairs={{0,16},{8,24},{16,0},{24,8},{1,17},{9,25},{17,1},{25,9},{2,18},{10... | collective-permute-start | bytes 98312 | tf_op jit(solution)/shard_map/ppermute | solution.py:20
  108.4 8.8 %collective-permute-start.23 = (bf16[32,512]{1,0:T(8,128)(2,1)S(1)}, bf16[32,512]{1,0:T(8,128)(2,1)S(1)}, u32[]{:S(2)}, u32[]{:S(2)}) collective-permute-start(bf16[32,512]{1,0:T(8,128)(2,1)S(1)} %get-tuple-element.49), channel_id=1, source_target_pairs={{0,8},{8,16},{16,24},{24,0},{1,9},{9,17},{17,25},{25,1},{2,10},{10... | collective-permute-start | bytes 98312 | tf_op jit(solution)/shard_map/ppermute | solution.py:20
  117.5 4.9 %collective-permute-start.24 = (f32[32]{0:T(128)S(1)}, f32[32]{0:T(128)S(1)}, u32[]{:S(2)}, u32[]{:S(2)}) collective-permute-start(f32[32]{0:T(128)S(1)} %get-tuple-element.72), channel_id=1, source_target_pairs={{0,1},{1,2},{2,3},{3,0},{4,5},{5,6},{6,7},{7,4},{8,9},{9,10},{10,1... | collective-permute-start | bytes 392 | tf_op jit(solution)/shard_map/ppermute | solution.py:20
  119.3 5.1 %collective-permute-start.25 = (f32[32]{0:T(128)S(1)}, f32[32]{0:T(128)S(1)}, u32[]{:S(2)}, u32[]{:S(2)}) collective-permute-start(f32[32]{0:T(128)S(1)} %get-tuple-element.72), channel_id=1, source_target_pairs={{0,2},{1,3},{2,0},{3,1},{4,6},{5,7},{6,4},{7,5},{8,10},{9,11},{10,... | collective-permute-start | bytes 392 | tf_op jit(solution)/shard_map/ppermute | solution.py:20
  121.4 3.6 %collective-permute-start.26 = (f32[32]{0:T(128)S(1)}, f32[32]{0:T(128)S(1)}, u32[]{:S(2)}, u32[]{:S(2)}) collective-permute-start(f32[32]{0:T(128)S(1)} %get-tuple-element.72), channel_id=1, source_target_pairs={{0,3},{1,0},{2,1},{3,2},{4,7},{5,4},{6,5},{7,6},{8,11},{9,8},{10,9... | collective-permute-start | bytes 392 | tf_op jit(solution)/shard_map/ppermute | solution.py:20

commit v3 on v2

--- a/solution.py
+++ b/solution.py
@@ -13,6 +13,7 @@
 norm_eps = 1e-06
 FEEDER_VMEM = 16 * 2**20
 STATE_CHUNKS = 4
+ROW_CHUNKS = 4
 
 
 def from_shift(array, axis, shift):
@@ -244,17 +245,55 @@
     )(place, *arrays)
 
 
-def expert_in_kernel(rows, gate, up, hidden):
-    gate_value = dot32(rows[...], gate[...])
-    hidden[...] = (silu(gate_value) * dot32(rows[...], up[...])).astype(jnp.bfloat16)
+def joined_halves(first, second):
+    pairs = first.shape[0] // 16
+    first = first.reshape(pairs, 2, 8, first.shape[1])
+    second = second.reshape(pairs, 2, 8, second.shape[1])
+    upper = first[:, 0] + pltpu.roll(second[:, 0], 4, 1)
+    lower = pltpu.roll(first[:, 1], 4, 1) + second[:, 1]
+    places = lax.broadcasted_iota(jnp.int32, upper.shape, 1)
+    return jnp.where(places < 4, upper, lower).reshape(pairs * 8, upper.shape[2])
+
+
+def expert_in_kernel(*refs):
+    rows, gate, up, *downs, hidden, down, sems = refs
+    copies = [
+        pltpu.make_async_copy(part, down.at[k], sems.at[k]) for k, part in enumerate(downs)
+    ]
+    for copy in copies:
+        copy.start()
+    half = gate.shape[0] // 2
+    gate_value, up_value = [
+        joined_halves(dot32(rows[...], w[:half]), dot32(rows[...], w[half:])) for w in (gate, up)
+    ]
+    hidden[...] = (silu(gate_value) * up_value).astype(jnp.bfloat16)
+    for copy in copies:
+        copy.wait()
+
+
+def expert_in(rows, gate, up, *downs):
+    vmem = pl.BlockSpec(memory_space=pltpu.VMEM)
+    hbm = pl.BlockSpec(memory_space=pltpu.HBM)
+    return pl.pallas_call(
+        expert_in_kernel,
+        name="expert_in",
+        in_specs=[vmem] * 3 + [hbm] * len(downs),
+        out_specs=[vmem] * 2,
+        compiler_params=pltpu.CompilerParams(vmem_limit_bytes=FEEDER_VMEM),
+        scratch_shapes=[pltpu.SemaphoreType.DMA((len(downs),))],
+        out_shape=[
+            jax.ShapeDtypeStruct((rows.shape[0] // 2, gate.shape[1]), jnp.bfloat16),
+            jax.ShapeDtypeStruct((len(downs), *downs[0].shape), jnp.bfloat16),
+        ],
+    )(rows, gate, up, *downs)
 
 
 def expert_out_kernel(*refs):
-    half = len(refs) // 2
-    total = dot32(refs[0][...], refs[half][...])
-    for k in range(1, half):
-        total = total + dot32(refs[k][...], refs[half + k][...])
-    refs[-1][...] = total.astype(jnp.bfloat16)
+    *parts, down, out = refs
+    total = dot32(parts[0][...], down[0])
+    for k in range(1, len(parts)):
+        total = total + dot32(parts[k][...], down[k])
+    out[...] = total.astype(jnp.bfloat16)
 
 
 def simple_call(kernel, shape, *arrays):
@@ -268,57 +307,91 @@
     )(*arrays)
 
 
+def slots_kernel(routes, in_slot, in_half_slot):
+    for out, halves in ((in_slot, 1), (in_half_slot, 2)):
+        _, columns = out.shape
+        seqs = columns // halves
+        slot_ids = lax.broadcasted_iota(jnp.int32, out.shape, 0)
+        token_ids = lax.broadcasted_iota(jnp.int32, out.shape, 1)
+        picked = jnp.zeros(out.shape, jnp.bool_)
+        for k in range(routes.shape[0]):
+            picked = picked | ((slot_ids >> (1 + halves)) == routes[k : k + 1, :columns])
+        before = lax.broadcasted_iota(jnp.int32, (columns, columns), 0)
+        after = lax.broadcasted_iota(jnp.int32, (columns, columns), 1)
+        earlier = (before < after) & ((before >= seqs) == (after >= seqs))
+        rank = dot32(
+            jnp.where(picked, 1.0, 0.0).astype(jnp.bfloat16),
+            jnp.where(earlier, 1.0, 0.0).astype(jnp.bfloat16),
+        )
+        here = picked & (rank.astype(jnp.int32) == (slot_ids & 3))
+        if halves == 2:
+            here = here & (((slot_ids & 4) != 0) == (token_ids >= seqs))
+        out[...] = jnp.where(here, 1.0, 0.0).astype(out.dtype)
+
+
+def slots_of(slots, routes):
+    seqs = routes.shape[1] // 2
+    vmem = pl.BlockSpec(memory_space=pltpu.VMEM)
+    return pl.pallas_call(
+        slots_kernel,
+        name="slots",
+        in_specs=[vmem],
+        out_specs=[vmem] * 2,
+        compiler_params=pltpu.CompilerParams(vmem_limit_bytes=FEEDER_VMEM),
+        out_shape=[
+            jax.ShapeDtypeStruct((slots, seqs), jnp.float32),
+            jax.ShapeDtypeStruct((2 * slots, 2 * seqs), jnp.bfloat16),
+        ],
+    )(routes)
+
+
 def feeder_kernel(
-    place, part_0, part_1, part_2, part_3, resid, post_gain, ffn_gain, routes,
-    stream_quarter, feed, feed_quarter, outgoing, in_slot,
+    place, part_0, part_1, part_2, part_3, resid, post_gain, ffn_gain, in_half_slot,
+    kept_out, feed_quarter, rows_out, kept, rows, sems,
 ):
-    slots, seqs = in_slot.shape
-    slot_ids = lax.broadcasted_iota(jnp.int32, (slots, seqs), 0)
-    picked = jnp.zeros((slots, seqs), jnp.bool_)
-    for k in range(routes.shape[0]):
-        picked = picked | ((slot_ids >> 2) == routes[k : k + 1])
-    earlier = lax.broadcasted_iota(jnp.int32, (seqs, seqs), 0) < lax.broadcasted_iota(
-        jnp.int32, (seqs, seqs), 1
-    )
-    rank = dot32(
-        jnp.where(picked, 1.0, 0.0).astype(jnp.bfloat16),
-        jnp.where(earlier, 1.0, 0.0).astype(jnp.bfloat16),
-    )
-    placed = jnp.where(picked & (rank.astype(jnp.int32) == (slot_ids & 3)), 1.0, 0.0)
-    in_slot[...] = placed
     mixed = sum_of([part_0[...], part_1[...], part_2[...], part_3[...]])
     total = resid[...].astype(jnp.float32) + scaled_rows(mixed, post_gain[...])
     total = total.astype(jnp.bfloat16)
     fed = scaled_rows(total, ffn_gain[...]).astype(jnp.bfloat16)
-    feed[...] = fed
-    quarter = feed_quarter.shape[1]
-    for q in range(feed.shape[1] // quarter):
+    width, quarter = fed.shape[1], feed_quarter.shape[1]
+    kept[:, :width] = fed
+    for q in range(width // quarter):
 
         @pl.when(place[0] == q)
         def _(q=q):
-            stream_quarter[...] = total[:, q * quarter : (q + 1) * quarter]
+            kept[:, width:] = total[:, q * quarter : (q + 1) * quarter]
             feed_quarter[...] = fed[:, q * quarter : (q + 1) * quarter]
 
-    outgoing[...] = dot32(placed.astype(jnp.bfloat16), fed).reshape(outgoing.shape).astype(jnp.bfloat16)
-
-
-def feeder(slots, quarter, place, *arrays):
+    half = fed.shape[1] // 2
+    halves = jnp.concatenate([fed[:, :half], fed[:, half:]], axis=0)
+    some = rows.shape[0] // ROW_CHUNKS
+    copies = []
+    for i in range(ROW_CHUNKS):
+        chunk = pl.ds(i * some, some)
+        rows[chunk] = dot32(in_half_slot[chunk], halves).astype(jnp.bfloat16)
+        copies.append(pltpu.make_async_copy(rows.at[chunk], rows_out.at[chunk], sems.at[i]))
+        copies[-1].start()
+    copies.append(pltpu.make_async_copy(kept, kept_out, sems.at[ROW_CHUNKS]))
+    copies[-1].start()
+    for copy in copies:
+        copy.wait()
+
+
+def feeder(quarter, place, *arrays):
     vmem = pl.BlockSpec(memory_space=pltpu.VMEM)
-    rows = jax.ShapeDtypeStruct(arrays[0].shape, jnp.bfloat16)
-    share = jax.ShapeDtypeStruct((arrays[0].shape[0], quarter), jnp.bfloat16)
+    hbm = pl.BlockSpec(memory_space=pltpu.HBM)
+    shape = arrays[1].shape
+    share, kept = (shape[0], quarter), (shape[0], shape[1] + quarter)
+    rows = (arrays[-1].shape[0], shape[1] // 2)
     return pl.pallas_call(
         feeder_kernel,
         name="feeder",
         in_specs=[pl.BlockSpec(memory_space=pltpu.SMEM)] + [vmem] * len(arrays),
-        out_specs=[vmem] * 5,
+        out_specs=[hbm, vmem, hbm],
         compiler_params=pltpu.CompilerParams(vmem_limit_bytes=FEEDER_VMEM),
-        out_shape=[
-            share,
-            rows,
-            share,
-            jax.ShapeDtypeStruct((slots // 4, 4, arrays[0].shape[1]), jnp.bfloat16),
-            jax.ShapeDtypeStruct((slots, arrays[0].shape[0]), jnp.float32),
-        ],
+        scratch_shapes=[pltpu.VMEM(x, jnp.bfloat16) for x in (kept, rows)]
+        + [pltpu.SemaphoreType.DMA((ROW_CHUNKS + 1,))],
+        out_shape=[jax.ShapeDtypeStruct(x, jnp.bfloat16) for x in (kept, share, rows)],
     )(place, *arrays)
 
 
@@ -388,21 +461,26 @@
     new_conv = new_conv.transpose(2, 0, 1, 3)
     mixed_parts = from_all(part, "tp")
     mixed_parts[0] = part.astype(jnp.float32)
-    stream_quarter, feed, feed_quarter, outgoing, in_slot = feeder(
-        expert_count * capacity, quarter, place, *mixed_parts, resid.astype(jnp.float32),
-        post_gain[None], ffn_gain[None], route_experts.T,
+    in_slot, in_half_slot = slots_of(
+        expert_count * capacity, jnp.tile(route_experts.T, (1, 2))
+    )
+    kept, feed_quarter, outgoing = feeder(
+        quarter, place, *mixed_parts, resid.astype(jnp.float32), post_gain[None],
+        ffn_gain[None], in_half_slot,
     )
 
     arrived = lax.all_to_all(
-        outgoing, EP, 0, 0, tiled=True
-    )
-    rows = arrived.reshape(expert_count * capacity, width)
-
-    tokens = jnp.concatenate([feed_quarter, from_flip(feed_quarter, "ep_0", 1)], axis=0)
+        outgoing.reshape(expert_count, 2 * capacity, width // 2), EP, 0, 0, tiled=True
+    )
+    rows = arrived.reshape(2 * expert_count * capacity, width // 2)
+
+    tokens = lax.optimization_barrier((feed_quarter, from_flip(feed_quarter, "ep_0", 1)))
+    tokens = jnp.concatenate(tokens, axis=0)
     tokens = jnp.concatenate(from_all(tokens, "ep_1"), axis=0)
     tokens = jnp.concatenate([tokens, from_flip(tokens, "ep_2", 1)], axis=0)
-    feed, tokens = lax.optimization_barrier((feed, tokens))
-    gate_rows, up_rows, down_rows = unit_rows
+    kept, tokens = lax.optimization_barrier((kept, tokens))
+    feed, stream_quarter = kept[:, :width], kept[:, width:]
+    down_rows = unit_rows[2]
     down = expert_down[0]
     down_parts = [
         lax.dynamic_slice_in_dim(down, ((tp_index + s) % tp_count) * quarter, quarter, 1)
@@ -410,9 +488,9 @@
     ]
     down_parts = [down_parts[0]] + [from_shift(down_parts[s], "tp", s) for s in range(1, tp_count)]
     across = (((1,), (1,)), ((), ()))
-    gate_piece = lax.dot_general(tokens, gate_rows, across, preferred_element_type=jnp.float32)
-    up_piece = lax.dot_general(tokens, up_rows, across, preferred_element_type=jnp.float32)
-    pieces = jnp.stack([gate_piece, up_piece]).astype(jnp.bfloat16)
+    pieces = lax.dot_general(
+        tokens, unit_rows[:2].reshape(-1, quarter), across, preferred_element_type=jnp.float32
+    ).astype(jnp.bfloat16)
     sums = from_all(pieces, "tp")
 
     features = (((0,), (1,)), ((), ()))
@@ -436,18 +514,19 @@
     weight_high = slot_weight.astype(jnp.bfloat16)
     weight_low = (slot_weight - weight_high.astype(jnp.float32)).astype(jnp.bfloat16)
     switch = jax.nn.sigmoid(dot32(feed, dense_switch))
-    rows, weight_high, weight_low, switch = lax.optimization_barrier(
-        (rows, weight_high, weight_low, switch)
-    )
-
-    hidden = simple_call(
-        expert_in_kernel, (rows.shape[0], expert_gate.shape[2]),
-        rows, expert_gate[0], expert_up[0],
-    )
+    stream_share = stream_quarter.astype(jnp.float32)
+    rows, weight_high, weight_low, switch, stream_share, *down_parts = (
+        lax.optimization_barrier(
+            (rows, weight_high, weight_low, switch, stream_share, *down_parts)
+        )
+    )
+
+    hidden, down_rows_here = expert_in(rows, expert_gate[0], expert_up[0], *down_parts)
     _, *sums = lax.optimization_barrier((hidden, *sums))
     hidden_parts = from_all(hidden, "tp")
     sums = sum_of(sums)
-    dense_hidden = (jax.nn.silu(sums[0]) * sums[1]).astype(jnp.bfloat16)
+    gate_sum, up_sum = jnp.split(sums, 2, axis=1)
+    dense_hidden = (jax.nn.silu(gate_sum) * up_sum).astype(jnp.bfloat16)
     dense_part = dot32(dense_hidden, down_rows).astype(jnp.bfloat16)
     half = dense_part.shape[0] // 2
     lots = sum_of([dense_part[:half], from_flip(dense_part[half:], "ep_2", 1)])
@@ -459,7 +538,9 @@
     )
     dense_out = dense_part
 
-    served = simple_call(expert_out_kernel, (rows.shape[0], quarter), *hidden_parts, *down_parts)
+    served = simple_call(
+        expert_out_kernel, (rows.shape[0] // 2, quarter), *hidden_parts, down_rows_here
+    )
     returned = lax.all_to_all(
         served.reshape(expert_count, capacity, quarter), EP, 0, 0, tiled=True
     ).reshape(expert_count * capacity, quarter)
@@ -473,7 +554,7 @@
     squares = jnp.sum(combined * combined, axis=1)
     total_square = sum_of(from_all(squares, "tp"))
     scale = lax.rsqrt(total_square / width + norm_eps)
-    layer_out = (stream_quarter.astype(jnp.float32) + combined * scale[:, None] * out_gain.astype(jnp.float32)).astype(
+    layer_out = (stream_share + combined * scale[:, None] * out_gain.astype(jnp.float32)).astype(
         jnp.bfloat16
     )
     return (layer_out, new_state, new_conv)

time: 127 us -> 127 us (level)
  waiting for transfers between devices: 39.3 us -> 27.8 us
  local copies, waits for them, and re-layouts: 3.9 us -> 9.29 us
  starting transfers between devices: 65.8 us -> 67.9 us
  matrix products: 1.98 us -> 3.97 us
  other arithmetic: 4.73 us -> 6.07 us
    all_to_all x1, waiting for transfers between devices: 8.52 us -> 0.02 us  [on_device(): lax.all_to_all(outgoing.reshape(expert_count, 2 * capacity, width // 2),...]
    unnamed x43 -> x47, local copies, waits for them, and re-layouts: 0.74 us -> 4.57 us
    ppermute x6, waiting for transfers between devices: 3.69 us -> 0.02 us  [from_flip(): return lax.ppermute(array, axis, [(i, i ^ bit) for i in range(count)])]
    pallas_call x0 -> x2, Pallas kernels: none -> 1.68 us  [the longest x1 1.37 us: expert_in(): pl.pallas_call(expert_in_kernel, name='expert_in', in_specs=[vmem] * 3 +...]
    all_to_all x1, starting transfers between devices: 8.95 us -> 10.5 us  [on_device(): lax.all_to_all(outgoing.reshape(expert_count, 2 * capacity, width // 2),...]
    dot_general x2 -> x1, matrix products: 0.58 us -> 2.07 us  [on_device(): lax.dot_general(tokens, unit_rows[:2].reshape(-1, quarter), across, prefe...]
    reshape x1 -> x0, local copies, waits for them, and re-layouts: 1.33 us -> none  [on_device(): rows = arrived.reshape(expert_count * capacity, width)]
  transfers between devices with their start and end apart: 29 -> 29, of which waited for: 12 -> 10; matrix products, arithmetic and copies ran while one was open for 6% -> 12% of each run, Pallas kernels for 2% -> 3%
where the time goes in v3:
time: 127 us; the launch traced here: 126 us
  starting transfers between devices  67.9 us (53%)
  waiting for transfers between devices  27.8 us (22%)
  Pallas kernels  9.53 us (8%)
  local copies, waits for them, and re-layouts  9.29 us (7%)
  other arithmetic  6.07 us (5%)
  matrix products  3.97 us (3%)
    ppermute x21, starting transfers between devices, from_shift(): lax.ppermute(array, axis, [(i, (i + shift) % count) for i in range(count)])  35.4 us
    ppermute x21, waiting for transfers between devices, from_shift(): lax.ppermute(array, axis, [(i, (i + shift) % count) for i in range(count)])  20.1 us
    all_to_all x1, starting transfers between devices, on_device(): lax.all_to_all(served.reshape(expert_count, capacity, quarter), EP, 0, 0,...  11.5 us
    all_to_all x1, starting transfers between devices, on_device(): lax.all_to_all(outgoing.reshape(expert_count, 2 * capacity, width // 2),...  10.5 us
    ppermute x6, starting transfers between devices, from_flip(): return lax.ppermute(array, axis, [(i, i ^ bit) for i in range(count)])  10.5 us
    all_to_all x1, waiting for transfers between devices, on_device(): lax.all_to_all(served.reshape(expert_count, capacity, quarter), EP, 0, 0,...  7.65 us
    pallas_call x1, Pallas kernels, mixer(): pl.pallas_call(mixer_kernel, name='mixer', in_specs=[pl.BlockSpec(memory_...  5.81 us
    unnamed x47, local copies, waits for them, and re-layouts  4.57 us
  transfers between devices with their start and end apart: 29, of which 10 were waited for; matrix products, arithmetic and copies ran while one was open for 12% of the time, Pallas kernels for 3%

profile of v3, /device:TPU:32, one launch (start us, length us, event | category | flops | bytes accessed | tf_op | source)
XLA Modules:
  0.0 125.7 jit_solution(11195909650013450443)
XLA Ops:
  0.7 5.8 %mixer.1 = (bf16[32,2048]{1,0:T(8,128)(2,1)}, f32[32,2,64,128]{3,2,1,0:T(8,128)}, bf16[3,3,32,128]{3,2,1,0:T(8,128)(2,1)}) custom-call(s32[1]{0:T(128)} %bitcast.place, bf16[32,2048]{1,0:T(8,128)(2,1)} %refs_0_.1, bf16[16,128]{1,0:T(8,128)(2,1)} %bitcast.105, bf16[2048,128]{1,0:T(8,128)(2,1)} %refs_2_.1, bf16[2048,128]{1,0:T(8,128)(2,1)} %refs_3_.1, ...), custom_call_target="tpu_custom_call" | custom-call | tf_op jit(solution)/shard_map/mixer/pallas_call | solution.py:226
  6.5 1.6 %collective-permute-start = (bf16[32,2048]{1,0:T(8,128)(2,1)}, bf16[32,2048]{1,0:T(8,128)(2,1)S(1)}, u32[]{:S(2)}, u32[]{:S(2)}) collective-permute-start(bf16[32,2048]{1,0:T(8,128)(2,1)} %get-tuple-element.30), channel_id=1, source_target_pairs={{0,1},{1,2},{2,3},{3,0},{4,5},{5,6},{6,7},{7,4},{8,9},{9,10},{10,1... | collective-permute-start | bytes 393224 | tf_op jit(solution)/shard_map/ppermute | solution.py:21
  8.1 2.7 %collective-permute-start.1 = (bf16[32,2048]{1,0:T(8,128)(2,1)}, bf16[32,2048]{1,0:T(8,128)(2,1)S(1)}, u32[]{:S(2)}, u32[]{:S(2)}) collective-permute-start(bf16[32,2048]{1,0:T(8,128)(2,1)} %get-tuple-element.30), channel_id=1, source_target_pairs={{0,2},{1,3},{2,0},{3,1},{4,6},{5,7},{6,4},{7,5},{8,10},{9,11},{10,... | collective-permute-start | bytes 393224 | tf_op jit(solution)/shard_map/ppermute | solution.py:21
  10.8 1.4 %collective-permute-start.2 = (bf16[32,2048]{1,0:T(8,128)(2,1)}, bf16[32,2048]{1,0:T(8,128)(2,1)S(1)}, u32[]{:S(2)}, u32[]{:S(2)}) collective-permute-start(bf16[32,2048]{1,0:T(8,128)(2,1)} %get-tuple-element.30), channel_id=1, source_target_pairs={{0,3},{1,0},{2,1},{3,2},{4,7},{5,4},{6,5},{7,6},{8,11},{9,8},{10,9... | collective-permute-start | bytes 393224 | tf_op jit(solution)/shard_map/ppermute | solution.py:21
  12.3 0.9 dynamic-slice_bitcast_fusion
  13.2 2.0 %collective-permute-start.8 = (bf16[256,512]{1,0:T(8,128)(2,1)}, bf16[256,512]{1,0:T(8,128)(2,1)S(1)}, u32[]{:S(2)}, u32[]{:S(2)}) collective-permute-start(bf16[256,512]{1,0:T(8,128)(2,1)} %get-tuple-element.58), channel_id=1, source_target_pairs={{0,1},{1,2},{2,3},{3,0},{4,5},{5,6},{6,7},{7,4},{8,9},{9,10},{10,1... | collective-permute-start | bytes 786440 | tf_op jit(solution)/shard_map/ppermute | solution.py:21
  15.4 0.3 slots.1
  15.7 0.7 collective-permute-start.9
  16.5 1.7 %collective-permute-done.1.part_2 = bf16[32,2048]{1,0:T(8,128)(2,1)S(1)} collective-permute-done((bf16[32,2048]{1,0:T(8,128)(2,1)}, bf16[32,2048]{1,0:T(8,128)(2,1)S(1)}, u32[]{:S(2)}, u32[]{:S(2)}) %collective-permute-start.1) | collective-permute-done | bytes 131104 | tf_op jit(solution)/shard_map/ppermute | solution.py:21
  18.2 1.6 %feeder.1 = (bf16[32,2560]{1,0:T(8,128)(2,1)S(1)}, bf16[32,512]{1,0:T(8,128)(2,1)S(1)}, bf16[512,1024]{1,0:T(8,128)(2,1)}) custom-call(s32[1]{0:T(128)} %bitcast.place, f32[32,2048]{1,0:T(8,128)S(1)} %convert_element_type.81.part_0, bf16[32,2048]{1,0:T(8,128)(2,1)S(1)} %collective-permute-done.part_1, bf16[32,2048]{1,0:T(8,128)(2,1)S(1)} %collective-permute-done.1.part_2, ...), custom_call_target="tpu_custom_call" | custom-call | tf_op jit(solution)/shard_map/feeder/pallas_call | solution.py:386
  19.8 1.3 %collective-permute-start.3 = (bf16[32,512]{1,0:T(8,128)(2,1)S(1)}, bf16[32,512]{1,0:T(8,128)(2,1)S(1)}, u32[]{:S(2)}, u32[]{:S(2)}) collective-permute-start(bf16[32,512]{1,0:T(8,128)(2,1)S(1)} %get-tuple-element.36), channel_id=1, source_target_pairs={{0,32},{32,0},{64,96},{96,64},{128,160},{160,128},{192,224},{224,1... | collective-permute-start | bytes 98312 | tf_op jit(solution)/shard_map/ppermute | solution.py:48
  21.1 0.8 maximum_bitcast_fusion.1
  21.9 6.2 %collective-permute-start.14 = (bf16[1,3,32,512]{3,2,0,1:T(8,128)(2,1)S(1)}, bf16[1,3,32,512]{3,2,0,1:T(8,128)(2,1)S(1)}, u32[]{:S(2)}, u32[]{:S(2)}) collective-permute-start(bf16[1,3,32,512]{3,2,0,1:T(8,128)(2,1)S(1)} %maximum_bitcast_fusion.1), channel_id=1, source_target_pairs={{0,128},{32,160},{64,192},{96,224},{128,0},{160,32},{192,64},{224,... | collective-permute-start | bytes 294920 | tf_op jit(solution)/shard_map/ppermute | solution.py:48
  28.1 0.6 constant_dynamic-update-slice_fusion.6
  28.7 0.6 constant_dynamic-update-slice_fusion.5
  29.4 1.6 %collective-permute-start.4 = (bf16[64,512]{1,0:T(8,128)(2,1)S(1)}, bf16[64,512]{1,0:T(8,128)(2,1)S(1)}, u32[]{:S(2)}, u32[]{:S(2)}) collective-permute-start(bf16[64,512]{1,0:T(8,128)(2,1)S(1)} %get-tuple-element.74), channel_id=1, source_target_pairs={{0,8},{8,16},{16,24},{24,0},{1,9},{9,17},{17,25},{25,1},{2,10},{10... | collective-permute-start | bytes 196616 | tf_op jit(solution)/shard_map/ppermute | solution.py:21
  30.9 0.7 pad_maximum_fusion
  31.6 2.8 %collective-permute-start.15 = (bf16[2,3,32,512]{3,2,0,1:T(8,128)(2,1)}, bf16[2,3,32,512]{3,2,0,1:T(8,128)(2,1)}, u32[]{:S(2)}, u32[]{:S(2)}) collective-permute-start(bf16[2,3,32,512]{3,2,0,1:T(8,128)(2,1)} %pad_maximum_fusion), channel_id=1, source_target_pairs={{0,64},{32,96},{64,0},{96,32},{128,192},{160,224},{192,128},{224,1... | collective-permute-start | bytes 589832 | tf_op jit(solution)/shard_map/ppermute | solution.py:48
  34.5 10.5 %all-to-all-start = ((bf16[64,8,1024]{2,1,0:T(8,128)(2,1)}), bf16[64,8,1024]{2,1,0:T(8,128)(2,1)S(1)}, u32[]{:S(2)}, u32[]{:S(2)}) async-start(bf16[64,8,1024]{2,1,0:T(8,128)(2,1)} %bitcast.6), calls=%async_computation | async-start | bytes 2097152 | tf_op jit(solution)/shard_map/all_to_all | solution.py:472
  45.0 3.1 %collective-permute-start.5 = (bf16[64,512]{1,0:T(8,128)(2,1)}, bf16[64,512]{1,0:T(8,128)(2,1)S(1)}, u32[]{:S(2)}, u32[]{:S(2)}) collective-permute-start(bf16[64,512]{1,0:T(8,128)(2,1)} %copy-done.13), channel_id=1, source_target_pairs={{0,16},{8,24},{16,0},{24,8},{1,17},{9,25},{17,1},{25,9},{2,18},{10... | collective-permute-start | bytes 196616 | tf_op jit(solution)/shard_map/ppermute | solution.py:21
  48.1 0.6 constant_dynamic-update-slice_fusion.4
  48.7 4.1 %collective-permute-done.5 = bf16[64,512]{1,0:T(8,128)(2,1)S(1)} collective-permute-done((bf16[64,512]{1,0:T(8,128)(2,1)}, bf16[64,512]{1,0:T(8,128)(2,1)S(1)}, u32[]{:S(2)}, u32[]{:S(2)}) %collective-permute-start.5) | collective-permute-done | bytes 65568 | tf_op jit(solution)/shard_map/ppermute | solution.py:21
  52.8 2.2 %collective-permute-start.6 = (bf16[64,512]{1,0:T(8,128)(2,1)}, bf16[64,512]{1,0:T(8,128)(2,1)S(1)}, u32[]{:S(2)}, u32[]{:S(2)}) collective-permute-start(bf16[64,512]{1,0:T(8,128)(2,1)} %copy-done.13), channel_id=1, source_target_pairs={{0,24},{8,0},{16,8},{24,16},{1,25},{9,1},{17,9},{25,17},{2,26},{10... | collective-permute-start | bytes 196616 | tf_op jit(solution)/shard_map/ppermute | solution.py:21
  55.0 0.6 constant_dynamic-update-slice_fusion.3
  55.6 2.6 %collective-permute-done.6 = bf16[64,512]{1,0:T(8,128)(2,1)S(1)} collective-permute-done((bf16[64,512]{1,0:T(8,128)(2,1)}, bf16[64,512]{1,0:T(8,128)(2,1)S(1)}, u32[]{:S(2)}, u32[]{:S(2)}) %collective-permute-start.6) | collective-permute-done | bytes 65568 | tf_op jit(solution)/shard_map/ppermute | solution.py:21
  58.2 0.6 constant_dynamic-update-slice_fusion.2
  58.9 0.7 copy-done.7
  59.7 1.0 maximum_bitcast_fusion
  60.7 0.7 constant_dynamic-update-slice_fusion.7
  61.4 2.1 %convolution_convert_fusion.1 = bf16[512,256]{1,0:T(8,128)(2,1)} fusion(bf16[512,512]{1,0:T(8,128)(2,1)} %constant_dynamic-update-slice_fusion.7, bf16[256,512]{1,0:T(8,128)(2,1)S(1)} %bitcast.96), kind=kOutput, calls=%fused_computation.1 | convolution fusion | flops 134348800 | bytes 1048576 | tf_op jit(solution)/shard_map/dot_general | solution.py:491
  63.5 0.9 collective-permute-start.16
  64.4 2.4 %collective-permute-start.17 = (bf16[512,256]{1,0:T(8,128)(2,1)}, bf16[512,256]{1,0:T(8,128)(2,1)}, u32[]{:S(2)}, u32[]{:S(2)}) collective-permute-start(bf16[512,256]{1,0:T(8,128)(2,1)} %convolution_convert_fusion.1), channel_id=1, source_target_pairs={{0,2},{1,3},{2,0},{3,1},{4,6},{5,7},{6,4},{7,5},{8,10},{9,11},{10,... | collective-permute-start | bytes 786440 | tf_op jit(solution)/shard_map/ppermute | solution.py:21
  66.8 0.6 slice_convert_fusion
  67.4 0.7 fusion.6
  68.3 0.3 fusion.24
  68.7 1.9 %collective-permute-start.18 = (bf16[512,256]{1,0:T(8,128)(2,1)}, bf16[512,256]{1,0:T(8,128)(2,1)}, u32[]{:S(2)}, u32[]{:S(2)}) collective-permute-start(bf16[512,256]{1,0:T(8,128)(2,1)} %convolution_convert_fusion.1), channel_id=1, source_target_pairs={{0,3},{1,0},{2,1},{3,2},{4,7},{5,4},{6,5},{7,6},{8,11},{9,8},{10,9... | collective-permute-start | bytes 786440 | tf_op jit(solution)/shard_map/ppermute | solution.py:21
  70.7 0.7 copy.31
  71.4 0.8 broadcast_in_dim.40
  72.2 0.7 subtract_convert_fusion
  72.9 1.2 copy-done.2
  74.1 1.4 %expert_in.1 = (bf16[256,256]{1,0:T(8,128)(2,1)S(1)}, bf16[4,256,512]{2,1,0:T(8,128)(2,1)S(1)}) custom-call(bf16[512,1024]{1,0:T(8,128)(2,1)S(1)} %bitcast.90, bf16[2048,256]{1,0:T(8,128)(2,1)S(1)} %bitcast.91, bf16[2048,256]{1,0:T(8,128)(2,1)S(1)} %bitcast.92, bf16[256,512]{1,0:T(8,128)(2,1)S(1)} %get-tuple-element.42.refs_3_, ...), custom_call_target="tpu_custom_call" | custom-call | tf_op jit(solution)/shard_map/expert_in/pallas_call | solution.py:277
  75.5 3.5 %collective-permute-done.17 = bf16[512,256]{1,0:T(8,128)(2,1)} collective-permute-done((bf16[512,256]{1,0:T(8,128)(2,1)}, bf16[512,256]{1,0:T(8,128)(2,1)}, u32[]{:S(2)}, u32[]{:S(2)}) %collective-permute-start.17) | collective-permute-done | bytes 262176 | tf_op jit(solution)/shard_map/ppermute | solution.py:21
  79.0 0.5 collective-permute-done.18
  79.5 1.3 %convert_add_fusion = f32[512,256]{1,0:T(8,128)S(1)} fusion(bf16[512,256]{1,0:T(8,128)(2,1)} %collective-permute-done.18, bf16[512,256]{1,0:T(8,128)(2,1)} %collective-permute-done.17, bf16[512,256]{1,0:T(8,128)(2,1)} %collective-permute-done.16, bf16[512,256]{1,0:T(8,128)(2,1)} %convolution_convert_fusion.1), kind=kLoop, calls=%fused_computation.14 | loop fusion | flops 917504 | bytes 1572864 | tf_op jit(solution)/shard_map/add | solution.py:42
  80.8 0.3 convolution_convert_fusion
  81.2 2.0 %collective-permute-start.11 = (bf16[256,256]{1,0:T(8,128)(2,1)S(1)}, bf16[256,256]{1,0:T(8,128)(2,1)S(1)}, u32[]{:S(2)}, u32[]{:S(2)}) collective-permute-start(bf16[256,256]{1,0:T(8,128)(2,1)S(1)} %get-tuple-element.46.refs_0_), channel_id=1, source_target_pairs={{0,1},{1,2},{2,3},{3,0},{4,5},{5,6},{6,7},{7,4},{8,9},{9,10},{10,1... | collective-permute-start | bytes 393224 | tf_op jit(solution)/shard_map/ppermute | solution.py:21
  83.3 2.2 %collective-permute-start.12 = (bf16[256,256]{1,0:T(8,128)(2,1)S(1)}, bf16[256,256]{1,0:T(8,128)(2,1)S(1)}, u32[]{:S(2)}, u32[]{:S(2)}) collective-permute-start(bf16[256,256]{1,0:T(8,128)(2,1)S(1)} %get-tuple-element.46.refs_0_), channel_id=1, source_target_pairs={{0,2},{1,3},{2,0},{3,1},{4,6},{5,7},{6,4},{7,5},{8,10},{9,11},{10,... | collective-permute-start | bytes 393224 | tf_op jit(solution)/shard_map/ppermute | solution.py:21
  85.5 1.1 collective-permute-start.13
  86.8 1.6 %collective-permute-done.11.refs_1_ = bf16[256,256]{1,0:T(8,128)(2,1)S(1)} collective-permute-done((bf16[256,256]{1,0:T(8,128)(2,1)S(1)}, bf16[256,256]{1,0:T(8,128)(2,1)S(1)}, u32[]{:S(2)}, u32[]{:S(2)}) %collective-permute-start.11) | collective-permute-done | bytes 131104 | tf_op jit(solution)/shard_map/ppermute | solution.py:21
  88.4 3.7 %collective-permute-done.12.refs_2_ = bf16[256,256]{1,0:T(8,128)(2,1)S(1)} collective-permute-done((bf16[256,256]{1,0:T(8,128)(2,1)S(1)}, bf16[256,256]{1,0:T(8,128)(2,1)S(1)}, u32[]{:S(2)}, u32[]{:S(2)}) %collective-permute-start.12) | collective-permute-done | bytes 131104 | tf_op jit(solution)/shard_map/ppermute | solution.py:21
  92.1 0.4 shard_map.274
  92.5 0.8 reshape.57
  93.3 11.5 %all-to-all-start.1 = ((bf16[64,4,512]{2,1,0:T(4,128)(2,1)}), bf16[64,4,512]{2,1,0:T(4,128)(2,1)S(1)}, u32[]{:S(2)}, u32[]{:S(2)}) async-start(bf16[64,4,512]{2,1,0:T(4,128)(2,1)} %reshape.57), calls=%async_computation.1 | async-start | bytes 524288 | tf_op jit(solution)/shard_map/all_to_all | solution.py:544
  104.9 2.8 %collective-permute-start.21 = (bf16[32,512]{1,0:T(8,128)(2,1)S(1)}, bf16[32,512]{1,0:T(8,128)(2,1)S(1)}, u32[]{:S(2)}, u32[]{:S(2)}) collective-permute-start(bf16[32,512]{1,0:T(8,128)(2,1)S(1)} %get-tuple-element.63), channel_id=1, source_target_pairs={{0,24},{8,0},{16,8},{24,16},{1,25},{9,1},{17,9},{25,17},{2,26},{10... | collective-permute-start | bytes 98312 | tf_op jit(solution)/shard_map/ppermute | solution.py:21
  107.6 0.9 collective-permute-start.22
  108.5 0.9 collective-permute-start.23
  109.3 7.6 %all-to-all-done.1 = bf16[64,4,512]{2,1,0:T(4,128)(2,1)S(1)} async-done(((bf16[64,4,512]{2,1,0:T(4,128)(2,1)}), bf16[64,4,512]{2,1,0:T(4,128)(2,1)S(1)}, u32[]{:S(2)}, u32[]{:S(2)}) %all-to-all-start.1) | async-done | bytes 262176 | tf_op jit(solution)/shard_map/all_to_all | solution.py:544
  117.3 0.3 multiply_reduce_fusion
  117.6 1.5 %collective-permute-start.24 = (f32[32]{0:T(128)S(1)}, f32[32]{0:T(128)S(1)}, u32[]{:S(2)}, u32[]{:S(2)}) collective-permute-start(f32[32]{0:T(128)S(1)} %get-tuple-element.87), channel_id=1, source_target_pairs={{0,1},{1,2},{2,3},{3,0},{4,5},{5,6},{6,7},{7,4},{8,9},{9,10},{10,1... | collective-permute-start | bytes 392 | tf_op jit(solution)/shard_map/ppermute | solution.py:21
  119.1 2.4 %collective-permute-start.25 = (f32[32]{0:T(128)S(1)}, f32[32]{0:T(128)S(1)}, u32[]{:S(2)}, u32[]{:S(2)}) collective-permute-start(f32[32]{0:T(128)S(1)} %get-tuple-element.87), channel_id=1, source_target_pairs={{0,2},{1,3},{2,0},{3,1},{4,6},{5,7},{6,4},{7,5},{8,10},{9,11},{10,... | collective-permute-start | bytes 392 | tf_op jit(solution)/shard_map/ppermute | solution.py:21
  121.4 1.2 collective-permute-start.26
  122.6 1.5 %collective-permute-done.25 = f32[32]{0:T(128)S(1)} collective-permute-done((f32[32]{0:T(128)S(1)}, f32[32]{0:T(128)S(1)}, u32[]{:S(2)}, u32[]{:S(2)}) %collective-permute-start.25) | collective-permute-done | bytes 160 | tf_op jit(solution)/shard_map/ppermute | solution.py:21
  124.1 0.9 collective-permute-done.26
  125.0 0.7 add_convert_fusion.1
  (86 shorter events, 1.2 us)
Async XLA Ops:
  0.6 67.7 %copy-start = (bf16[2048,64]{0,1:T(8,128)(2,1)S(1)}, bf16[2048,64]{0,1:T(8,128)(2,1)}, u32[]{:S(2)}) copy-start(bf16[2048,64]{0,1:T(8,128)(2,1)} %param.44) | copy-start | bytes 786436
  0.7 11.6 %copy-start.6 = (bf16[1,256,2048]{2,1,0:T(8,128)(2,1)S(1)}, bf16[1,256,2048]{2,1,0:T(8,128)(2,1)}, u32[]{:S(2)}) copy-start(bf16[1,256,2048]{2,1,0:T(8,128)(2,1)} %param.48) | copy-start | bytes 3145732
  6.5 8.7 %copy-start.12 = (bf16[32,2048]{1,0:T(8,128)(2,1)S(1)}, bf16[32,2048]{1,0:T(8,128)(2,1)}, u32[]{:S(2)}) copy-start(bf16[32,2048]{1,0:T(8,128)(2,1)} %get-tuple-element.30) | copy-start | bytes 393220
  6.5 8.7 %copy-start.8 = (bf16[32,2048]{1,0:T(8,128)(2,1)S(1)}, bf16[32,2048]{1,0:T(8,128)(2,1)}, u32[]{:S(2)}) copy-start(bf16[32,2048]{1,0:T(8,128)(2,1)} %refs_0_.1) | copy-start | bytes 393220
  6.5 8.8 %copy-start.14 = (s32[32,4]{0,1:T(4,128)S(1)}, s32[32,4]{0,1:T(4,128)}, u32[]{:S(2)}) copy-start(s32[32,4]{0,1:T(4,128)} %param.45) | copy-start | bytes 1540
  6.5 9.2 %copy-start.15 = (bf16[2048]{0:T(1024)(128)(2,1)S(1)}, bf16[2048]{0:T(1024)(128)(2,1)}, u32[]{:S(2)}) copy-start(bf16[2048]{0:T(1024)(128)(2,1)} %param.41) | copy-start | bytes 12292
  6.5 9.2 %copy-start.16 = (bf16[2048]{0:T(1024)(128)(2,1)S(1)}, bf16[2048]{0:T(1024)(128)(2,1)}, u32[]{:S(2)}) copy-start(bf16[2048]{0:T(1024)(128)(2,1)} %param.42) | copy-start | bytes 12292
  6.5 9.2 %collective-permute-start = (bf16[32,2048]{1,0:T(8,128)(2,1)}, bf16[32,2048]{1,0:T(8,128)(2,1)S(1)}, u32[]{:S(2)}, u32[]{:S(2)}) collective-permute-start(bf16[32,2048]{1,0:T(8,128)(2,1)} %get-tuple-element.30), channel_id=1, source_target_pairs={{0,1},{1,2},{2,3},{3,0},{4,5},{5,6},{6,7},{7,4},{8,9},{9,10},{10,1... | collective-permute-start | bytes 393224 | tf_op jit(solution)/shard_map/ppermute | solution.py:21
  8.1 10.1 %collective-permute-start.1 = (bf16[32,2048]{1,0:T(8,128)(2,1)}, bf16[32,2048]{1,0:T(8,128)(2,1)S(1)}, u32[]{:S(2)}, u32[]{:S(2)}) collective-permute-start(bf16[32,2048]{1,0:T(8,128)(2,1)} %get-tuple-element.30), channel_id=1, source_target_pairs={{0,2},{1,3},{2,0},{3,1},{4,6},{5,7},{6,4},{7,5},{8,10},{9,11},{10,... | collective-permute-start | bytes 393224 | tf_op jit(solution)/shard_map/ppermute | solution.py:21
  10.8 7.4 %collective-permute-start.2 = (bf16[32,2048]{1,0:T(8,128)(2,1)}, bf16[32,2048]{1,0:T(8,128)(2,1)S(1)}, u32[]{:S(2)}, u32[]{:S(2)}) collective-permute-start(bf16[32,2048]{1,0:T(8,128)(2,1)} %get-tuple-element.30), channel_id=1, source_target_pairs={{0,3},{1,0},{2,1},{3,2},{4,7},{5,4},{6,5},{7,6},{8,11},{9,8},{10,9... | collective-permute-start | bytes 393224 | tf_op jit(solution)/shard_map/ppermute | solution.py:21
  13.2 55.5 %collective-permute-start.10 = (bf16[256,512]{1,0:T(8,128)(2,1)}, bf16[256,512]{1,0:T(8,128)(2,1)S(1)}, u32[]{:S(2)}, u32[]{:S(2)}) collective-permute-start(bf16[256,512]{1,0:T(8,128)(2,1)} %get-tuple-element.57), channel_id=1, source_target_pairs={{0,3},{1,0},{2,1},{3,2},{4,7},{5,4},{6,5},{7,6},{8,11},{9,8},{10,9... | collective-permute-start | bytes 786440 | tf_op jit(solution)/shard_map/ppermute | solution.py:21
  13.2 59.7 %collective-permute-start.8 = (bf16[256,512]{1,0:T(8,128)(2,1)}, bf16[256,512]{1,0:T(8,128)(2,1)S(1)}, u32[]{:S(2)}, u32[]{:S(2)}) collective-permute-start(bf16[256,512]{1,0:T(8,128)(2,1)} %get-tuple-element.58), channel_id=1, source_target_pairs={{0,1},{1,2},{2,3},{3,0},{4,5},{5,6},{6,7},{7,4},{8,9},{9,10},{10,1... | collective-permute-start | bytes 786440 | tf_op jit(solution)/shard_map/ppermute | solution.py:21
  15.7 57.2 %collective-permute-start.9 = (bf16[256,512]{1,0:T(8,128)(2,1)}, bf16[256,512]{1,0:T(8,128)(2,1)S(1)}, u32[]{:S(2)}, u32[]{:S(2)}) collective-permute-start(bf16[256,512]{1,0:T(8,128)(2,1)} %get-tuple-element.60), channel_id=1, source_target_pairs={{0,2},{1,3},{2,0},{3,1},{4,6},{5,7},{6,4},{7,5},{8,10},{9,11},{10,... | collective-permute-start | bytes 786440 | tf_op jit(solution)/shard_map/ppermute | solution.py:21
  18.2 40.7 %copy-start.17 = (bf16[2048]{0:T(1024)(128)(2,1)S(1)}, bf16[2048]{0:T(1024)(128)(2,1)}, u32[]{:S(2)}) copy-start(bf16[2048]{0:T(1024)(128)(2,1)} %param.49) | copy-start | bytes 12292
  19.8 39.1 %copy-start.3 = (bf16[32,2560]{1,0:T(8,128)(2,1)}, bf16[32,2560]{1,0:T(8,128)(2,1)S(1)}, u32[]{:S(2)}) copy-start(bf16[32,2560]{1,0:T(8,128)(2,1)S(1)} %get-tuple-element.38) | copy-start | bytes 491524
  19.8 8.3 %collective-permute-start.3 = (bf16[32,512]{1,0:T(8,128)(2,1)S(1)}, bf16[32,512]{1,0:T(8,128)(2,1)S(1)}, u32[]{:S(2)}, u32[]{:S(2)}) collective-permute-start(bf16[32,512]{1,0:T(8,128)(2,1)S(1)} %get-tuple-element.36), channel_id=1, source_target_pairs={{0,32},{32,0},{64,96},{96,64},{128,160},{160,128},{192,224},{224,1... | collective-permute-start | bytes 98312 | tf_op jit(solution)/shard_map/ppermute | solution.py:48
  21.9 9.0 %collective-permute-start.14 = (bf16[1,3,32,512]{3,2,0,1:T(8,128)(2,1)S(1)}, bf16[1,3,32,512]{3,2,0,1:T(8,128)(2,1)S(1)}, u32[]{:S(2)}, u32[]{:S(2)}) collective-permute-start(bf16[1,3,32,512]{3,2,0,1:T(8,128)(2,1)S(1)} %maximum_bitcast_fusion.1), channel_id=1, source_target_pairs={{0,128},{32,160},{64,192},{96,224},{128,0},{160,32},{192,64},{224,... | collective-permute-start | bytes 294920 | tf_op jit(solution)/shard_map/ppermute | solution.py:48
  29.4 15.7 %copy-start.13 = (bf16[64,512]{1,0:T(8,128)(2,1)}, bf16[64,512]{1,0:T(8,128)(2,1)S(1)}, u32[]{:S(2)}) copy-start(bf16[64,512]{1,0:T(8,128)(2,1)S(1)} %get-tuple-element.74) | copy-start | bytes 196612
  29.4 15.7 %collective-permute-start.4 = (bf16[64,512]{1,0:T(8,128)(2,1)S(1)}, bf16[64,512]{1,0:T(8,128)(2,1)S(1)}, u32[]{:S(2)}, u32[]{:S(2)}) collective-permute-start(bf16[64,512]{1,0:T(8,128)(2,1)S(1)} %get-tuple-element.74), channel_id=1, source_target_pairs={{0,8},{8,16},{16,24},{24,0},{1,9},{9,17},{17,25},{25,1},{2,10},{10... | collective-permute-start | bytes 196616 | tf_op jit(solution)/shard_map/ppermute | solution.py:21
  31.6 27.3 %collective-permute-start.15 = (bf16[2,3,32,512]{3,2,0,1:T(8,128)(2,1)}, bf16[2,3,32,512]{3,2,0,1:T(8,128)(2,1)}, u32[]{:S(2)}, u32[]{:S(2)}) collective-permute-start(bf16[2,3,32,512]{3,2,0,1:T(8,128)(2,1)} %pad_maximum_fusion), channel_id=1, source_target_pairs={{0,64},{32,96},{64,0},{96,32},{128,192},{160,224},{192,128},{224,1... | collective-permute-start | bytes 589832 | tf_op jit(solution)/shard_map/ppermute | solution.py:48
  34.5 38.5 %all-to-all-start = ((bf16[64,8,1024]{2,1,0:T(8,128)(2,1)}), bf16[64,8,1024]{2,1,0:T(8,128)(2,1)S(1)}, u32[]{:S(2)}, u32[]{:S(2)}) async-start(bf16[64,8,1024]{2,1,0:T(8,128)(2,1)} %bitcast.6), calls=%async_computation | async-start | bytes 2097152 | tf_op jit(solution)/shard_map/all_to_all | solution.py:472
  45.0 23.1 %copy-start.20 = (bf16[2048,2]{0,1:T(2,128)(2,1)S(1)}, bf16[2048,2]{0,1:T(2,128)(2,1)}, u32[]{:S(2)}) copy-start(bf16[2048,2]{0,1:T(2,128)(2,1)} %param.43) | copy-start | bytes 24580
  45.0 7.8 %collective-permute-start.5 = (bf16[64,512]{1,0:T(8,128)(2,1)}, bf16[64,512]{1,0:T(8,128)(2,1)S(1)}, u32[]{:S(2)}, u32[]{:S(2)}) collective-permute-start(bf16[64,512]{1,0:T(8,128)(2,1)} %copy-done.13), channel_id=1, source_target_pairs={{0,16},{8,24},{16,0},{24,8},{1,17},{9,25},{17,1},{25,9},{2,18},{10... | collective-permute-start | bytes 196616 | tf_op jit(solution)/shard_map/ppermute | solution.py:21
  52.8 5.4 %collective-permute-start.6 = (bf16[64,512]{1,0:T(8,128)(2,1)}, bf16[64,512]{1,0:T(8,128)(2,1)S(1)}, u32[]{:S(2)}, u32[]{:S(2)}) collective-permute-start(bf16[64,512]{1,0:T(8,128)(2,1)} %copy-done.13), channel_id=1, source_target_pairs={{0,24},{8,0},{16,8},{24,16},{1,25},{9,1},{17,9},{25,17},{2,26},{10... | collective-permute-start | bytes 196616 | tf_op jit(solution)/shard_map/ppermute | solution.py:21
  58.9 0.8 copy-start.7
  58.9 1.8 %collective-permute-start.7 = (bf16[256,512]{1,0:T(8,128)(2,1)}, bf16[256,512]{1,0:T(8,128)(2,1)S(1)}, u32[]{:S(2)}, u32[]{:S(2)}) collective-permute-start(bf16[256,512]{1,0:T(8,128)(2,1)} %get-tuple-element.66), channel_id=1, source_target_pairs={{0,4},{4,0},{1,5},{5,1},{2,6},{6,2},{3,7},{7,3},{8,12},{12,8},{9,1... | collective-permute-start | bytes 786440 | tf_op jit(solution)/shard_map/ppermute | solution.py:48
  60.6 8.0 %copy-start.5 = (bf16[3,4,32,512]{3,2,1,0:T(8,128)(2,1)}, bf16[3,4,32,512]{3,2,1,0:T(8,128)(2,1)S(1)}, u32[]{:S(2)}) copy-start(bf16[3,4,32,512]{3,2,1,0:T(8,128)(2,1)S(1)} %maximum_bitcast_fusion) | copy-start | bytes 1179652
  60.6 6.2 %copy-start.4 = (bf16[32,2560]{1,0:T(8,128)(2,1)S(1)}, bf16[32,2560]{1,0:T(8,128)(2,1)}, u32[]{:S(2)}) copy-start(bf16[32,2560]{1,0:T(8,128)(2,1)} %copy-done.3) | copy-start | bytes 491524
  60.7 12.3 %copy-start.1 = (bf16[1,2048,256]{2,1,0:T(8,128)(2,1)S(1)}, bf16[1,2048,256]{2,1,0:T(8,128)(2,1)}, u32[]{:S(2)}) copy-start(bf16[1,2048,256]{2,1,0:T(8,128)(2,1)} %param.46) | copy-start | bytes 3145732
  63.5 12.0 %collective-permute-start.16 = (bf16[512,256]{1,0:T(8,128)(2,1)}, bf16[512,256]{1,0:T(8,128)(2,1)}, u32[]{:S(2)}, u32[]{:S(2)}) collective-permute-start(bf16[512,256]{1,0:T(8,128)(2,1)} %convolution_convert_fusion.1), channel_id=1, source_target_pairs={{0,1},{1,2},{2,3},{3,0},{4,5},{5,6},{6,7},{7,4},{8,9},{9,10},{10,1... | collective-permute-start | bytes 786440 | tf_op jit(solution)/shard_map/ppermute | solution.py:21
  64.4 14.6 %collective-permute-start.17 = (bf16[512,256]{1,0:T(8,128)(2,1)}, bf16[512,256]{1,0:T(8,128)(2,1)}, u32[]{:S(2)}, u32[]{:S(2)}) collective-permute-start(bf16[512,256]{1,0:T(8,128)(2,1)} %convolution_convert_fusion.1), channel_id=1, source_target_pairs={{0,2},{1,3},{2,0},{3,1},{4,6},{5,7},{6,4},{7,5},{8,10},{9,11},{10,... | collective-permute-start | bytes 786440 | tf_op jit(solution)/shard_map/ppermute | solution.py:21
  68.7 10.8 %collective-permute-start.18 = (bf16[512,256]{1,0:T(8,128)(2,1)}, bf16[512,256]{1,0:T(8,128)(2,1)}, u32[]{:S(2)}, u32[]{:S(2)}) collective-permute-start(bf16[512,256]{1,0:T(8,128)(2,1)} %convolution_convert_fusion.1), channel_id=1, source_target_pairs={{0,3},{1,0},{2,1},{3,2},{4,7},{5,4},{6,5},{7,6},{8,11},{9,8},{10,9... | collective-permute-start | bytes 786440 | tf_op jit(solution)/shard_map/ppermute | solution.py:21
  72.9 1.2 copy-start.2
  74.1 6.6 %slice-start = ((bf16[3,4,32,512]{3,2,1,0:T(8,128)(2,1)}), bf16[1,4,32,512]{3,2,1,0:T(8,128)(2,1)S(1)}, s32[]{:S(2)}) async-start(bf16[3,4,32,512]{3,2,1,0:T(8,128)(2,1)} %copy-done.5), calls=%async_computation.2 | async-start | bytes 262144 | tf_op jit(solution)/shard_map/slice | solution.py:483
  81.1 23.7 %copy-start.18 = (bf16[512]{0:T(512)(128)(2,1)S(1)}, bf16[512]{0:T(512)(128)(2,1)}, u32[]{:S(2)}) copy-start(bf16[512]{0:T(512)(128)(2,1)} %param.53) | copy-start | bytes 3076
  81.1 5.4 %collective-permute-start.19 = (bf16[256,512]{1,0:T(8,128)(2,1)S(1)}, bf16[256,512]{1,0:T(8,128)(2,1)S(1)}, u32[]{:S(2)}, u32[]{:S(2)}) collective-permute-start(bf16[256,512]{1,0:T(8,128)(2,1)S(1)} %slice.70), channel_id=1, source_target_pairs={{0,4},{4,0},{1,5},{5,1},{2,6},{6,2},{3,7},{7,3},{8,12},{12,8},{9,1... | collective-permute-start | bytes 786440 | tf_op jit(solution)/shard_map/ppermute | solution.py:48
  81.2 7.1 %collective-permute-start.11 = (bf16[256,256]{1,0:T(8,128)(2,1)S(1)}, bf16[256,256]{1,0:T(8,128)(2,1)S(1)}, u32[]{:S(2)}, u32[]{:S(2)}) collective-permute-start(bf16[256,256]{1,0:T(8,128)(2,1)S(1)} %get-tuple-element.46.refs_0_), channel_id=1, source_target_pairs={{0,1},{1,2},{2,3},{3,0},{4,5},{5,6},{6,7},{7,4},{8,9},{9,10},{10,1... | collective-permute-start | bytes 393224 | tf_op jit(solution)/shard_map/ppermute | solution.py:21
  83.3 8.8 %collective-permute-start.12 = (bf16[256,256]{1,0:T(8,128)(2,1)S(1)}, bf16[256,256]{1,0:T(8,128)(2,1)S(1)}, u32[]{:S(2)}, u32[]{:S(2)}) collective-permute-start(bf16[256,256]{1,0:T(8,128)(2,1)S(1)} %get-tuple-element.46.refs_0_), channel_id=1, source_target_pairs={{0,2},{1,3},{2,0},{3,1},{4,6},{5,7},{6,4},{7,5},{8,10},{9,11},{10,... | collective-permute-start | bytes 393224 | tf_op jit(solution)/shard_map/ppermute | solution.py:21
  85.5 6.6 %collective-permute-start.13 = (bf16[256,256]{1,0:T(8,128)(2,1)S(1)}, bf16[256,256]{1,0:T(8,128)(2,1)S(1)}, u32[]{:S(2)}, u32[]{:S(2)}) collective-permute-start(bf16[256,256]{1,0:T(8,128)(2,1)S(1)} %get-tuple-element.46.refs_0_), channel_id=1, source_target_pairs={{0,3},{1,0},{2,1},{3,2},{4,7},{5,4},{6,5},{7,6},{8,11},{9,8},{10,9... | collective-permute-start | bytes 393224 | tf_op jit(solution)/shard_map/ppermute | solution.py:21
  86.6 30.4 %copy-start.11 = (bf16[256,32]{1,0:T(8,128)(2,1)S(1)}, bf16[256,32]{1,0:T(8,128)(2,1)}, u32[]{:S(2)}) copy-start(bf16[256,32]{1,0:T(8,128)(2,1)} %get-tuple-element.48) | copy-start | bytes 49156
  86.7 18.1 %collective-permute-start.20 = (bf16[4,32,512]{2,1,0:T(8,128)(2,1)S(1)}, bf16[4,32,512]{2,1,0:T(8,128)(2,1)S(1)}, u32[]{:S(2)}, u32[]{:S(2)}) collective-permute-start(bf16[4,32,512]{2,1,0:T(8,128)(2,1)S(1)} %slice_bitcast_fusion), channel_id=1, source_target_pairs={{0,32},{32,0},{64,96},{96,64},{128,160},{160,128},{192,224},{224,1... | collective-permute-start | bytes 393224 | tf_op jit(solution)/shard_map/ppermute | solution.py:48
  92.1 25.2 %copy-start.9 = (bf16[256,32]{1,0:T(8,128)(2,1)S(1)}, bf16[256,32]{1,0:T(8,128)(2,1)}, u32[]{:S(2)}) copy-start(bf16[256,32]{1,0:T(8,128)(2,1)} %get-tuple-element.40) | copy-start | bytes 49156
  92.1 25.2 %copy-start.19 = (f32[32]{0:T(128)S(1)}, f32[32]{0:T(128)}, u32[]{:S(2)}) copy-start(f32[32]{0:T(128)} %fusion.6) | copy-start | bytes 388
  92.1 33.0 %copy-start.10 = (f32[32,512]{1,0:T(8,128)S(1)}, f32[32,512]{1,0:T(8,128)}, u32[]{:S(2)}) copy-start(f32[32,512]{1,0:T(8,128)} %slice_convert_fusion) | copy-start | bytes 196612
  93.3 23.7 %all-to-all-start.1 = ((bf16[64,4,512]{2,1,0:T(4,128)(2,1)}), bf16[64,4,512]{2,1,0:T(4,128)(2,1)S(1)}, u32[]{:S(2)}, u32[]{:S(2)}) async-start(bf16[64,4,512]{2,1,0:T(4,128)(2,1)} %reshape.57), calls=%async_computation.1 | async-start | bytes 524288 | tf_op jit(solution)/shard_map/all_to_all | solution.py:544
  104.9 12.4 %collective-permute-start.21 = (bf16[32,512]{1,0:T(8,128)(2,1)S(1)}, bf16[32,512]{1,0:T(8,128)(2,1)S(1)}, u32[]{:S(2)}, u32[]{:S(2)}) collective-permute-start(bf16[32,512]{1,0:T(8,128)(2,1)S(1)} %get-tuple-element.63), channel_id=1, source_target_pairs={{0,24},{8,0},{16,8},{24,16},{1,25},{9,1},{17,9},{25,17},{2,26},{10... | collective-permute-start | bytes 98312 | tf_op jit(solution)/shard_map/ppermute | solution.py:21
  107.6 9.6 %collective-permute-start.22 = (bf16[32,512]{1,0:T(8,128)(2,1)S(1)}, bf16[32,512]{1,0:T(8,128)(2,1)S(1)}, u32[]{:S(2)}, u32[]{:S(2)}) collective-permute-start(bf16[32,512]{1,0:T(8,128)(2,1)S(1)} %get-tuple-element.65), channel_id=1, source_target_pairs={{0,16},{8,24},{16,0},{24,8},{1,17},{9,25},{17,1},{25,9},{2,18},{10... | collective-permute-start | bytes 98312 | tf_op jit(solution)/shard_map/ppermute | solution.py:21
  108.5 8.8 %collective-permute-start.23 = (bf16[32,512]{1,0:T(8,128)(2,1)S(1)}, bf16[32,512]{1,0:T(8,128)(2,1)S(1)}, u32[]{:S(2)}, u32[]{:S(2)}) collective-permute-start(bf16[32,512]{1,0:T(8,128)(2,1)S(1)} %get-tuple-element.64), channel_id=1, source_target_pairs={{0,8},{8,16},{16,24},{24,0},{1,9},{9,17},{17,25},{25,1},{2,10},{10... | collective-permute-start | bytes 98312 | tf_op jit(solution)/shard_map/ppermute | solution.py:21
  117.6 5.0 %collective-permute-start.24 = (f32[32]{0:T(128)S(1)}, f32[32]{0:T(128)S(1)}, u32[]{:S(2)}, u32[]{:S(2)}) collective-permute-start(f32[32]{0:T(128)S(1)} %get-tuple-element.87), channel_id=1, source_target_pairs={{0,1},{1,2},{2,3},{3,0},{4,5},{5,6},{6,7},{7,4},{8,9},{9,10},{10,1... | collective-permute-start | bytes 392 | tf_op jit(solution)/shard_map/ppermute | solution.py:21
  119.1 5.1 %collective-permute-start.25 = (f32[32]{0:T(128)S(1)}, f32[32]{0:T(128)S(1)}, u32[]{:S(2)}, u32[]{:S(2)}) collective-permute-start(f32[32]{0:T(128)S(1)} %get-tuple-element.87), channel_id=1, source_target_pairs={{0,2},{1,3},{2,0},{3,1},{4,6},{5,7},{6,4},{7,5},{8,10},{9,11},{10,... | collective-permute-start | bytes 392 | tf_op jit(solution)/shard_map/ppermute | solution.py:21
  121.4 3.6 %collective-permute-start.26 = (f32[32]{0:T(128)S(1)}, f32[32]{0:T(128)S(1)}, u32[]{:S(2)}, u32[]{:S(2)}) collective-permute-start(f32[32]{0:T(128)S(1)} %get-tuple-element.87), channel_id=1, source_target_pairs={{0,3},{1,0},{2,1},{3,2},{4,7},{5,4},{6,5},{7,6},{8,11},{9,8},{10,9... | collective-permute-start | bytes 392 | tf_op jit(solution)/shard_map/ppermute | solution.py:21

commit v4 on v3

--- a/solution.py
+++ b/solution.py
@@ -339,7 +339,7 @@
         out_specs=[vmem] * 2,
         compiler_params=pltpu.CompilerParams(vmem_limit_bytes=FEEDER_VMEM),
         out_shape=[
-            jax.ShapeDtypeStruct((slots, seqs), jnp.float32),
+            jax.ShapeDtypeStruct((slots, seqs), jnp.bfloat16),
             jax.ShapeDtypeStruct((2 * slots, 2 * seqs), jnp.bfloat16),
         ],
     )(routes)
@@ -478,7 +478,6 @@
     tokens = jnp.concatenate(tokens, axis=0)
     tokens = jnp.concatenate(from_all(tokens, "ep_1"), axis=0)
     tokens = jnp.concatenate([tokens, from_flip(tokens, "ep_2", 1)], axis=0)
-    kept, tokens = lax.optimization_barrier((kept, tokens))
     feed, stream_quarter = kept[:, :width], kept[:, width:]
     down_rows = unit_rows[2]
     down = expert_down[0]
@@ -510,7 +509,7 @@
     logits = lax.dot_general(expert_router, feed, features, preferred_element_type=jnp.float32)
     pick_exp = jnp.exp(jnp.where(picked, logits, -jnp.inf))
     pick_weight = pick_exp / jnp.sum(pick_exp, axis=0, keepdims=True) * group_weight
-    slot_weight = in_slot * jnp.repeat(pick_weight, capacity, axis=0)
+    slot_weight = in_slot.astype(jnp.float32) * jnp.repeat(pick_weight, capacity, axis=0)
     weight_high = slot_weight.astype(jnp.bfloat16)
     weight_low = (slot_weight - weight_high.astype(jnp.float32)).astype(jnp.bfloat16)
     switch = jax.nn.sigmoid(dot32(feed, dense_switch))

time: 127 us -> 148 us (1.17)
  waiting for transfers between devices: 27.8 us -> 56.4 us
  local copies, waits for them, and re-layouts: 9.29 us -> 3.44 us
  matrix products: 3.97 us -> 2.39 us
    ppermute x6, waiting for transfers between devices: 0.02 us -> 25.5 us  [from_flip(): return lax.ppermute(array, axis, [(i, i ^ bit) for i in range(count)])]
    unnamed x47, local copies, waits for them, and re-layouts: 4.57 us -> 1.37 us
    ppermute x21, waiting for transfers between devices: 20.1 us -> 23.2 us  [from_shift(): lax.ppermute(array, axis, [(i, (i + shift) % count) for i in range(count)])]
    ppermute x6, starting transfers between devices: 10.5 us -> 12.5 us  [from_flip(): return lax.ppermute(array, axis, [(i, i ^ bit) for i in range(count)])]
  transfers between devices with their start and end apart: 29 -> 29, of which waited for: 10 -> 11; matrix products, arithmetic and copies ran while one was open for 12% -> 5% of each run, Pallas kernels for 3% -> 3%
where the time goes in v4:
time: 148 us; the launch traced here: 147 us
  starting transfers between devices  68.1 us (46%)
  waiting for transfers between devices  56.4 us (38%)
  Pallas kernels  9.53 us (6%)
  other arithmetic  6.09 us (4%)
  local copies, waits for them, and re-layouts  3.44 us (2%)
  matrix products  2.39 us (2%)
    ppermute x21, starting transfers between devices, from_shift(): lax.ppermute(array, axis, [(i, (i + shift) % count) for i in range(count)])  34.7 us
    ppermute x6, waiting for transfers between devices, from_flip(): return lax.ppermute(array, axis, [(i, i ^ bit) for i in range(count)])  25.5 us
    ppermute x21, waiting for transfers between devices, from_shift(): lax.ppermute(array, axis, [(i, (i + shift) % count) for i in range(count)])  23.2 us
    ppermute x6, starting transfers between devices, from_flip(): return lax.ppermute(array, axis, [(i, i ^ bit) for i in range(count)])  12.5 us
    all_to_all x1, starting transfers between devices, on_device(): lax.all_to_all(served.reshape(expert_count, capacity, quarter), EP, 0, 0,...  11.1 us
    all_to_all x1, starting transfers between devices, on_device(): lax.all_to_all(outgoing.reshape(expert_count, 2 * capacity, width // 2),...  9.81 us
    all_to_all x1, waiting for transfers between devices, on_device(): lax.all_to_all(served.reshape(expert_count, capacity, quarter), EP, 0, 0,...  7.65 us
    pallas_call x1, Pallas kernels, mixer(): pl.pallas_call(mixer_kernel, name='mixer', in_specs=[pl.BlockSpec(memory_...  5.81 us
  transfers between devices with their start and end apart: 29, of which 11 were waited for; matrix products, arithmetic and copies ran while one was open for 5% of the time, Pallas kernels for 3%

profile of v4, /device:TPU:32, one launch (start us, length us, event | category | flops | bytes accessed | tf_op | source)
XLA Modules:
  0.0 147.0 jit_solution(7830816289730249770)
XLA Ops:
  0.7 5.8 %mixer.1 = (bf16[32,2048]{1,0:T(8,128)(2,1)}, f32[32,2,64,128]{3,2,1,0:T(8,128)}, bf16[3,3,32,128]{3,2,1,0:T(8,128)(2,1)}) custom-call(s32[1]{0:T(128)} %bitcast.place, bf16[32,2048]{1,0:T(8,128)(2,1)} %refs_0_.1, bf16[16,128]{1,0:T(8,128)(2,1)} %bitcast.105, bf16[2048,128]{1,0:T(8,128)(2,1)} %refs_2_.1, bf16[2048,128]{1,0:T(8,128)(2,1)} %refs_3_.1, ...), custom_call_target="tpu_custom_call" | custom-call | tf_op jit(solution)/shard_map/mixer/pallas_call | solution.py:226
  6.6 1.6 %collective-permute-start = (bf16[32,2048]{1,0:T(8,128)(2,1)}, bf16[32,2048]{1,0:T(8,128)(2,1)S(1)}, u32[]{:S(2)}, u32[]{:S(2)}) collective-permute-start(bf16[32,2048]{1,0:T(8,128)(2,1)} %get-tuple-element.28), channel_id=1, source_target_pairs={{0,1},{1,2},{2,3},{3,0},{4,5},{5,6},{6,7},{7,4},{8,9},{9,10},{10,1... | collective-permute-start | bytes 393224 | tf_op jit(solution)/shard_map/ppermute | solution.py:21
  8.2 2.7 %collective-permute-start.1 = (bf16[32,2048]{1,0:T(8,128)(2,1)}, bf16[32,2048]{1,0:T(8,128)(2,1)S(1)}, u32[]{:S(2)}, u32[]{:S(2)}) collective-permute-start(bf16[32,2048]{1,0:T(8,128)(2,1)} %get-tuple-element.28), channel_id=1, source_target_pairs={{0,2},{1,3},{2,0},{3,1},{4,6},{5,7},{6,4},{7,5},{8,10},{9,11},{10,... | collective-permute-start | bytes 393224 | tf_op jit(solution)/shard_map/ppermute | solution.py:21
  10.9 1.4 collective-permute-start.2
  12.3 0.9 dynamic-slice_bitcast_fusion
  13.3 0.6 collective-permute-start.3
  13.9 6.4 %collective-permute-start.14 = (bf16[1,3,32,512]{3,2,0,1:T(8,128)(2,1)S(1)}, bf16[1,3,32,512]{3,2,0,1:T(8,128)(2,1)S(1)}, u32[]{:S(2)}, u32[]{:S(2)}) collective-permute-start(bf16[1,3,32,512]{3,2,0,1:T(8,128)(2,1)S(1)} %maximum_bitcast_fusion.1), channel_id=1, source_target_pairs={{0,128},{32,160},{64,192},{96,224},{128,0},{160,32},{192,64},{224,... | collective-permute-start | bytes 294920 | tf_op jit(solution)/shard_map/ppermute | solution.py:48
  20.4 0.1 tile.10.routes
  20.5 0.3 slots.1
  20.9 3.1 %collective-permute-done.14 = bf16[1,3,32,512]{3,2,0,1:T(8,128)(2,1)S(1)} collective-permute-done((bf16[1,3,32,512]{3,2,0,1:T(8,128)(2,1)S(1)}, bf16[1,3,32,512]{3,2,0,1:T(8,128)(2,1)S(1)}, u32[]{:S(2)}, u32[]{:S(2)}) %collective-permute-start.14) | collective-permute-done | bytes 98336 | tf_op jit(solution)/shard_map/ppermute | solution.py:48
  24.0 0.9 collective-permute-start.4
  24.9 0.7 pad_maximum_fusion
  25.6 1.9 %collective-permute-start.5 = (bf16[256,512]{1,0:T(8,128)(2,1)}, bf16[256,512]{1,0:T(8,128)(2,1)S(1)}, u32[]{:S(2)}, u32[]{:S(2)}) collective-permute-start(bf16[256,512]{1,0:T(8,128)(2,1)} %get-tuple-element.53), channel_id=1, source_target_pairs={{0,3},{1,0},{2,1},{3,2},{4,7},{5,4},{6,5},{7,6},{8,11},{9,8},{10,9... | collective-permute-start | bytes 786440 | tf_op jit(solution)/shard_map/ppermute | solution.py:21
  27.5 2.8 %collective-permute-start.15 = (bf16[2,3,32,512]{3,2,0,1:T(8,128)(2,1)}, bf16[2,3,32,512]{3,2,0,1:T(8,128)(2,1)}, u32[]{:S(2)}, u32[]{:S(2)}) collective-permute-start(bf16[2,3,32,512]{3,2,0,1:T(8,128)(2,1)} %pad_maximum_fusion), channel_id=1, source_target_pairs={{0,64},{32,96},{64,0},{96,32},{128,192},{160,224},{192,128},{224,1... | collective-permute-start | bytes 589832 | tf_op jit(solution)/shard_map/ppermute | solution.py:48
  30.2 1.6 %feeder.1 = (bf16[32,2560]{1,0:T(8,128)(2,1)S(1)}, bf16[32,512]{1,0:T(8,128)(2,1)S(1)}, bf16[512,1024]{1,0:T(8,128)(2,1)}) custom-call(s32[1]{0:T(128)} %bitcast.place, f32[32,2048]{1,0:T(8,128)S(1)} %convert_element_type.84.part_0, bf16[32,2048]{1,0:T(8,128)(2,1)S(1)} %collective-permute-done.part_1, bf16[32,2048]{1,0:T(8,128)(2,1)S(1)} %collective-permute-done.1.part_2, ...), custom_call_target="tpu_custom_call" | custom-call | tf_op jit(solution)/shard_map/feeder/pallas_call | solution.py:386
  31.9 9.8 %all-to-all-start = ((bf16[64,8,1024]{2,1,0:T(8,128)(2,1)}), bf16[64,8,1024]{2,1,0:T(8,128)(2,1)S(1)}, u32[]{:S(2)}, u32[]{:S(2)}) async-start(bf16[64,8,1024]{2,1,0:T(8,128)(2,1)} %bitcast.6), calls=%async_computation | async-start | bytes 2097152 | tf_op jit(solution)/shard_map/all_to_all | solution.py:472
  41.7 0.5 collective-permute-start.9
  42.2 0.3 fusion.25
  42.5 0.2 fusion.24
  42.7 22.4 %collective-permute-done.9 = bf16[32,512]{1,0:T(8,128)(2,1)S(1)} collective-permute-done((bf16[32,512]{1,0:T(8,128)(2,1)S(1)}, bf16[32,512]{1,0:T(8,128)(2,1)S(1)}, u32[]{:S(2)}, u32[]{:S(2)}) %collective-permute-start.9) | collective-permute-done | bytes 32800 | tf_op jit(solution)/shard_map/ppermute | solution.py:48
  65.1 1.8 %collective-permute-start.10 = (bf16[64,512]{1,0:T(8,128)(2,1)S(1)}, bf16[64,512]{1,0:T(8,128)(2,1)S(1)}, u32[]{:S(2)}, u32[]{:S(2)}) collective-permute-start(bf16[64,512]{1,0:T(8,128)(2,1)S(1)} %get-tuple-element.70), channel_id=1, source_target_pairs={{0,8},{8,16},{16,24},{24,0},{1,9},{9,17},{17,25},{25,1},{2,10},{10... | collective-permute-start | bytes 196616 | tf_op jit(solution)/shard_map/ppermute | solution.py:21
  66.9 0.1 fusion.6
  67.0 3.8 %collective-permute-done.10 = bf16[64,512]{1,0:T(8,128)(2,1)S(1)} collective-permute-done((bf16[64,512]{1,0:T(8,128)(2,1)S(1)}, bf16[64,512]{1,0:T(8,128)(2,1)S(1)}, u32[]{:S(2)}, u32[]{:S(2)}) %collective-permute-start.10) | collective-permute-done | bytes 65568 | tf_op jit(solution)/shard_map/ppermute | solution.py:21
  70.8 1.8 %collective-permute-start.11 = (bf16[64,512]{1,0:T(8,128)(2,1)S(1)}, bf16[64,512]{1,0:T(8,128)(2,1)S(1)}, u32[]{:S(2)}, u32[]{:S(2)}) collective-permute-start(bf16[64,512]{1,0:T(8,128)(2,1)S(1)} %get-tuple-element.70), channel_id=1, source_target_pairs={{0,16},{8,24},{16,0},{24,8},{1,17},{9,25},{17,1},{25,9},{2,18},{10... | collective-permute-start | bytes 196616 | tf_op jit(solution)/shard_map/ppermute | solution.py:21
  72.7 3.9 %collective-permute-done.11 = bf16[64,512]{1,0:T(8,128)(2,1)S(1)} collective-permute-done((bf16[64,512]{1,0:T(8,128)(2,1)S(1)}, bf16[64,512]{1,0:T(8,128)(2,1)S(1)}, u32[]{:S(2)}, u32[]{:S(2)}) %collective-permute-start.11) | collective-permute-done | bytes 65568 | tf_op jit(solution)/shard_map/ppermute | solution.py:21
  76.6 1.2 collective-permute-start.12
  77.9 3.0 %collective-permute-done.12 = bf16[64,512]{1,0:T(8,128)(2,1)S(1)} collective-permute-done((bf16[64,512]{1,0:T(8,128)(2,1)S(1)}, bf16[64,512]{1,0:T(8,128)(2,1)S(1)}, u32[]{:S(2)}, u32[]{:S(2)}) %collective-permute-start.12) | collective-permute-done | bytes 65568 | tf_op jit(solution)/shard_map/ppermute | solution.py:21
  80.9 0.3 collective-permute-start.13
  81.2 1.4 slice_convert_fusion
  82.6 1.1 maximum_bitcast_fusion
  83.7 1.0 convolution_convert_fusion.1
  84.8 0.8 collective-permute-start.16
  85.6 2.0 %collective-permute-start.17 = (bf16[512,256]{1,0:T(8,128)(2,1)}, bf16[512,256]{1,0:T(8,128)(2,1)}, u32[]{:S(2)}, u32[]{:S(2)}) collective-permute-start(bf16[512,256]{1,0:T(8,128)(2,1)} %convolution_convert_fusion.1), channel_id=1, source_target_pairs={{0,2},{1,3},{2,0},{3,1},{4,6},{5,7},{6,4},{7,5},{8,10},{9,11},{10,... | collective-permute-start | bytes 786440 | tf_op jit(solution)/shard_map/ppermute | solution.py:21
  87.6 2.6 %collective-permute-start.18 = (bf16[512,256]{1,0:T(8,128)(2,1)}, bf16[512,256]{1,0:T(8,128)(2,1)}, u32[]{:S(2)}, u32[]{:S(2)}) collective-permute-start(bf16[512,256]{1,0:T(8,128)(2,1)} %convolution_convert_fusion.1), channel_id=1, source_target_pairs={{0,3},{1,0},{2,1},{3,2},{4,7},{5,4},{6,5},{7,6},{8,11},{9,8},{10,9... | collective-permute-start | bytes 786440 | tf_op jit(solution)/shard_map/ppermute | solution.py:21
  90.2 0.1 divide_multiply_fusion
  90.3 0.1 copy.31
  90.4 0.7 subtract_convert_fusion
  91.1 1.2 copy-done.2
  92.3 1.4 expert_in.1
  93.7 6.9 %collective-permute-done.16 = bf16[512,256]{1,0:T(8,128)(2,1)} collective-permute-done((bf16[512,256]{1,0:T(8,128)(2,1)}, bf16[512,256]{1,0:T(8,128)(2,1)}, u32[]{:S(2)}, u32[]{:S(2)}) %collective-permute-start.16) | collective-permute-done | bytes 262176 | tf_op jit(solution)/shard_map/ppermute | solution.py:21
  100.6 0.6 collective-permute-done.18
  101.2 1.3 convert_add_fusion
  102.6 0.3 convolution_convert_fusion
  102.9 0.1 collective-permute-start.19
  103.0 1.8 %collective-permute-start.6 = (bf16[256,256]{1,0:T(8,128)(2,1)S(1)}, bf16[256,256]{1,0:T(8,128)(2,1)S(1)}, u32[]{:S(2)}, u32[]{:S(2)}) collective-permute-start(bf16[256,256]{1,0:T(8,128)(2,1)S(1)} %get-tuple-element.40.refs_0_), channel_id=1, source_target_pairs={{0,1},{1,2},{2,3},{3,0},{4,5},{5,6},{6,7},{7,4},{8,9},{9,10},{10,1... | collective-permute-start | bytes 393224 | tf_op jit(solution)/shard_map/ppermute | solution.py:21
  104.8 2.4 %collective-permute-start.7 = (bf16[256,256]{1,0:T(8,128)(2,1)S(1)}, bf16[256,256]{1,0:T(8,128)(2,1)S(1)}, u32[]{:S(2)}, u32[]{:S(2)}) collective-permute-start(bf16[256,256]{1,0:T(8,128)(2,1)S(1)} %get-tuple-element.40.refs_0_), channel_id=1, source_target_pairs={{0,2},{1,3},{2,0},{3,1},{4,6},{5,7},{6,4},{7,5},{8,10},{9,11},{10,... | collective-permute-start | bytes 393224 | tf_op jit(solution)/shard_map/ppermute | solution.py:21
  107.2 1.3 collective-permute-start.8
  108.6 2.5 %collective-permute-start.20 = (bf16[4,32,512]{2,1,0:T(8,128)(2,1)S(1)}, bf16[4,32,512]{2,1,0:T(8,128)(2,1)S(1)}, u32[]{:S(2)}, u32[]{:S(2)}) collective-permute-start(bf16[4,32,512]{2,1,0:T(8,128)(2,1)S(1)} %slice_bitcast_fusion), channel_id=1, source_target_pairs={{0,32},{32,0},{64,96},{96,64},{128,160},{160,128},{192,224},{224,1... | collective-permute-start | bytes 393224 | tf_op jit(solution)/shard_map/ppermute | solution.py:48
  111.1 2.7 %collective-permute-done.7.refs_2_ = bf16[256,256]{1,0:T(8,128)(2,1)S(1)} collective-permute-done((bf16[256,256]{1,0:T(8,128)(2,1)S(1)}, bf16[256,256]{1,0:T(8,128)(2,1)S(1)}, u32[]{:S(2)}, u32[]{:S(2)}) %collective-permute-start.7) | collective-permute-done | bytes 131104 | tf_op jit(solution)/shard_map/ppermute | solution.py:21
  113.8 0.4 shard_map.274
  114.2 0.8 reshape.57
  115.0 11.1 %all-to-all-start.1 = ((bf16[64,4,512]{2,1,0:T(4,128)(2,1)}), bf16[64,4,512]{2,1,0:T(4,128)(2,1)S(1)}, u32[]{:S(2)}, u32[]{:S(2)}) async-start(bf16[64,4,512]{2,1,0:T(4,128)(2,1)} %reshape.57), calls=%async_computation.1 | async-start | bytes 524288 | tf_op jit(solution)/shard_map/all_to_all | solution.py:543
  126.1 2.8 %collective-permute-start.21 = (bf16[32,512]{1,0:T(8,128)(2,1)S(1)}, bf16[32,512]{1,0:T(8,128)(2,1)S(1)}, u32[]{:S(2)}, u32[]{:S(2)}) collective-permute-start(bf16[32,512]{1,0:T(8,128)(2,1)S(1)} %get-tuple-element.59), channel_id=1, source_target_pairs={{0,24},{8,0},{16,8},{24,16},{1,25},{9,1},{17,9},{25,17},{2,26},{10... | collective-permute-start | bytes 98312 | tf_op jit(solution)/shard_map/ppermute | solution.py:21
  128.9 0.9 collective-permute-start.22
  129.8 0.9 collective-permute-start.23
  130.6 7.6 %all-to-all-done.1 = bf16[64,4,512]{2,1,0:T(4,128)(2,1)S(1)} async-done(((bf16[64,4,512]{2,1,0:T(4,128)(2,1)}), bf16[64,4,512]{2,1,0:T(4,128)(2,1)S(1)}, u32[]{:S(2)}, u32[]{:S(2)}) %all-to-all-start.1) | async-done | bytes 262176 | tf_op jit(solution)/shard_map/all_to_all | solution.py:543
  138.3 0.2 fusion.26
  138.5 0.3 multiply_reduce_fusion
  138.8 1.5 %collective-permute-start.24 = (f32[32]{0:T(128)S(1)}, f32[32]{0:T(128)S(1)}, u32[]{:S(2)}, u32[]{:S(2)}) collective-permute-start(f32[32]{0:T(128)S(1)} %get-tuple-element.83), channel_id=1, source_target_pairs={{0,1},{1,2},{2,3},{3,0},{4,5},{5,6},{6,7},{7,4},{8,9},{9,10},{10,1... | collective-permute-start | bytes 392 | tf_op jit(solution)/shard_map/ppermute | solution.py:21
  140.4 2.4 %collective-permute-start.25 = (f32[32]{0:T(128)S(1)}, f32[32]{0:T(128)S(1)}, u32[]{:S(2)}, u32[]{:S(2)}) collective-permute-start(f32[32]{0:T(128)S(1)} %get-tuple-element.83), channel_id=1, source_target_pairs={{0,2},{1,3},{2,0},{3,1},{4,6},{5,7},{6,4},{7,5},{8,10},{9,11},{10,... | collective-permute-start | bytes 392 | tf_op jit(solution)/shard_map/ppermute | solution.py:21
  142.8 1.3 collective-permute-start.26
  144.1 1.4 collective-permute-done.25
  145.4 0.9 collective-permute-done.26
  146.3 0.7 add_convert_fusion.1
  (86 shorter events, 0.6 us)
Async XLA Ops:
  0.6 41.6 %copy-start = (bf16[2048,64]{0,1:T(8,128)(2,1)S(1)}, bf16[2048,64]{0,1:T(8,128)(2,1)}, u32[]{:S(2)}) copy-start(bf16[2048,64]{0,1:T(8,128)(2,1)} %param.44) | copy-start | bytes 786436
  0.7 11.7 %copy-start.5 = (bf16[1,256,2048]{2,1,0:T(8,128)(2,1)S(1)}, bf16[1,256,2048]{2,1,0:T(8,128)(2,1)}, u32[]{:S(2)}) copy-start(bf16[1,256,2048]{2,1,0:T(8,128)(2,1)} %param.48) | copy-start | bytes 3145732
  6.5 7.4 %copy-start.12 = (bf16[32,512]{1,0:T(8,128)(2,1)S(1)}, bf16[32,512]{1,0:T(8,128)(2,1)}, u32[]{:S(2)}) copy-start(bf16[32,512]{1,0:T(8,128)(2,1)} %param.52) | copy-start | bytes 98308
  6.5 7.4 %copy-start.13 = (bf16[32,512]{1,0:T(8,128)(2,1)S(1)}, bf16[32,512]{1,0:T(8,128)(2,1)}, u32[]{:S(2)}) copy-start(bf16[32,512]{1,0:T(8,128)(2,1)} %param.51) | copy-start | bytes 98308
  6.5 7.4 %copy-start.14 = (bf16[32,512]{1,0:T(8,128)(2,1)S(1)}, bf16[32,512]{1,0:T(8,128)(2,1)}, u32[]{:S(2)}) copy-start(bf16[32,512]{1,0:T(8,128)(2,1)} %param.50) | copy-start | bytes 98308
  6.5 13.8 %copy-start.15 = (s32[32,4]{0,1:T(4,128)S(1)}, s32[32,4]{0,1:T(4,128)}, u32[]{:S(2)}) copy-start(s32[32,4]{0,1:T(4,128)} %param.45) | copy-start | bytes 1540
  6.5 13.8 %copy-start.11 = (bf16[32,2048]{1,0:T(8,128)(2,1)S(1)}, bf16[32,2048]{1,0:T(8,128)(2,1)}, u32[]{:S(2)}) copy-start(bf16[32,2048]{1,0:T(8,128)(2,1)} %get-tuple-element.28) | copy-start | bytes 393220
  6.5 13.8 %copy-start.7 = (bf16[32,2048]{1,0:T(8,128)(2,1)S(1)}, bf16[32,2048]{1,0:T(8,128)(2,1)}, u32[]{:S(2)}) copy-start(bf16[32,2048]{1,0:T(8,128)(2,1)} %refs_0_.1) | copy-start | bytes 393220
  6.5 14.2 %copy-start.16 = (bf16[2048]{0:T(1024)(128)(2,1)S(1)}, bf16[2048]{0:T(1024)(128)(2,1)}, u32[]{:S(2)}) copy-start(bf16[2048]{0:T(1024)(128)(2,1)} %param.41) | copy-start | bytes 12292
  6.6 14.2 %copy-start.17 = (bf16[2048]{0:T(1024)(128)(2,1)S(1)}, bf16[2048]{0:T(1024)(128)(2,1)}, u32[]{:S(2)}) copy-start(bf16[2048]{0:T(1024)(128)(2,1)} %param.42) | copy-start | bytes 12292
  6.6 14.3 %copy-start.18 = (bf16[2048]{0:T(1024)(128)(2,1)S(1)}, bf16[2048]{0:T(1024)(128)(2,1)}, u32[]{:S(2)}) copy-start(bf16[2048]{0:T(1024)(128)(2,1)} %param.49) | copy-start | bytes 12292
  6.6 19.0 %collective-permute-start = (bf16[32,2048]{1,0:T(8,128)(2,1)}, bf16[32,2048]{1,0:T(8,128)(2,1)S(1)}, u32[]{:S(2)}, u32[]{:S(2)}) collective-permute-start(bf16[32,2048]{1,0:T(8,128)(2,1)} %get-tuple-element.28), channel_id=1, source_target_pairs={{0,1},{1,2},{2,3},{3,0},{4,5},{5,6},{6,7},{7,4},{8,9},{9,10},{10,1... | collective-permute-start | bytes 393224 | tf_op jit(solution)/shard_map/ppermute | solution.py:21
  8.2 19.3 %collective-permute-start.1 = (bf16[32,2048]{1,0:T(8,128)(2,1)}, bf16[32,2048]{1,0:T(8,128)(2,1)S(1)}, u32[]{:S(2)}, u32[]{:S(2)}) collective-permute-start(bf16[32,2048]{1,0:T(8,128)(2,1)} %get-tuple-element.28), channel_id=1, source_target_pairs={{0,2},{1,3},{2,0},{3,1},{4,6},{5,7},{6,4},{7,5},{8,10},{9,11},{10,... | collective-permute-start | bytes 393224 | tf_op jit(solution)/shard_map/ppermute | solution.py:21
  10.9 19.4 %collective-permute-start.2 = (bf16[32,2048]{1,0:T(8,128)(2,1)}, bf16[32,2048]{1,0:T(8,128)(2,1)S(1)}, u32[]{:S(2)}, u32[]{:S(2)}) collective-permute-start(bf16[32,2048]{1,0:T(8,128)(2,1)} %get-tuple-element.28), channel_id=1, source_target_pairs={{0,3},{1,0},{2,1},{3,2},{4,7},{5,4},{6,5},{7,6},{8,11},{9,8},{10,9... | collective-permute-start | bytes 393224 | tf_op jit(solution)/shard_map/ppermute | solution.py:21
  13.3 74.3 %collective-permute-start.3 = (bf16[256,512]{1,0:T(8,128)(2,1)}, bf16[256,512]{1,0:T(8,128)(2,1)S(1)}, u32[]{:S(2)}, u32[]{:S(2)}) collective-permute-start(bf16[256,512]{1,0:T(8,128)(2,1)} %get-tuple-element.54), channel_id=1, source_target_pairs={{0,1},{1,2},{2,3},{3,0},{4,5},{5,6},{6,7},{7,4},{8,9},{9,10},{10,1... | collective-permute-start | bytes 786440 | tf_op jit(solution)/shard_map/ppermute | solution.py:21
  13.9 11.7 %copy-start.6 = (bf16[1,3,32,512]{3,2,0,1:T(8,128)(2,1)}, bf16[1,3,32,512]{3,2,0,1:T(8,128)(2,1)S(1)}, u32[]{:S(2)}) copy-start(bf16[1,3,32,512]{3,2,0,1:T(8,128)(2,1)S(1)} %maximum_bitcast_fusion.1) | copy-start | bytes 294916
  13.9 10.1 %collective-permute-start.14 = (bf16[1,3,32,512]{3,2,0,1:T(8,128)(2,1)S(1)}, bf16[1,3,32,512]{3,2,0,1:T(8,128)(2,1)S(1)}, u32[]{:S(2)}, u32[]{:S(2)}) collective-permute-start(bf16[1,3,32,512]{3,2,0,1:T(8,128)(2,1)S(1)} %maximum_bitcast_fusion.1), channel_id=1, source_target_pairs={{0,128},{32,160},{64,192},{96,224},{128,0},{160,32},{192,64},{224,... | collective-permute-start | bytes 294920 | tf_op jit(solution)/shard_map/ppermute | solution.py:48
  20.4 22.2 %copy-start.20 = (bf16[2048,2]{0,1:T(2,128)(2,1)S(1)}, bf16[2048,2]{0,1:T(2,128)(2,1)}, u32[]{:S(2)}) copy-start(bf16[2048,2]{0,1:T(2,128)(2,1)} %param.43) | copy-start | bytes 24580
  24.0 1.6 %copy-start.8 = (bf16[1,3,32,512]{3,2,0,1:T(8,128)(2,1)}, bf16[1,3,32,512]{3,2,0,1:T(8,128)(2,1)S(1)}, u32[]{:S(2)}) copy-start(bf16[1,3,32,512]{3,2,0,1:T(8,128)(2,1)S(1)} %collective-permute-done.14) | copy-start | bytes 294916
  24.0 67.1 %collective-permute-start.4 = (bf16[256,512]{1,0:T(8,128)(2,1)}, bf16[256,512]{1,0:T(8,128)(2,1)S(1)}, u32[]{:S(2)}, u32[]{:S(2)}) collective-permute-start(bf16[256,512]{1,0:T(8,128)(2,1)} %get-tuple-element.56), channel_id=1, source_target_pairs={{0,2},{1,3},{2,0},{3,1},{4,6},{5,7},{6,4},{7,5},{8,10},{9,11},{10,... | collective-permute-start | bytes 786440 | tf_op jit(solution)/shard_map/ppermute | solution.py:21
  25.6 65.5 %collective-permute-start.5 = (bf16[256,512]{1,0:T(8,128)(2,1)}, bf16[256,512]{1,0:T(8,128)(2,1)S(1)}, u32[]{:S(2)}, u32[]{:S(2)}) collective-permute-start(bf16[256,512]{1,0:T(8,128)(2,1)} %get-tuple-element.53), channel_id=1, source_target_pairs={{0,3},{1,0},{2,1},{3,2},{4,7},{5,4},{6,5},{7,6},{8,11},{9,8},{10,9... | collective-permute-start | bytes 786440 | tf_op jit(solution)/shard_map/ppermute | solution.py:21
  27.5 55.1 %collective-permute-start.15 = (bf16[2,3,32,512]{3,2,0,1:T(8,128)(2,1)}, bf16[2,3,32,512]{3,2,0,1:T(8,128)(2,1)}, u32[]{:S(2)}, u32[]{:S(2)}) collective-permute-start(bf16[2,3,32,512]{3,2,0,1:T(8,128)(2,1)} %pad_maximum_fusion), channel_id=1, source_target_pairs={{0,64},{32,96},{64,0},{96,32},{128,192},{160,224},{192,128},{224,1... | collective-permute-start | bytes 589832 | tf_op jit(solution)/shard_map/ppermute | solution.py:48
  31.9 46.0 %copy-start.3 = (bf16[32,2560]{1,0:T(8,128)(2,1)}, bf16[32,2560]{1,0:T(8,128)(2,1)S(1)}, u32[]{:S(2)}) copy-start(bf16[32,2560]{1,0:T(8,128)(2,1)S(1)} %get-tuple-element.32) | copy-start | bytes 491524
  31.9 59.2 %all-to-all-start = ((bf16[64,8,1024]{2,1,0:T(8,128)(2,1)}), bf16[64,8,1024]{2,1,0:T(8,128)(2,1)S(1)}, u32[]{:S(2)}, u32[]{:S(2)}) async-start(bf16[64,8,1024]{2,1,0:T(8,128)(2,1)} %bitcast.6), calls=%async_computation | async-start | bytes 2097152 | tf_op jit(solution)/shard_map/all_to_all | solution.py:472
  41.7 23.4 %collective-permute-start.9 = (bf16[32,512]{1,0:T(8,128)(2,1)S(1)}, bf16[32,512]{1,0:T(8,128)(2,1)S(1)}, u32[]{:S(2)}, u32[]{:S(2)}) collective-permute-start(bf16[32,512]{1,0:T(8,128)(2,1)S(1)} %get-tuple-element.45), channel_id=1, source_target_pairs={{0,32},{32,0},{64,96},{96,64},{128,160},{160,128},{192,224},{224,1... | collective-permute-start | bytes 98312 | tf_op jit(solution)/shard_map/ppermute | solution.py:48
  65.1 5.7 %collective-permute-start.10 = (bf16[64,512]{1,0:T(8,128)(2,1)S(1)}, bf16[64,512]{1,0:T(8,128)(2,1)S(1)}, u32[]{:S(2)}, u32[]{:S(2)}) collective-permute-start(bf16[64,512]{1,0:T(8,128)(2,1)S(1)} %get-tuple-element.70), channel_id=1, source_target_pairs={{0,8},{8,16},{16,24},{24,0},{1,9},{9,17},{17,25},{25,1},{2,10},{10... | collective-permute-start | bytes 196616 | tf_op jit(solution)/shard_map/ppermute | solution.py:21
  70.8 5.8 %collective-permute-start.11 = (bf16[64,512]{1,0:T(8,128)(2,1)S(1)}, bf16[64,512]{1,0:T(8,128)(2,1)S(1)}, u32[]{:S(2)}, u32[]{:S(2)}) collective-permute-start(bf16[64,512]{1,0:T(8,128)(2,1)S(1)} %get-tuple-element.70), channel_id=1, source_target_pairs={{0,16},{8,24},{16,0},{24,8},{1,17},{9,25},{17,1},{25,9},{2,18},{10... | collective-permute-start | bytes 196616 | tf_op jit(solution)/shard_map/ppermute | solution.py:21
  76.6 4.3 %collective-permute-start.12 = (bf16[64,512]{1,0:T(8,128)(2,1)S(1)}, bf16[64,512]{1,0:T(8,128)(2,1)S(1)}, u32[]{:S(2)}, u32[]{:S(2)}) collective-permute-start(bf16[64,512]{1,0:T(8,128)(2,1)S(1)} %get-tuple-element.70), channel_id=1, source_target_pairs={{0,24},{8,0},{16,8},{24,16},{1,25},{9,1},{17,9},{25,17},{2,26},{10... | collective-permute-start | bytes 196616 | tf_op jit(solution)/shard_map/ppermute | solution.py:21
  77.8 13.2 %copy-start.1 = (bf16[1,2048,256]{2,1,0:T(8,128)(2,1)S(1)}, bf16[1,2048,256]{2,1,0:T(8,128)(2,1)}, u32[]{:S(2)}) copy-start(bf16[1,2048,256]{2,1,0:T(8,128)(2,1)} %param.46) | copy-start | bytes 3145732
  80.9 2.8 %collective-permute-start.13 = (bf16[256,512]{1,0:T(8,128)(2,1)S(1)}, bf16[256,512]{1,0:T(8,128)(2,1)S(1)}, u32[]{:S(2)}, u32[]{:S(2)}) collective-permute-start(bf16[256,512]{1,0:T(8,128)(2,1)S(1)} %get-tuple-element.62), channel_id=1, source_target_pairs={{0,4},{4,0},{1,5},{5,1},{2,6},{6,2},{3,7},{7,3},{8,12},{12,8},{9,1... | collective-permute-start | bytes 786440 | tf_op jit(solution)/shard_map/ppermute | solution.py:48
  83.7 3.9 %copy-start.4 = (bf16[3,4,32,512]{3,2,1,0:T(8,128)(2,1)}, bf16[3,4,32,512]{3,2,1,0:T(8,128)(2,1)S(1)}, u32[]{:S(2)}) copy-start(bf16[3,4,32,512]{3,2,1,0:T(8,128)(2,1)S(1)} %maximum_bitcast_fusion) | copy-start | bytes 1179652
  84.8 15.9 %collective-permute-start.16 = (bf16[512,256]{1,0:T(8,128)(2,1)}, bf16[512,256]{1,0:T(8,128)(2,1)}, u32[]{:S(2)}, u32[]{:S(2)}) collective-permute-start(bf16[512,256]{1,0:T(8,128)(2,1)} %convolution_convert_fusion.1), channel_id=1, source_target_pairs={{0,1},{1,2},{2,3},{3,0},{4,5},{5,6},{6,7},{7,4},{8,9},{9,10},{10,1... | collective-permute-start | bytes 786440 | tf_op jit(solution)/shard_map/ppermute | solution.py:21
  85.6 15.0 %collective-permute-start.17 = (bf16[512,256]{1,0:T(8,128)(2,1)}, bf16[512,256]{1,0:T(8,128)(2,1)}, u32[]{:S(2)}, u32[]{:S(2)}) collective-permute-start(bf16[512,256]{1,0:T(8,128)(2,1)} %convolution_convert_fusion.1), channel_id=1, source_target_pairs={{0,2},{1,3},{2,0},{3,1},{4,6},{5,7},{6,4},{7,5},{8,10},{9,11},{10,... | collective-permute-start | bytes 786440 | tf_op jit(solution)/shard_map/ppermute | solution.py:21
  87.6 13.7 %collective-permute-start.18 = (bf16[512,256]{1,0:T(8,128)(2,1)}, bf16[512,256]{1,0:T(8,128)(2,1)}, u32[]{:S(2)}, u32[]{:S(2)}) collective-permute-start(bf16[512,256]{1,0:T(8,128)(2,1)} %convolution_convert_fusion.1), channel_id=1, source_target_pairs={{0,3},{1,0},{2,1},{3,2},{4,7},{5,4},{6,5},{7,6},{8,11},{9,8},{10,9... | collective-permute-start | bytes 786440 | tf_op jit(solution)/shard_map/ppermute | solution.py:21
  91.1 1.2 copy-start.2
  92.3 10.3 %slice-start = ((bf16[3,4,32,512]{3,2,1,0:T(8,128)(2,1)}), bf16[1,4,32,512]{3,2,1,0:T(8,128)(2,1)S(1)}, s32[]{:S(2)}) async-start(bf16[3,4,32,512]{3,2,1,0:T(8,128)(2,1)} %copy-done.4), calls=%async_computation.2 | async-start | bytes 262144 | tf_op jit(solution)/shard_map/slice | solution.py:482
  102.9 23.2 %copy-start.19 = (bf16[512]{0:T(512)(128)(2,1)S(1)}, bf16[512]{0:T(512)(128)(2,1)}, u32[]{:S(2)}) copy-start(bf16[512]{0:T(512)(128)(2,1)} %param.53) | copy-start | bytes 3076
  102.9 5.6 %collective-permute-start.19 = (bf16[256,512]{1,0:T(8,128)(2,1)S(1)}, bf16[256,512]{1,0:T(8,128)(2,1)S(1)}, u32[]{:S(2)}, u32[]{:S(2)}) collective-permute-start(bf16[256,512]{1,0:T(8,128)(2,1)S(1)} %slice.70), channel_id=1, source_target_pairs={{0,4},{4,0},{1,5},{5,1},{2,6},{6,2},{3,7},{7,3},{8,12},{12,8},{9,1... | collective-permute-start | bytes 786440 | tf_op jit(solution)/shard_map/ppermute | solution.py:48
  103.0 8.1 %collective-permute-start.6 = (bf16[256,256]{1,0:T(8,128)(2,1)S(1)}, bf16[256,256]{1,0:T(8,128)(2,1)S(1)}, u32[]{:S(2)}, u32[]{:S(2)}) collective-permute-start(bf16[256,256]{1,0:T(8,128)(2,1)S(1)} %get-tuple-element.40.refs_0_), channel_id=1, source_target_pairs={{0,1},{1,2},{2,3},{3,0},{4,5},{5,6},{6,7},{7,4},{8,9},{9,10},{10,1... | collective-permute-start | bytes 393224 | tf_op jit(solution)/shard_map/ppermute | solution.py:21
  104.8 9.0 %collective-permute-start.7 = (bf16[256,256]{1,0:T(8,128)(2,1)S(1)}, bf16[256,256]{1,0:T(8,128)(2,1)S(1)}, u32[]{:S(2)}, u32[]{:S(2)}) collective-permute-start(bf16[256,256]{1,0:T(8,128)(2,1)S(1)} %get-tuple-element.40.refs_0_), channel_id=1, source_target_pairs={{0,2},{1,3},{2,0},{3,1},{4,6},{5,7},{6,4},{7,5},{8,10},{9,11},{10,... | collective-permute-start | bytes 393224 | tf_op jit(solution)/shard_map/ppermute | solution.py:21
  107.2 6.6 %collective-permute-start.8 = (bf16[256,256]{1,0:T(8,128)(2,1)S(1)}, bf16[256,256]{1,0:T(8,128)(2,1)S(1)}, u32[]{:S(2)}, u32[]{:S(2)}) collective-permute-start(bf16[256,256]{1,0:T(8,128)(2,1)S(1)} %get-tuple-element.40.refs_0_), channel_id=1, source_target_pairs={{0,3},{1,0},{2,1},{3,2},{4,7},{5,4},{6,5},{7,6},{8,11},{9,8},{10,9... | collective-permute-start | bytes 393224 | tf_op jit(solution)/shard_map/ppermute | solution.py:21
  108.6 29.8 %copy-start.9 = (bf16[256,32]{1,0:T(8,128)(2,1)S(1)}, bf16[256,32]{1,0:T(8,128)(2,1)}, u32[]{:S(2)}) copy-start(bf16[256,32]{1,0:T(8,128)(2,1)} %get-tuple-element.42) | copy-start | bytes 49156
  108.6 17.5 %collective-permute-start.20 = (bf16[4,32,512]{2,1,0:T(8,128)(2,1)S(1)}, bf16[4,32,512]{2,1,0:T(8,128)(2,1)S(1)}, u32[]{:S(2)}, u32[]{:S(2)}) collective-permute-start(bf16[4,32,512]{2,1,0:T(8,128)(2,1)S(1)} %slice_bitcast_fusion), channel_id=1, source_target_pairs={{0,32},{32,0},{64,96},{96,64},{128,160},{160,128},{192,224},{224,1... | collective-permute-start | bytes 393224 | tf_op jit(solution)/shard_map/ppermute | solution.py:48
  113.8 32.5 %copy-start.10 = (f32[32,512]{1,0:T(8,128)S(1)}, f32[32,512]{1,0:T(8,128)}, u32[]{:S(2)}) copy-start(f32[32,512]{1,0:T(8,128)} %slice_convert_fusion) | copy-start | bytes 196612
  115.0 23.3 %all-to-all-start.1 = ((bf16[64,4,512]{2,1,0:T(4,128)(2,1)}), bf16[64,4,512]{2,1,0:T(4,128)(2,1)S(1)}, u32[]{:S(2)}, u32[]{:S(2)}) async-start(bf16[64,4,512]{2,1,0:T(4,128)(2,1)} %reshape.57), calls=%async_computation.1 | async-start | bytes 524288 | tf_op jit(solution)/shard_map/all_to_all | solution.py:543
  126.1 12.4 %collective-permute-start.21 = (bf16[32,512]{1,0:T(8,128)(2,1)S(1)}, bf16[32,512]{1,0:T(8,128)(2,1)S(1)}, u32[]{:S(2)}, u32[]{:S(2)}) collective-permute-start(bf16[32,512]{1,0:T(8,128)(2,1)S(1)} %get-tuple-element.59), channel_id=1, source_target_pairs={{0,24},{8,0},{16,8},{24,16},{1,25},{9,1},{17,9},{25,17},{2,26},{10... | collective-permute-start | bytes 98312 | tf_op jit(solution)/shard_map/ppermute | solution.py:21
  128.9 9.6 %collective-permute-start.22 = (bf16[32,512]{1,0:T(8,128)(2,1)S(1)}, bf16[32,512]{1,0:T(8,128)(2,1)S(1)}, u32[]{:S(2)}, u32[]{:S(2)}) collective-permute-start(bf16[32,512]{1,0:T(8,128)(2,1)S(1)} %get-tuple-element.61), channel_id=1, source_target_pairs={{0,16},{8,24},{16,0},{24,8},{1,17},{9,25},{17,1},{25,9},{2,18},{10... | collective-permute-start | bytes 98312 | tf_op jit(solution)/shard_map/ppermute | solution.py:21
  129.8 8.8 %collective-permute-start.23 = (bf16[32,512]{1,0:T(8,128)(2,1)S(1)}, bf16[32,512]{1,0:T(8,128)(2,1)S(1)}, u32[]{:S(2)}, u32[]{:S(2)}) collective-permute-start(bf16[32,512]{1,0:T(8,128)(2,1)S(1)} %get-tuple-element.60), channel_id=1, source_target_pairs={{0,8},{8,16},{16,24},{24,0},{1,9},{9,17},{17,25},{25,1},{2,10},{10... | collective-permute-start | bytes 98312 | tf_op jit(solution)/shard_map/ppermute | solution.py:21
  138.8 5.3 %collective-permute-start.24 = (f32[32]{0:T(128)S(1)}, f32[32]{0:T(128)S(1)}, u32[]{:S(2)}, u32[]{:S(2)}) collective-permute-start(f32[32]{0:T(128)S(1)} %get-tuple-element.83), channel_id=1, source_target_pairs={{0,1},{1,2},{2,3},{3,0},{4,5},{5,6},{6,7},{7,4},{8,9},{9,10},{10,1... | collective-permute-start | bytes 392 | tf_op jit(solution)/shard_map/ppermute | solution.py:21
  140.4 5.1 %collective-permute-start.25 = (f32[32]{0:T(128)S(1)}, f32[32]{0:T(128)S(1)}, u32[]{:S(2)}, u32[]{:S(2)}) collective-permute-start(f32[32]{0:T(128)S(1)} %get-tuple-element.83), channel_id=1, source_target_pairs={{0,2},{1,3},{2,0},{3,1},{4,6},{5,7},{6,4},{7,5},{8,10},{9,11},{10,... | collective-permute-start | bytes 392 | tf_op jit(solution)/shard_map/ppermute | solution.py:21
  142.8 3.6 %collective-permute-start.26 = (f32[32]{0:T(128)S(1)}, f32[32]{0:T(128)S(1)}, u32[]{:S(2)}, u32[]{:S(2)}) collective-permute-start(f32[32]{0:T(128)S(1)} %get-tuple-element.83), channel_id=1, source_target_pairs={{0,3},{1,0},{2,1},{3,2},{4,7},{5,4},{6,5},{7,6},{8,11},{9,8},{10,9... | collective-permute-start | bytes 392 | tf_op jit(solution)/shard_map/ppermute | solution.py:21
